TPU v7x, 128 devices: a whole 4x4x4 slice. The times are simulated.
128 devices in a mesh: sp: 16 (over z, x), tp: 8 (over y, core).
Axes of the slice: x: 4, y: 4, z: 4, core: 2. Of those that a mesh axis runs over, the one named last changes fastest.
Arguments:
- latent: bfloat16 [2, 8192, 2048], P(None, ('sp', 'tp')), may hold values from -6 to 6
- context: bfloat16 [2, 1024, 2048], P(None, 'sp'), may hold values from -6 to 6
- cond: bfloat16 [2, 2048], replicated, may hold values from -6 to 6
- ctx_cond: bfloat16 [2048], replicated, may hold values from -6 to 6
- w_shift: bfloat16 [2048, 2048], P('sp', 'tp'), may hold values from -0.125 to 0.125
- w_scale: bfloat16 [2048, 2048], P('sp', 'tp'), may hold values from -0.125 to 0.125
- w_gate: bfloat16 [2048, 2048], P('sp', 'tp'), may hold values from -0.125 to 0.125
- norm_gain: float32 [2048], replicated, may hold values from 0.1 to 1.9
- w_query: bfloat16 [2048, 2048], P(None, 'tp'), may hold values from -1.08275726 to 1.08275726
- w_key: bfloat16 [2048, 2048], P(None, 'tp'), may hold values from -0.090598056 to 0.090598056
- w_value: bfloat16 [2048, 2048], P(None, 'tp'), may hold values from -0.125 to 0.125
- w_out: bfloat16 [2048, 2048], P('tp'), may hold values from -1.5 to 1.5
- rel_bias: float32 [32, 15, 31], P('tp'), may hold values from -4 to 4
- ctx_bias: float32 [32], P('tp'), may hold values from -3.5 to -2
Outputs:
- mixed: bfloat16 [2, 8192, 2048], P(None, ('sp', 'tp'))
All inputs are finite; a program needn't handle non-finite values.
Results may differ from a plain program's by a relative error of at most 0.0154.
Values may be sent and summed in bfloat16 or wider, within the bound.
No kernel may reach another device: no remote copies, remote signals or barrier semaphores. Data moves between devices by JAX's collectives and lax.ppermute only.
A program may use at most 128 MiB of HBM per device.

v0:
```python
import jax
import jax.numpy as jnp
from jax import lax
from jax.sharding import PartitionSpec as P

HEAD_DIM = 64
GRID_W = 64
WIN_ROWS = 8
WIN_COLS = 16


EPSILON = 1e-06


def copy_for_each(shard, axis):
    length = lax.axis_size(axis)
    return lax.all_to_all(
        jnp.broadcast_to(shard[None], (length, *shard.shape)), axis, 0, 0, tiled=True
    )


def of_everyone(shard, axis):
    everything = copy_for_each(shard, axis)
    return jnp.sum(everything, axis=0)


def laid_out(tiles, dim):
    tiles = jnp.moveaxis(tiles, 0, dim)
    lengths = tiles.shape
    return tiles.reshape(*lengths[:dim], lengths[dim] * lengths[dim + 1], *lengths[dim + 2 :])


def gather_directly(shard, axis, dim):
    tiles = copy_for_each(shard, axis)
    return laid_out(tiles, dim)


def extended(shard, sides, width):
    for axis, dim in sides:
        size, length = (lax.axis_size(axis), shard.shape[dim])
        up = [(i, (i + 1) % size) for i in range(size - 1)]
        down = [(j, i) for i, j in up]
        last = lax.slice_in_dim(shard, length - width, length, axis=dim)
        first = lax.slice_in_dim(shard, 0, width, axis=dim)
        before = lax.ppermute(last, axis, up)
        after = lax.ppermute(first, axis, down)
        shard = jnp.concatenate([before, shard, after], axis=dim)
    return shard


def silu_rows(values):
    return jax.nn.silu(values.astype(jnp.float32)).astype(jnp.bfloat16)


def modulate_rows(rows, gain, shift, scale):
    floats = rows.astype(jnp.float32)
    inverse = lax.rsqrt(jnp.mean(floats * floats, axis=-1, keepdims=True) + EPSILON)
    return (floats * inverse * gain * (1.0 + scale) + shift).astype(jnp.bfloat16)


def on_device(
    latent,
    context,
    cond,
    ctx_cond,
    w_shift,
    w_scale,
    w_gate,
    norm_gain,
    w_query,
    w_key,
    w_value,
    w_out,
    rel_bias,
    ctx_bias,
):
    samples = latent.shape[0]
    rows_sp = w_shift.shape[0]
    local_cols = w_shift.shape[1]
    sp_index = lax.axis_index("sp")
    ada = silu_rows(jnp.concatenate([cond, ctx_cond[None, :]], axis=0))
    ada_rows = lax.dynamic_slice_in_dim(ada, sp_index * rows_sp, rows_sp, 1)
    partial_value = jnp.stack(
        [
            jnp.dot(ada_rows, weight, preferred_element_type=jnp.float32)
            for weight in (w_shift, w_scale, w_gate)
        ]
    )
    summed = of_everyone(partial_value, "sp")
    modulation = gather_directly(summed, "tp", 2)
    hidden = modulate_rows(
        latent, norm_gain, modulation[0, :samples, None, :], modulation[1, :samples, None, :]
    )
    w_triple = jnp.concatenate([w_query, w_key, w_value], axis=1)
    triple = jnp.dot(
        lax.all_gather(hidden, "tp", axis=1, tiled=True),
        w_triple,
        preferred_element_type=jnp.float32,
    ).astype(jnp.bfloat16)
    ctx_hidden = modulate_rows(context, norm_gain, modulation[0, samples], modulation[1, samples])
    w_pair = jnp.concatenate([w_key, w_value], axis=1)
    ctx_pair = jnp.dot(
        lax.all_gather(ctx_hidden, "sp", axis=1, tiled=True),
        w_pair,
        preferred_element_type=jnp.float32,
    ).astype(jnp.bfloat16)
    heads = local_cols // HEAD_DIM
    tokens_sp = triple.shape[1]
    rows_dev = tokens_sp // GRID_W
    rows_all = rows_dev * lax.axis_size("sp")
    blocks = GRID_W // WIN_COLS
    span = 2 * WIN_COLS
    reach = WIN_ROWS // 2
    padded_count = rows_dev + 2 * reach
    query = triple[..., :local_cols].reshape(samples, rows_dev, GRID_W, local_cols)
    pair = triple[..., local_cols:].reshape(samples, rows_dev, GRID_W, 2 * local_cols)
    padded_pair = extended(pair, (("sp", 1),), reach)
    global_row = sp_index * rows_dev + jnp.arange(rows_dev, dtype=jnp.int32)
    start_row = jnp.clip(global_row - reach, 0, rows_all - WIN_ROWS)
    key_row = sp_index * rows_dev - reach + jnp.arange(padded_count, dtype=jnp.int32)
    row_inside = (key_row[None, :] >= start_row[:, None]) & (
        key_row[None, :] < start_row[:, None] + WIN_ROWS
    )
    row_offset = key_row[None, :] - global_row[:, None] + WIN_ROWS - 1
    row_onehot = (
        row_offset[:, :, None] == jnp.arange(2 * WIN_ROWS - 1, dtype=jnp.int32)[None, None, :]
    ).astype(jnp.float32)
    ctx_count = ctx_pair.shape[1]
    ctx_view = ctx_pair.reshape(samples, ctx_count, 2, heads, HEAD_DIM)
    factor = HEAD_DIM ** (-0.5)
    queries_block = rows_dev * WIN_COLS
    keys_block = padded_count * span
    results = []
    for block in range(blocks):
        first = min(max(WIN_COLS * block - WIN_COLS // 2, 0), GRID_W - span)
        query_col = WIN_COLS * block + jnp.arange(WIN_COLS, dtype=jnp.int32)
        key_col = first + jnp.arange(span, dtype=jnp.int32)
        col_start = jnp.clip(query_col - WIN_COLS // 2, 0, GRID_W - WIN_COLS)
        col_inside = (key_col[None, :] >= col_start[:, None]) & (
            key_col[None, :] < col_start[:, None] + WIN_COLS
        )
        col_onehot = (
            key_col[None, :, None] - query_col[:, None, None] + WIN_COLS - 1
            == jnp.arange(2 * WIN_COLS - 1, dtype=jnp.int32)[None, None, :]
        ).astype(jnp.float32)
        bias = jnp.einsum(
            "rpa,hac,qkc->hrqpk", row_onehot, rel_bias, col_onehot, precision=lax.Precision.HIGHEST
        )
        bias = bias.reshape(heads, queries_block, keys_block)
        inside = (row_inside[:, None, :, None] & col_inside[None, :, None, :]).reshape(
            queries_block, keys_block
        )
        block_query = query[:, :, WIN_COLS * block : WIN_COLS * (block + 1)].reshape(
            samples, queries_block, heads, HEAD_DIM
        )
        block_pair = padded_pair[:, :, first : first + span].reshape(
            samples, keys_block, 2, heads, HEAD_DIM
        )
        near = (
            jnp.einsum(
                "snhd,skhd->shnk",
                block_query,
                block_pair[:, :, 0],
                preferred_element_type=jnp.float32,
            )
            * factor
            + bias[None]
        )
        near = jnp.where(inside[None, None], near, -jnp.inf)
        far = (
            jnp.einsum(
                "snhd,schd->shnc",
                block_query,
                ctx_view[:, :, 0],
                preferred_element_type=jnp.float32,
            )
            * factor
            + ctx_bias[None, :, None, None]
        )
        top = jnp.maximum(jnp.max(near, axis=-1), jnp.max(far, axis=-1))[..., None]
        near_exp = jnp.exp(near - top)
        far_exp = jnp.exp(far - top)
        total = jnp.sum(near_exp, axis=-1, keepdims=True) + jnp.sum(far_exp, axis=-1, keepdims=True)
        near_weight = (near_exp / total).astype(jnp.bfloat16)
        far_weight = (far_exp / total).astype(jnp.bfloat16)
        mixed_near = jnp.einsum(
            "shnk,skhd->snhd", near_weight, block_pair[:, :, 1], preferred_element_type=jnp.float32
        )
        mixed_far = jnp.einsum(
            "shnc,schd->snhd", far_weight, ctx_view[:, :, 1], preferred_element_type=jnp.float32
        )
        results.append(
            (mixed_near + mixed_far)
            .astype(jnp.bfloat16)
            .reshape(samples, rows_dev, WIN_COLS, local_cols)
        )
    attended = jnp.stack(results, axis=2).reshape(samples, tokens_sp, local_cols).transpose(1, 0, 2)
    update = lax.psum_scatter(
        jnp.einsum("tsc,cd->tsd", attended, w_out, preferred_element_type=jnp.float32).astype(
            jnp.bfloat16
        ),
        "tp",
        scatter_dimension=0,
        tiled=True,
    ).astype(jnp.float32)
    gate = modulation[2, :samples, None, :]
    result = latent.astype(jnp.float32) + gate * update.transpose(1, 0, 2)
    return result.astype(jnp.bfloat16)


def solution(mesh):
    return jax.shard_map(
        on_device,
        mesh=mesh,
        in_specs=(
            P(None, ("sp", "tp"), None),
            P(None, "sp", None),
            P(),
            P(),
            P("sp", "tp"),
            P("sp", "tp"),
            P("sp", "tp"),
            P(),
            P(None, "tp"),
            P(None, "tp"),
            P(None, "tp"),
            P("tp", None),
            P("tp", None, None),
            P("tp"),
        ),
        out_specs=P(None, ("sp", "tp"), None),
        check_vma=False,
    )
```

profile of v0, /device:TPU:0, one launch (start us, length us, event | category | flops | bytes accessed | tf_op | source)
XLA Modules:
  0.0 255.1 jit_solution(4507588202694883402)
XLA Ops:
  11.7 8.0 %all-to-all-start = ((f32[16,3,3,256]{3,2,1,0:T(4,128)}), f32[16,3,3,256]{3,2,1,0:T(4,128)S(1)}, u32[]{:S(2)}, u32[]{:S(2)}) async-start(f32[16,3,3,256]{3,2,1,0:T(4,128)} %broadcast_in_dim.33), calls=%async_computation | async-start | bytes 393216 | tf_op jit(solution)/shard_map/all_to_all | solution.py:17
  22.2 5.9 %all-to-all-done = f32[16,3,3,256]{3,2,1,0:T(4,128)S(1)} async-done(((f32[16,3,3,256]{3,2,1,0:T(4,128)}), f32[16,3,3,256]{3,2,1,0:T(4,128)S(1)}, u32[]{:S(2)}, u32[]{:S(2)}) %all-to-all-start) | async-done | bytes 147488 | tf_op jit(solution)/shard_map/all_to_all | solution.py:17
  28.8 4.5 %all-to-all-start.1 = ((f32[8,3,3,256]{3,2,1,0:T(4,128)}), f32[8,3,3,256]{3,2,1,0:T(4,128)S(1)}, u32[]{:S(2)}, u32[]{:S(2)}) async-start(f32[8,3,3,256]{3,2,1,0:T(4,128)} %broadcast_in_dim.34), calls=%async_computation.1 | async-start | bytes 196608 | tf_op jit(solution)/shard_map/all_to_all | solution.py:17
  33.3 5.7 %all-to-all-done.1 = f32[8,3,3,256]{3,2,1,0:T(4,128)S(1)} async-done(((f32[8,3,3,256]{3,2,1,0:T(4,128)}), f32[8,3,3,256]{3,2,1,0:T(4,128)S(1)}, u32[]{:S(2)}, u32[]{:S(2)}) %all-to-all-start.1) | async-done | bytes 73760 | tf_op jit(solution)/shard_map/all_to_all | solution.py:17
  39.2 2.1 fusion.38
  47.9 2.4 copy.161
  54.6 2.6 %copy.185 = f32[4,8,16,16,32]{4,3,2,1,0:T(8,128)} copy(f32[4,8,16,16,32]{4,3,1,0,2:T(8,128)S(1)} %convolution_bitcast_fusion) | data formatting | bytes 2097152 | tf_op jit(solution)/shard_map/rpa,hac,qkc->hrqpk/transpose | solution.py:146
  57.2 4.4 %add.477 = f32[4,128,512]{2,1,0:T(8,128)} reshape(f32[4,8,16,16,32]{4,3,2,1,0:T(8,128)} %copy.185) | data formatting | bytes 2097152 | tf_op jit(solution)/shard_map/add | solution.py:160
  64.4 2.6 %copy.178 = f32[4,8,16,16,32]{4,3,2,1,0:T(8,128)} copy(f32[4,8,16,16,32]{4,3,1,0,2:T(8,128)S(1)} %convolution_bitcast_fusion.1) | data formatting | bytes 2097152 | tf_op jit(solution)/shard_map/rpa,hac,qkc->hrqpk/transpose | solution.py:146
  67.0 4.4 %add.467 = f32[4,128,512]{2,1,0:T(8,128)} reshape(f32[4,8,16,16,32]{4,3,2,1,0:T(8,128)} %copy.178) | data formatting | bytes 2097152 | tf_op jit(solution)/shard_map/add | solution.py:160
  74.1 2.6 %copy.171 = f32[4,8,16,16,32]{4,3,2,1,0:T(8,128)} copy(f32[4,8,16,16,32]{4,3,1,0,2:T(8,128)S(1)} %convolution_bitcast_fusion.2) | data formatting | bytes 2097152 | tf_op jit(solution)/shard_map/rpa,hac,qkc->hrqpk/transpose | solution.py:146
  76.7 4.9 %add.457 = f32[4,128,512]{2,1,0:T(8,128)} reshape(f32[4,8,16,16,32]{4,3,2,1,0:T(8,128)} %copy.171) | data formatting | bytes 2097152 | tf_op jit(solution)/shard_map/add | solution.py:160
  82.5 6.2 %fusion.25 = bf16[2,512,768]{2,1,0:T(8,128)(2,1)S(1)} fusion(bf16[2,512,2048]{2,1,0:T(8,128)(2,1)} %all-gather.3.cloned.1.call-done, bf16[2048,256]{1,0:T(8,128)(2,1)S(1)} %copy-done.14, bf16[2048,256]{1,0:T(8,128)(2,1)} %param.23, bf16[2048,256]{1,0:T(8,128)(2,1)} %param.22), kind=kOutput, calls=%fused_computation.57 | convolution fusion | flops 3231449088 | bytes 8912896 | tf_op jit(solution)/shard_map/dot_general | solution.py:95
  89.8 3.5 %collective-permute-start = (bf16[2,4,64,512]{3,2,1,0:T(8,128)(2,1)}, bf16[2,4,64,512]{3,2,1,0:T(8,128)(2,1)}, u32[]{:S(2)}, u32[]{:S(2)}) collective-permute-start(bf16[2,4,64,512]{3,2,1,0:T(8,128)(2,1)} %get-tuple-element.24), channel_id=1, source_target_pairs={{0,8},{8,16},{16,24},{24,32},{32,40},{40,48},{48,56},{56,64},{64,7... | collective-permute-start | bytes 1572872 | tf_op jit(solution)/shard_map/ppermute | solution.py:45
  96.5 2.6 %copy.160 = f32[4,8,16,16,32]{4,3,2,1,0:T(8,128)} copy(f32[4,8,16,16,32]{4,3,1,0,2:T(8,128)S(1)} %convolution_bitcast_fusion.3) | data formatting | bytes 2097152 | tf_op jit(solution)/shard_map/rpa,hac,qkc->hrqpk/transpose | solution.py:146
  99.1 4.4 %add.440 = f32[4,128,512]{2,1,0:T(8,128)} reshape(f32[4,8,16,16,32]{4,3,2,1,0:T(8,128)} %copy.160) | data formatting | bytes 2097152 | tf_op jit(solution)/shard_map/add | solution.py:160
  110.1 2.1 fusion.103
  112.2 3.6 %reshape.670 = bf16[2,512,2,4,64]{4,3,2,1,0:T(4,128)(2,1)S(1)} reshape(bf16[2,16,32,512]{3,2,1,0:T(8,128)(2,1)} %get-tuple-element.20) | data formatting | bytes 2097152 | tf_op jit(solution)/shard_map/reshape | solution.py:156
  115.9 2.0 fusion.101
  117.9 2.3 copy.205
  120.2 2.3 copy.206
  122.5 3.6 %reshape.672 = bf16[2,512,2,4,64]{4,3,2,1,0:T(4,128)(2,1)S(1)} reshape(bf16[2,16,32,512]{3,2,1,0:T(8,128)(2,1)} %get-tuple-element.21) | data formatting | bytes 2097152 | tf_op jit(solution)/shard_map/reshape | solution.py:156
  126.0 2.1 fusion.102
  128.1 2.3 copy.207
  130.4 2.3 copy.208
  132.7 3.6 %reshape.668 = bf16[2,512,2,4,64]{4,3,2,1,0:T(4,128)(2,1)S(1)} reshape(bf16[2,16,32,512]{3,2,1,0:T(8,128)(2,1)} %get-tuple-element.22) | data formatting | bytes 2097152 | tf_op jit(solution)/shard_map/reshape | solution.py:156
  136.2 2.1 fusion.100
  138.3 2.3 copy.203
  140.6 2.3 copy.204
  142.8 3.7 %reshape.664 = bf16[2,512,2,4,64]{4,3,2,1,0:T(4,128)(2,1)S(1)} reshape(bf16[2,16,32,512]{3,2,1,0:T(8,128)(2,1)} %get-tuple-element.23) | data formatting | bytes 2097152 | tf_op jit(solution)/shard_map/reshape | solution.py:156
  146.5 2.1 fusion.99
  148.6 2.3 copy.199
  150.9 2.3 copy.200
  153.2 2.8 %fusion.106 = (f32[2,4,128]{2,1,0:T(4,128)}, f32[2,4,128,512]{3,2,1,0:T(8,128)S(1)}) fusion(f32[4,128,512]{2,1,0:T(8,128)} %add.477, bf16[2,128,4,64]{1,3,2,0:T(8,128)(2,1)} %copy.183, bf16[2,512,1,4,64]{1,4,3,0,2:T(8,128)(2,1)} %copy.208, pred[128,512]{1,0:T(8,128)(4,1)} %and.127), kind=kOutput, calls=%fused_computation.193 | convolution fusion | flops 69204992 | bytes 3870720 | tf_op jit(solution)/shard_map/snhd,skhd->shnk/dot_general | solution.py:160
  156.0 4.0 %fusion.109 = (f32[2,4,128]{2,1,0:T(4,128)}, f32[2,4,128,512]{3,2,1,0:T(8,128)}) fusion(f32[4,128,512]{2,1,0:T(8,128)} %add.467, bf16[2,128,4,64]{1,3,2,0:T(8,128)(2,1)S(1)} %copy.176, bf16[2,512,1,4,64]{1,4,3,0,2:T(8,128)(2,1)} %copy.206, pred[128,512]{1,0:T(8,128)(4,1)} %and.123), kind=kOutput, calls=%fused_computation.196 | convolution fusion | flops 69204992 | bytes 3870720 | tf_op jit(solution)/shard_map/snhd,skhd->shnk/dot_general | solution.py:160
  160.0 2.5 fusion.108
  162.5 2.6 %fusion.107 = (f32[2,4,128]{2,1,0:T(4,128)}, f32[2,4,128,512]{3,2,1,0:T(8,128)}) fusion(f32[4,128,512]{2,1,0:T(8,128)S(1)} %copy-done.7, bf16[2,128,4,64]{1,3,2,0:T(8,128)(2,1)S(1)} %copy.158, bf16[2,512,1,4,64]{1,4,3,0,2:T(8,128)(2,1)S(1)} %copy-done.10, pred[128,512]{1,0:T(8,128)(4,1)S(1)} %copy-done.18), kind=kOutput, calls=%fused_computation.194 | convolution fusion | flops 69204992 | bytes 3870720 | tf_op jit(solution)/shard_map/snhd,skhd->shnk/dot_general | solution.py:160
  165.1 8.4 %fusion.20 = bf16[2,1024,512]{1,2,0:T(8,128)(2,1)S(1)} fusion(bf16[2,1024,2048]{2,1,0:T(8,128)(2,1)} %all-gather.5.cloned.1.call-done, bf16[2048,256]{0,1:T(8,128)(2,1)} %copy.162, bf16[2048,256]{0,1:T(8,128)(2,1)} %copy.161), kind=kOutput, calls=%fused_computation.52 | convolution fusion | flops 4300210176 | bytes 12582912 | tf_op jit(solution)/shard_map/dot_general | solution.py:102
  177.4 3.3 %fusion.4 = (f32[2,4,128]{2,1,0:T(4,128)S(1)}, f32[2,4,128]{2,1,0:T(4,128)S(1)}, f32[2,4,128]{2,1,0:T(4,128)S(1)}, f32[2,4,128]{2,1,0:T(4,128)S(1)}, f32[2,4,128,1024]{3,2,1,0:T(8,128)S(1)}) fusion(f32[2,4,128,1024]{3,2,1,0:T(8,128)S(1)} %get-tuple-element.46, f32[2,4,128]{2,1,0:T(4,128)S(1)} %max.48, f32[4]{0:T(128)S(1)} %copy-done.28, ...), kind=kOutput, calls=%fused_computation.17 | convolution fusion | flops 147845120 | bytes 17977856 | tf_op jit(solution)/shard_map/snhd,schd->shnc/dot_general | solution.py:171
  180.8 2.2 fusion.16
  185.9 2.9 %fusion.5 = (f32[2,4,128]{2,1,0:T(4,128)S(1)}, f32[2,4,128]{2,1,0:T(4,128)S(1)}, f32[2,4,128]{2,1,0:T(4,128)S(1)}) fusion(f32[2,4,128,1024]{3,2,1,0:T(8,128)S(1)} %get-tuple-element.47, f32[2,4,128]{2,1,0:T(4,128)S(1)} %max.49, f32[4]{0:T(128)S(1)} %copy-done.28, f32[2,4,128]{2,1,0:T(4,128)S(1)} %max.50, f32[2,4,128,1024]{3,2,1,0:T(8,128)S(1)} %fusion.47, ...), kind=kLoop, calls=%fused_computation.18 | loop fusion | flops 12579840 | bytes 12607504 | tf_op jit(solution)/shard_map/reduce_sum | solution.py:183
  188.9 2.2 fusion.19
  191.1 2.2 fusion.17
  195.9 3.0 %fusion.32 = bf16[2,128,4,64]{1,3,2,0:T(8,128)(2,1)} fusion(f32[2,4,64,128]{3,2,1,0:T(8,128)} %fusion.17, f32[2,4,128,512]{3,2,1,0:T(8,128)} %get-tuple-element.49, f32[2,4,128]{2,1,0:T(4,128)} %copy-done.32, f32[2,4,128]{2,1,0:T(4,128)} %copy-done.23, bf16[2,512,1,4,64]{1,4,3,0,2:T(8,128)(2,1)} %copy.203), kind=kOutput, calls=%fused_computation.77 | convolution fusion | flops 68812800 | bytes 3022848 | tf_op jit(solution)/shard_map/shnk,skhd->snhd/dot_general | solution.py:186
  203.2 2.4 fusion.33
  206.2 3.2 %convolution_convert_fusion = bf16[512,2,2048]{2,0,1:T(8,128)(2,1)} fusion(bf16[512,2,256]{2,0,1:T(8,128)(2,1)S(1)} %bitcast.223, bf16[256,2048]{1,0:T(8,128)(2,1)S(1)} %copy-done), kind=kOutput, calls=%fused_computation.12 | convolution fusion | flops 1075838976 | bytes 5767168 | tf_op jit(solution)/shard_map/tsc,cd->tsd/dot_general | solution.py:199
  209.4 37.0 %reduce-scatter.2.cloned.1.call-done = bf16[64,2,2048]{2,0,1:T(8,128)(2,1)} async-done(((bf16[512,2,2048]{2,0,1:T(8,128)(2,1)}), bf16[64,2,2048]{2,0,1:T(8,128)(2,1)}) %reduce-scatter.2.cloned.1.call-update) | async-done | bytes 524304 | tf_op jit(solution)/shard_map/reduce_scatter | solution.py:198
  246.4 2.0 fusion.44
  (172 shorter events, 50.4 us)
Async XLA Ops:
  6.5 199.6 %copy-start = (bf16[256,2048]{1,0:T(8,128)(2,1)S(1)}, bf16[256,2048]{1,0:T(8,128)(2,1)}, u32[]{:S(2)}) copy-start(bf16[256,2048]{1,0:T(8,128)(2,1)} %param.25) | copy-start | bytes 3145732
  6.5 32.6 %copy-start.8 = (bf16[2,64,2048]{2,1,0:T(8,128)(2,1)S(1)}, bf16[2,64,2048]{2,1,0:T(8,128)(2,1)}, u32[]{:S(2)}) copy-start(bf16[2,64,2048]{2,1,0:T(8,128)(2,1)} %param.15) | copy-start | bytes 1572868
  6.5 32.6 %copy-start.4 = (bf16[2,64,2048]{2,1,0:T(8,128)(2,1)S(1)}, bf16[2,64,2048]{2,1,0:T(8,128)(2,1)}, u32[]{:S(2)}) copy-start(bf16[2,64,2048]{2,1,0:T(8,128)(2,1)} %param.14) | copy-start | bytes 1572868
  11.7 16.3 %all-to-all-start = ((f32[16,3,3,256]{3,2,1,0:T(4,128)}), f32[16,3,3,256]{3,2,1,0:T(4,128)S(1)}, u32[]{:S(2)}, u32[]{:S(2)}) async-start(f32[16,3,3,256]{3,2,1,0:T(4,128)} %broadcast_in_dim.33), calls=%async_computation | async-start | bytes 393216 | tf_op jit(solution)/shard_map/all_to_all | solution.py:17
  28.8 10.3 %all-to-all-start.1 = ((f32[8,3,3,256]{3,2,1,0:T(4,128)}), f32[8,3,3,256]{3,2,1,0:T(4,128)S(1)}, u32[]{:S(2)}, u32[]{:S(2)}) async-start(f32[8,3,3,256]{3,2,1,0:T(4,128)} %broadcast_in_dim.34), calls=%async_computation.1 | async-start | bytes 196608 | tf_op jit(solution)/shard_map/all_to_all | solution.py:17
  33.2 49.2 %all-gather.3.cloned.1.call-start = ((), (), s32[]{:S(2)}) async-start(), calls=%async_computation.3 | async-start | bytes 4718592 | tf_op jit(solution)/shard_map/all_gather | solution.py:96
  41.3 9.0 %copy-start.13 = (bf16[2048,256]{1,0:T(8,128)(2,1)S(1)}, bf16[2048,256]{1,0:T(8,128)(2,1)}, u32[]{:S(2)}) copy-start(bf16[2048,256]{1,0:T(8,128)(2,1)} %param.24) | copy-start | bytes 3145732
  41.4 123.7 %all-gather.5.cloned.1.call-start = ((), (), s32[]{:S(2)}) async-start(), calls=%async_computation.4 | async-start | bytes 8912896 | tf_op jit(solution)/shard_map/all_gather | solution.py:103
  42.1 204.2 %reduce-scatter.2.cloned.1.call-start = ((), (), s32[]{:S(2)}) async-start(), calls=%async_computation.5 | async-start | bytes 4718592 | tf_op jit(solution)/shard_map/reduce_scatter | solution.py:198
  42.7 9.2 %copy-start.15 = (f32[4,15,31]{2,0,1:T(4,128)S(1)}, f32[4,15,31]{2,0,1:T(4,128)}, u32[]{:S(2)}) copy-start(f32[4,15,31]{2,0,1:T(4,128)} %param.26) | copy-start | bytes 22324
  76.7 5.7 %copy-start.14 = (bf16[2048,256]{1,0:T(8,128)(2,1)S(1)}, bf16[2048,256]{1,0:T(8,128)(2,1)}, u32[]{:S(2)}) copy-start(bf16[2048,256]{1,0:T(8,128)(2,1)} %param.24) | copy-start | bytes 3145732
  88.7 4.7 %copy-start.11 = (bf16[2,512,768]{2,1,0:T(8,128)(2,1)}, bf16[2,512,768]{2,1,0:T(8,128)(2,1)S(1)}, u32[]{:S(2)}) copy-start(bf16[2,512,768]{2,1,0:T(8,128)(2,1)S(1)} %fusion.25) | copy-start | bytes 4718596
  89.8 17.3 %collective-permute-start = (bf16[2,4,64,512]{3,2,1,0:T(8,128)(2,1)}, bf16[2,4,64,512]{3,2,1,0:T(8,128)(2,1)}, u32[]{:S(2)}, u32[]{:S(2)}) collective-permute-start(bf16[2,4,64,512]{3,2,1,0:T(8,128)(2,1)} %get-tuple-element.24), channel_id=1, source_target_pairs={{0,8},{8,16},{16,24},{24,32},{32,40},{40,48},{48,56},{56,64},{64,7... | collective-permute-start | bytes 1572872 | tf_op jit(solution)/shard_map/ppermute | solution.py:45
  93.3 15.3 %collective-permute-start.1 = (bf16[2,4,64,512]{3,2,1,0:T(8,128)(2,1)S(1)}, bf16[2,4,64,512]{3,2,1,0:T(8,128)(2,1)}, u32[]{:S(2)}, u32[]{:S(2)}) collective-permute-start(bf16[2,4,64,512]{3,2,1,0:T(8,128)(2,1)S(1)} %get-tuple-element.25), channel_id=1, source_target_pairs={{8,0},{16,8},{24,16},{32,24},{40,32},{48,40},{56,48},{64,56},{72,6... | collective-permute-start | bytes 1572872 | tf_op jit(solution)/shard_map/ppermute | solution.py:46
  99.1 4.4 %slice-start = ((bf16[2,512,768]{2,1,0:T(8,128)(2,1)}), bf16[2,512,256]{2,1,0:T(8,128)(2,1)S(1)}, s32[]{:S(2)}) async-start(bf16[2,512,768]{2,1,0:T(8,128)(2,1)} %copy-done.11), calls=%async_computation.6 | async-start | bytes 1048576 | tf_op jit(solution)/shard_map/slice | solution.py:115
  153.2 6.8 %copy-start.6 = (f32[4,128,512]{2,1,0:T(8,128)S(1)}, f32[4,128,512]{2,1,0:T(8,128)}, u32[]{:S(2)}) copy-start(f32[4,128,512]{2,1,0:T(8,128)} %add.457) | copy-start | bytes 3145732
  153.2 6.8 %copy-start.9 = (bf16[2,512,1,4,64]{1,4,3,0,2:T(8,128)(2,1)S(1)}, bf16[2,512,1,4,64]{1,4,3,0,2:T(8,128)(2,1)}, u32[]{:S(2)}) copy-start(bf16[2,512,1,4,64]{1,4,3,0,2:T(8,128)(2,1)} %copy.204) | copy-start | bytes 1572868
  153.2 6.8 %copy-start.19 = (pred[128,512]{1,0:T(8,128)(4,1)S(1)}, pred[128,512]{1,0:T(8,128)(4,1)}, u32[]{:S(2)}) copy-start(pred[128,512]{1,0:T(8,128)(4,1)} %and.119) | copy-start | bytes 196612
  156.0 6.5 %copy-start.7 = (f32[4,128,512]{2,1,0:T(8,128)S(1)}, f32[4,128,512]{2,1,0:T(8,128)}, u32[]{:S(2)}) copy-start(f32[4,128,512]{2,1,0:T(8,128)} %add.440) | copy-start | bytes 3145732
  156.0 6.5 %copy-start.10 = (bf16[2,512,1,4,64]{1,4,3,0,2:T(8,128)(2,1)S(1)}, bf16[2,512,1,4,64]{1,4,3,0,2:T(8,128)(2,1)}, u32[]{:S(2)}) copy-start(bf16[2,512,1,4,64]{1,4,3,0,2:T(8,128)(2,1)} %copy.200) | copy-start | bytes 1572868
  156.0 6.5 %copy-start.18 = (pred[128,512]{1,0:T(8,128)(4,1)S(1)}, pred[128,512]{1,0:T(8,128)(4,1)}, u32[]{:S(2)}) copy-start(pred[128,512]{1,0:T(8,128)(4,1)} %and.115) | copy-start | bytes 196612
  173.5 0.9 copy-start.12
  174.4 0.8 copy-start.28
  175.2 0.9 copy-start.27
  175.2 1.6 copy-start.1
  176.1 4.7 %copy-start.20 = (f32[2,4,128]{2,1,0:T(4,128)}, f32[2,4,128]{2,1,0:T(4,128)S(1)}, u32[]{:S(2)}) copy-start(f32[2,4,128]{2,1,0:T(4,128)S(1)} %max.48) | copy-start | bytes 12292
  180.8 2.3 copy-start.29
  180.8 2.3 copy-start.24
  180.8 2.3 copy-start.25
  180.8 2.3 copy-start.26
  180.8 2.3 copy-start.2
  183.0 1.6 copy-start.3
  183.0 5.8 %copy-start.22 = (f32[2,4,128]{2,1,0:T(4,128)}, f32[2,4,128]{2,1,0:T(4,128)S(1)}, u32[]{:S(2)}) copy-start(f32[2,4,128]{2,1,0:T(4,128)S(1)} %max.51) | copy-start | bytes 12292
  183.1 8.0 %copy-start.23 = (f32[2,4,128]{2,1,0:T(4,128)}, f32[2,4,128]{2,1,0:T(4,128)S(1)}, u32[]{:S(2)}) copy-start(f32[2,4,128]{2,1,0:T(4,128)S(1)} %max.49) | copy-start | bytes 12292
  188.8 2.2 copy-start.31
  191.1 2.2 copy-start.32
  193.3 1.6 copy-start.16
  201.0 2.2 copy-start.21
  201.0 2.2 copy-start.30
  203.2 2.9 %copy-start.17 = (bf16[2,8,1,16,256]{4,3,1,0,2:T(8,128)(2,1)S(1)}, bf16[2,8,1,16,256]{4,3,1,0,2:T(8,128)(2,1)}, u32[]{:S(2)}) copy-start(bf16[2,8,1,16,256]{4,3,1,0,2:T(8,128)(2,1)} %stack_reshape.13) | copy-start | bytes 393220
  209.4 37.0 %copy-start.5 = (bf16[2,64,2048]{2,1,0:T(8,128)(2,1)S(1)}, bf16[2,64,2048]{2,1,0:T(8,128)(2,1)}, u32[]{:S(2)}) copy-start(bf16[2,64,2048]{2,1,0:T(8,128)(2,1)} %param.14) | copy-start | bytes 1572868
Sparse Core Ops, SparseCore 0:
  41.5 27.7 all-gather.2
  71.4 78.3 all-gather.4
  209.5 36.7 reduce-scatter.1
where the time goes:
time: 260 us; the launch traced here: 255 us
  local copies, waits for them, and re-layouts  92 us (35%)
  matrix products  64.9 us (25%)
  waiting for transfers between devices  50.9 us (20%)
  starting transfers between devices  17.3 us (7%)
  other arithmetic  15.9 us (6%)
  between operations  14.1 us (5%)
    reduce_scatter x1, waiting for transfers between devices, on_device(): lax.psum_scatter(jnp.einsum('tsc,cd->tsd', attended, w_out, preferred_ele...  37 us
    unnamed x76, local copies, waits for them, and re-layouts  23.9 us
    add x4, local copies, waits for them, and re-layouts, on_device(): jnp.einsum('snhd,skhd->shnk', block_query, block_pair[:, :, 0], preferred...  18.2 us
    reshape x4, local copies, waits for them, and re-layouts, on_device(): padded_pair[:, :, first:first + span]  14.4 us
    all_to_all x2, starting transfers between devices, copy_for_each(): lax.all_to_all(jnp.broadcast_to(shard[None], (length, *shard.shape)), axi...  12.5 us
    dot_general x4, matrix products, on_device(): jnp.einsum('snhd,skhd->shnk', block_query, block_pair[:, :, 0], preferred...  11.8 us
    all_to_all x2, waiting for transfers between devices, copy_for_each(): lax.all_to_all(jnp.broadcast_to(shard[None], (length, *shard.shape)), axi...  11.6 us
    dot_general x8, matrix products, on_device(): jnp.einsum('rpa,hac,qkc->hrqpk', row_onehot, rel_bias, col_onehot, precis...  10.6 us
  transfers between devices with their start and end apart: 7, of which 4 were waited for; matrix products, arithmetic and copies ran while one was open for 47% of the time, Pallas kernels for 0%

commit v1 on v0

v1 whole, which is shorter than its diff:
```python
import jax
import jax.numpy as jnp
from jax import lax
from jax.experimental import pallas as pl
from jax.experimental.pallas import tpu as pltpu
from jax.sharding import PartitionSpec as P

HEAD_DIM = 64
GRID_W = 64
WIN_ROWS = 8
WIN_COLS = 16
EPSILON = 1e-06
MASKED = -1e30
REACH = WIN_ROWS // 2
BIAS_BLOCKS = 7


def copy_for_each(shard, axis):
    length = lax.axis_size(axis)
    return lax.all_to_all(
        jnp.broadcast_to(shard[None], (length, *shard.shape)), axis, 0, 0, tiled=True
    )


def silu_rows(values):
    return jax.nn.silu(values.astype(jnp.float32)).astype(jnp.bfloat16)


def whole(shape):
    return pl.BlockSpec(shape, lambda *_: (0,) * len(shape))


def project(rows, gain, shift, scale, weights, parts, block):
    count, width = rows.shape
    cols = weights[0].shape[1]

    def body(rows_ref, gain_ref, shift_ref, scale_ref, *refs):
        weight_refs, out_refs = refs[: len(weights)], refs[len(weights) :]
        floats = rows_ref[...].astype(jnp.float32)
        inverse = lax.rsqrt(jnp.mean(floats * floats, axis=-1, keepdims=True) + EPSILON)
        factor = gain_ref[...] * (1.0 + scale_ref[...])
        hidden = (floats * inverse * factor + shift_ref[...]).astype(jnp.bfloat16)
        at = 0
        for out_ref, part in zip(out_refs, parts):
            for index, multiple in enumerate(part):
                product = jnp.dot(hidden, weight_refs[at][...], preferred_element_type=jnp.float32)
                if multiple != 1.0:
                    product = product.astype(jnp.bfloat16).astype(jnp.float32) * multiple
                out_ref[:, index * cols : (index + 1) * cols] = product.astype(jnp.bfloat16)
                at += 1

    return pl.pallas_call(
        body,
        grid=(count // block,),
        in_specs=[pl.BlockSpec((block, width), lambda i: (i, 0))]
        + [whole((1, width))] * 3
        + [whole(weight.shape) for weight in weights],
        out_specs=[pl.BlockSpec((block, cols * len(part)), lambda i: (i, 0)) for part in parts],
        out_shape=[
            jax.ShapeDtypeStruct((count, cols * len(part)), jnp.bfloat16) for part in parts
        ],
        name="project",
    )(rows, gain, shift, scale, *weights)


def bias_table(rel_bias):
    heads, offsets, spread = rel_bias.shape
    slots = 2 * BIAS_BLOCKS + 2
    padded = jnp.pad(rel_bias, ((0, 0), (0, slots - offsets), (0, 128 - spread)))
    padded = padded.reshape(heads * slots, 128)

    def body(rel_ref, out_ref):
        query = lax.broadcasted_iota(jnp.int32, (GRID_W, 128), 0)
        lane = lax.broadcasted_iota(jnp.int32, (GRID_W, 128), 1)
        low = lane < GRID_W
        key = jnp.where(low, lane, lane - GRID_W)
        start = jnp.clip(query - WIN_COLS // 2, 0, GRID_W - WIN_COLS)
        inside = (key >= start) & (key < start + WIN_COLS)

        def diagonal(head, slot, move):
            row = jnp.broadcast_to(rel_ref[pl.ds(head * slots + slot, 1), :], (GRID_W, 128))
            return pltpu.roll(row, (128 - (WIN_COLS - 1) + move) % 128, 1, stride=1, stride_axis=0)

        for parity in range(2):
            for head in range(heads):
                for block in range(BIAS_BLOCKS):
                    slot = 2 * block + parity
                    both = jnp.where(
                        low, diagonal(head, slot, 0), diagonal(head, slot + 1, GRID_W)
                    )
                    out_ref[
                        parity, head * GRID_W : (head + 1) * GRID_W, block * 128 : (block + 1) * 128
                    ] = jnp.where(inside, both, MASKED)

    return pl.pallas_call(
        body,
        out_shape=jax.ShapeDtypeStruct((2, heads * GRID_W, BIAS_BLOCKS * 128), jnp.float32),
        name="bias_table",
    )(padded)


def attend(place, query, before, pair, after, ctx_pair, table, ctx_bias, rows_all):
    tokens, cols = query.shape
    heads = cols // HEAD_DIM
    rows_dev = tokens // GRID_W
    near_keys = WIN_ROWS * GRID_W
    padded = before.shape[0] + pair.shape[0] + after.shape[0]
    ctx_count = ctx_pair.shape[0]
    queries = heads * GRID_W

    def body(place_ref, q_ref, before_ref, pair_ref, after_ref, ctx_ref, table_ref, cb_ref, out_ref, keys):
        row = pl.program_id(0)

        @pl.when(row == 0)
        def _():
            first = before_ref.shape[0]
            keys[0:first] = before_ref[...]
            keys[first : first + tokens] = pair_ref[...]
            keys[first + tokens : padded] = after_ref[...]

        base = place_ref[0] * rows_dev
        actual = base + row
        start = jnp.clip(actual - REACH, 0, rows_all - WIN_ROWS)
        local = start - base + REACH
        offset = start - actual + WIN_ROWS - 1
        q = q_ref[...]
        lane = lax.broadcasted_iota(jnp.int32, (GRID_W, cols), 1)
        masks = [(lane >= h * HEAD_DIM) & (lane < (h + 1) * HEAD_DIM) for h in range(heads)]
        spread = jnp.concatenate([jnp.where(mask, q, jnp.zeros_like(q)) for mask in masks], axis=0)
        at = pl.multiple_of(local * GRID_W, GRID_W)
        near_pair = keys[pl.ds(at, near_keys), :]
        nt = (((1,), (1,)), ((), ()))
        near = lax.dot_general(
            spread, near_pair[:, :cols], nt, preferred_element_type=jnp.float32
        )
        column = pl.multiple_of((offset // 2) * 128, 128)
        near = near + table_ref[offset % 2, :, pl.ds(column, near_keys)]
        far = lax.dot_general(
            spread, ctx_ref[:, :cols], nt, preferred_element_type=jnp.float32
        )
        cb = cb_ref[...]
        top = jnp.maximum(
            jnp.max(near, axis=-1, keepdims=True), jnp.max(far, axis=-1, keepdims=True) + cb
        )
        near_exp = jnp.exp(near - top)
        far_exp = jnp.exp(far - (top - cb))
        total = jnp.sum(near_exp, axis=-1, keepdims=True) + jnp.sum(far_exp, axis=-1, keepdims=True)
        mixed = jnp.dot(
            near_exp.astype(jnp.bfloat16), near_pair[:, cols:], preferred_element_type=jnp.float32
        ) + jnp.dot(
            far_exp.astype(jnp.bfloat16), ctx_ref[:, cols:], preferred_element_type=jnp.float32
        )
        mixed = mixed / total
        result = jnp.where(masks[0], mixed[:GRID_W], 0.0)
        for h in range(1, heads):
            result = jnp.where(masks[h], mixed[h * GRID_W : (h + 1) * GRID_W], result)
        out_ref[...] = result.astype(jnp.bfloat16)

    return pl.pallas_call(
        body,
        grid=(rows_dev,),
        in_specs=[
            pl.BlockSpec(memory_space=pltpu.SMEM),
            pl.BlockSpec((GRID_W, cols), lambda i: (i, 0)),
            whole(before.shape),
            whole(pair.shape),
            whole(after.shape),
            whole(ctx_pair.shape),
            whole(table.shape),
            whole((queries, 1)),
        ],
        out_specs=pl.BlockSpec((GRID_W, cols), lambda i: (i, 0)),
        out_shape=jax.ShapeDtypeStruct((tokens, cols), jnp.bfloat16),
        scratch_shapes=[pltpu.VMEM((padded, 2 * cols), jnp.bfloat16)],
        name="attend",
    )(place, query, before, pair, after, ctx_pair, table, ctx_bias)


def on_device(
    latent,
    context,
    cond,
    ctx_cond,
    w_shift,
    w_scale,
    w_gate,
    norm_gain,
    w_query,
    w_key,
    w_value,
    w_out,
    rel_bias,
    ctx_bias,
):
    samples, tokens_dev, width = latent.shape
    rows_sp, local_cols = w_shift.shape
    heads = local_cols // HEAD_DIM
    sp_index = lax.axis_index("sp")
    sp_size = lax.axis_size("sp")
    gathered = [lax.all_gather(latent[s], "tp", axis=0, tiled=True) for s in range(samples)]
    ada = silu_rows(jnp.concatenate([cond, ctx_cond[None, :]], axis=0))
    ada_rows = lax.dynamic_slice_in_dim(ada, sp_index * rows_sp, rows_sp, 1)
    partial_value = jnp.stack(
        [
            jnp.dot(ada_rows, weight, preferred_element_type=jnp.float32)
            for weight in (w_shift, w_scale, w_gate)
        ]
    )
    summed = jnp.sum(copy_for_each(partial_value, "sp"), axis=0)
    tiles = copy_for_each(summed, "tp")
    modulation = jnp.moveaxis(tiles, 0, 2).reshape(3, samples + 1, width)
    gain = norm_gain[None, :]
    table = bias_table(rel_bias)
    place = jnp.full((1,), sp_index, jnp.int32)
    ctx_rows = context.shape[1]
    (ctx_pair,) = project(
        context.reshape(samples * ctx_rows, width),
        gain,
        modulation[0, samples][None],
        modulation[1, samples][None],
        (w_key, w_value),
        ((1.0, 1.0),),
        samples * ctx_rows,
    )
    ctx_pair = lax.all_gather(
        ctx_pair.reshape(samples, ctx_rows, 2 * local_cols), "sp", axis=1, tiled=True
    )
    cb = jnp.repeat(ctx_bias, GRID_W)[:, None]
    up = [(i, i + 1) for i in range(sp_size - 1)]
    down = [(j, i) for i, j in up]
    outs = []
    for s in range(samples):
        query, pair = project(
            gathered[s],
            gain,
            modulation[0, s][None],
            modulation[1, s][None],
            (w_query, w_key, w_value),
            ((HEAD_DIM**-0.5,), (1.0, 1.0)),
            128,
        )
        tokens = pair.shape[0]
        before = lax.ppermute(pair[tokens - REACH * GRID_W :], "sp", up)
        after = lax.ppermute(pair[: (WIN_ROWS - REACH - 1) * GRID_W], "sp", down)
        attended = attend(
            place,
            query,
            before,
            pair,
            after,
            ctx_pair[s],
            table,
            cb,
            tokens // GRID_W * sp_size,
        )
        part = jnp.dot(attended, w_out, preferred_element_type=jnp.float32).astype(jnp.bfloat16)
        update = lax.psum_scatter(part, "tp", scatter_dimension=0, tiled=True)
        outs.append(
            (
                latent[s].astype(jnp.float32)
                + modulation[2, s][None] * update.astype(jnp.float32)
            ).astype(jnp.bfloat16)
        )
    return jnp.stack(outs)


def solution(mesh):
    return jax.shard_map(
        on_device,
        mesh=mesh,
        in_specs=(
            P(None, ("sp", "tp"), None),
            P(None, "sp", None),
            P(),
            P(),
            P("sp", "tp"),
            P("sp", "tp"),
            P("sp", "tp"),
            P(),
            P(None, "tp"),
            P(None, "tp"),
            P(None, "tp"),
            P("tp", None),
            P("tp", None, None),
            P("tp"),
        ),
        out_specs=P(None, ("sp", "tp"), None),
        check_vma=False,
    )
```

time: 260 us -> 196 us (0.75)
  the two profiles are of different devices: /device:TPU:0 before, /device:TPU:32 now
where the time goes in v1:
time: 196 us; the launch traced here: 194 us
  waiting for transfers between devices  70 us (36%)
  Pallas kernels  45.6 us (23%)
  blocking collectives  24.1 us (12%)
  starting transfers between devices  16.1 us (8%)
  local copies, waits for them, and re-layouts  14.2 us (7%)
  between operations  13.3 us (7%)
  matrix products  8.98 us (5%)
  other arithmetic  1.97 us (1%)
    reduce_scatter x2, waiting for transfers between devices, on_device(): update = lax.psum_scatter(part, 'tp', scatter_dimension=0, tiled=True)  35.8 us
    pallas_call x2, Pallas kernels, attend(): pl.pallas_call(body, grid=(rows_dev,), in_specs=[pl.BlockSpec(memory_spac...  27.5 us
    all_to_all x2, blocking collectives, copy_for_each(): lax.all_to_all(jnp.broadcast_to(shard[None], (length, *shard.shape)), axi...  24.1 us
    all_gather x1, waiting for transfers between devices, on_device(): lax.all_gather(ctx_pair.reshape(samples, ctx_rows, 2 * local_cols), 'sp',...  23.2 us
    pallas_call x3, Pallas kernels, project(): pl.pallas_call(body, grid=(count // block,), in_specs=[pl.BlockSpec((bloc...  15.1 us
    ppermute x2, starting transfers between devices, on_device(): after = lax.ppermute(pair[:(WIN_ROWS - REACH - 1) * GRID_W], 'sp', down)  10.1 us
    dot_general x2, matrix products, on_device(): jnp.dot(attended, w_out, preferred_element_type=jnp.float32)  6.06 us
    all_gather x2, waiting for transfers between devices, on_device(): lax.all_gather(latent[s], 'tp', axis=0, tiled=True)  6.03 us
  transfers between devices with their start and end apart: 9, of which 4 were waited for; matrix products, arithmetic and copies ran while one was open for 10% of the time, Pallas kernels for 23%

profile of v1, /device:TPU:32, one launch (start us, length us, event | category | flops | bytes accessed | tf_op | source)
XLA Modules:
  0.0 194.2 jit_solution(715594332215936973)
XLA Ops:
  6.5 2.0 %fusion.8 = (bf16[1,64,2048]{2,1,0:T(8,128)(2,1)}, bf16[1,64,2048]{2,1,0:T(8,128)(2,1)}) fusion(bf16[2,64,2048]{2,1,0:T(8,128)(2,1)} %param.14), kind=kLoop, calls=%fused_computation.24 | loop fusion | bytes 1048576 | tf_op jit(solution)/shard_map/slice | solution.py:260
  8.5 0.0 all-gather.10.cloned.1.call-update
  8.5 0.0 all-gather.6.cloned.1.call-start
  8.6 0.7 broadcast_in_dim.24
  9.3 0.7 maximum_convert_fusion
  10.0 1.0 convolution_bitcast_fusion
  11.0 1.0 convolution_bitcast_fusion.1
  11.9 1.0 convolution_bitcast_fusion.2
  12.9 14.1 %all_to_all.10 = f32[16,3,3,256]{3,2,1,0:T(4,128)S(1)} all-to-all(f32[16,3,3,256]{3,2,1,0:T(4,128)S(1)} %broadcast_in_dim.25), channel_id=1, replica_groups=mesh['sp'=16,'tp'=8] {'sp'}, dimensions={0} | all-to-all | bytes 294912 | tf_op jit(solution)/shard_map/all_to_all | solution.py:20
  27.1 10.1 %all_to_all.11 = f32[8,3,3,256]{3,2,1,0:T(4,128)S(1)} all-to-all(f32[8,3,3,256]{3,2,1,0:T(4,128)S(1)} %broadcast_in_dim.26), channel_id=1, replica_groups=mesh['sp'=16,'tp'=8] {'tp'}, dimensions={0} | all-to-all | bytes 147456 | tf_op jit(solution)/shard_map/all_to_all | solution.py:20
  37.2 0.7 fusion.9
  37.9 3.0 %project.4 = bf16[128,512]{1,0:T(8,128)(2,1)} custom-call(bf16[128,2048]{1,0:T(8,128)(2,1)} %bitcast.53, f32[1,2048]{1,0:T(1,128)} %bitcast.57, f32[1,2048]{1,0:T(1,128)} %get-tuple-element.24.shift_ref, f32[1,2048]{1,0:T(1,128)} %get-tuple-element.23.scale_ref, bf16[2048,256]{1,0:T(8,128)(2,1)} %refs_1_.5, bf16[2048,256]{1,0:T(8,128)(2,1)} %refs_2_.3), custom_call_target="tpu_custom_call" | custom-call | tf_op jit(solution)/shard_map/project/pallas_call | solution.py:52
  40.9 0.0 all-gather.6.cloned.1.call-update
  40.9 0.0 all-gather.8.cloned.1.call-start
  41.0 0.7 all-gather.8.cloned.1.call-update
  41.6 0.0 reduce-scatter.5.cloned.1.call-start
  41.7 0.6 pad.4.clone
  42.3 3.0 %bias_table.1.table_ref = f32[2,256,896]{2,1,0:T(8,128)} custom-call(f32[64,128]{1,0:T(8,128)} %bitcast.56), custom_call_target="tpu_custom_call" | custom-call | tf_op jit(solution)/shard_map/bias_table/pallas_call | solution.py:95
  45.4 0.1 broadcast_in_dim.29
  45.4 0.8 broadcast_in_dim_reshape.4.cb_ref
  46.2 6.1 %project.5 = (bf16[512,256]{1,0:T(8,128)(2,1)}, bf16[512,512]{1,0:T(8,128)(2,1)}) custom-call(bf16[512,2048]{1,0:T(8,128)(2,1)} %bitcast.51, f32[1,2048]{1,0:T(1,128)} %bitcast.58, f32[1,2048]{1,0:T(1,128)} %get-tuple-element.21.shift_ref, f32[1,2048]{1,0:T(1,128)} %get-tuple-element.20.scale_ref, bf16[2048,256]{1,0:T(8,128)(2,1)} %refs_0_.5, ...), custom_call_target="tpu_custom_call" | custom-call | tf_op jit(solution)/shard_map/project/pallas_call | solution.py:52
  52.3 1.0 slice.63
  53.3 0.9 slice.64
  54.2 2.5 %collective-permute-start.2 = (bf16[256,512]{1,0:T(8,128)(2,1)S(1)}, bf16[256,512]{1,0:T(8,128)(2,1)S(1)}, u32[]{:S(2)}, u32[]{:S(2)}) collective-permute-start(bf16[256,512]{1,0:T(8,128)(2,1)S(1)} %slice.63), channel_id=1, source_target_pairs={{0,8},{8,16},{16,24},{24,32},{32,40},{40,48},{48,56},{56,64},{64,7... | collective-permute-start | bytes 786440 | tf_op jit(solution)/shard_map/ppermute | solution.py:243
  56.7 5.5 %collective-permute-start.3 = (bf16[192,512]{1,0:T(8,128)(2,1)S(1)}, bf16[192,512]{1,0:T(8,128)(2,1)S(1)}, u32[]{:S(2)}, u32[]{:S(2)}) collective-permute-start(bf16[192,512]{1,0:T(8,128)(2,1)S(1)} %slice.64), channel_id=1, source_target_pairs={{8,0},{16,8},{24,16},{32,24},{40,32},{48,40},{56,48},{64,56},{72,6... | collective-permute-start | bytes 589832 | tf_op jit(solution)/shard_map/ppermute | solution.py:244
  62.2 23.2 %all-gather.6.cloned.1.call-done = bf16[2,1024,512]{2,1,0:T(8,128)(2,1)} async-done(((bf16[2,64,512]{2,1,0:T(8,128)(2,1)}), bf16[2,1024,512]{2,1,0:T(8,128)(2,1)}) %all-gather.6.cloned.1.call-update) | async-done | bytes 2097168 | tf_op jit(solution)/shard_map/all_gather | solution.py:225
  85.4 3.1 %slice_bitcast_fusion.1 = (bf16[1024,512]{1,0:T(8,128)(2,1)}, bf16[1024,512]{1,0:T(8,128)(2,1)}) fusion(bf16[2,1024,512]{2,1,0:T(8,128)(2,1)} %all-gather.6.cloned.1.call-done), kind=kLoop, calls=%fused_computation.6 | loop fusion | bytes 4194304 | tf_op jit(solution)/shard_map/squeeze | solution.py:251
  88.4 0.7 copy-done.4
  89.1 0.1 copy-done.2
  89.2 13.7 %attend.3 = bf16[512,256]{1,0:T(8,128)(2,1)} custom-call(s32[1]{0:T(128)} %bitcast.6.place_ref, bf16[512,256]{1,0:T(8,128)(2,1)} %get-tuple-element.11.q_ref, bf16[256,512]{1,0:T(8,128)(2,1)} %copy-done.2, bf16[512,512]{1,0:T(8,128)(2,1)} %get-tuple-element.12.pair_ref, bf16[192,512]{1,0:T(8,128)(2,1)} %copy-done.4, ...), custom_call_target="tpu_custom_call" | custom-call | tf_op jit(solution)/shard_map/attend/pallas_call | solution.py:159
  103.0 3.0 %convolution_convert_fusion = bf16[512,2048]{1,0:T(8,128)(2,1)} fusion(bf16[512,256]{1,0:T(8,128)(2,1)} %attend.3, bf16[256,2048]{1,0:T(8,128)(2,1)S(1)} %copy-done), kind=kOutput, calls=%fused_computation | convolution fusion | flops 537919488 | bytes 3407872 | tf_op jit(solution)/shard_map/dot_general | solution.py:256
  106.0 0.0 reduce-scatter.5.cloned.1.call-update
  106.0 0.0 reduce-scatter.3.cloned.1.call-start
  106.0 6.0 %all-gather.8.cloned.1.call-done = bf16[1,512,2048]{2,1,0:T(8,128)(2,1)} async-done(((bf16[1,64,2048]{2,1,0:T(8,128)(2,1)}), bf16[1,512,2048]{2,1,0:T(8,128)(2,1)}) %all-gather.8.cloned.1.call-update) | async-done | bytes 2097168 | tf_op jit(solution)/shard_map/all_gather | solution.py:200
  112.1 6.1 %project.3 = (bf16[512,256]{1,0:T(8,128)(2,1)}, bf16[512,512]{1,0:T(8,128)(2,1)}) custom-call(bf16[512,2048]{1,0:T(8,128)(2,1)} %bitcast.52, f32[1,2048]{1,0:T(1,128)} %bitcast.59, f32[1,2048]{1,0:T(1,128)} %get-tuple-element.26.shift_ref, f32[1,2048]{1,0:T(1,128)} %get-tuple-element.25.scale_ref, bf16[2048,256]{1,0:T(8,128)(2,1)} %refs_0_.5, ...), custom_call_target="tpu_custom_call" | custom-call | tf_op jit(solution)/shard_map/project/pallas_call | solution.py:52
  118.1 1.0 slice.54
  119.1 3.4 %collective-permute-start = (bf16[256,512]{1,0:T(8,128)(2,1)S(1)}, bf16[256,512]{1,0:T(8,128)(2,1)S(1)}, u32[]{:S(2)}, u32[]{:S(2)}) collective-permute-start(bf16[256,512]{1,0:T(8,128)(2,1)S(1)} %slice.54), channel_id=1, source_target_pairs={{0,8},{8,16},{16,24},{24,32},{32,40},{40,48},{48,56},{56,64},{64,7... | collective-permute-start | bytes 786440 | tf_op jit(solution)/shard_map/ppermute | solution.py:243
  122.5 1.0 slice.55
  123.4 4.6 %collective-permute-start.1 = (bf16[192,512]{1,0:T(8,128)(2,1)S(1)}, bf16[192,512]{1,0:T(8,128)(2,1)S(1)}, u32[]{:S(2)}, u32[]{:S(2)}) collective-permute-start(bf16[192,512]{1,0:T(8,128)(2,1)S(1)} %slice.55), channel_id=1, source_target_pairs={{8,0},{16,8},{24,16},{32,24},{40,32},{48,40},{56,48},{64,56},{72,6... | collective-permute-start | bytes 589832 | tf_op jit(solution)/shard_map/ppermute | solution.py:244
  128.0 4.2 %collective-permute-done.1.after_ref = bf16[192,512]{1,0:T(8,128)(2,1)S(1)} collective-permute-done((bf16[192,512]{1,0:T(8,128)(2,1)S(1)}, bf16[192,512]{1,0:T(8,128)(2,1)S(1)}, u32[]{:S(2)}, u32[]{:S(2)}) %collective-permute-start.1) | collective-permute-done | bytes 196640 | tf_op jit(solution)/shard_map/ppermute | solution.py:244
  132.3 0.7 copy-done.5
  132.9 0.1 copy-done.3
  133.1 13.7 %attend.2 = bf16[512,256]{1,0:T(8,128)(2,1)} custom-call(s32[1]{0:T(128)} %bitcast.6.place_ref, bf16[512,256]{1,0:T(8,128)(2,1)} %get-tuple-element.9.q_ref, bf16[256,512]{1,0:T(8,128)(2,1)} %copy-done.3, bf16[512,512]{1,0:T(8,128)(2,1)} %get-tuple-element.10.pair_ref, bf16[192,512]{1,0:T(8,128)(2,1)} %copy-done.5, ...), custom_call_target="tpu_custom_call" | custom-call | tf_op jit(solution)/shard_map/attend/pallas_call | solution.py:159
  146.8 3.1 %convolution_convert_fusion.1 = bf16[512,2048]{1,0:T(8,128)(2,1)} fusion(bf16[512,256]{1,0:T(8,128)(2,1)} %attend.2, bf16[256,2048]{1,0:T(8,128)(2,1)S(1)} %copy-done), kind=kOutput, calls=%fused_computation.1 | convolution fusion | flops 537919488 | bytes 3407872 | tf_op jit(solution)/shard_map/dot_general | solution.py:256
  149.9 0.0 reduce-scatter.5.cloned.1.call-done
  149.9 35.8 %reduce-scatter.3.cloned.1.call-done = bf16[64,2048]{1,0:T(8,128)(2,1)} async-done(((bf16[512,2048]{1,0:T(8,128)(2,1)}), bf16[64,2048]{1,0:T(8,128)(2,1)}) %reduce-scatter.3.cloned.1.call-update) | async-done | bytes 262160 | tf_op jit(solution)/shard_map/reduce_scatter | solution.py:257
  185.7 1.2 fusion.2
  186.9 0.8 copy-done.8
  (27 shorter events, 0.2 us)
Async XLA Ops:
  6.5 96.4 %copy-start = (bf16[256,2048]{1,0:T(8,128)(2,1)S(1)}, bf16[256,2048]{1,0:T(8,128)(2,1)}, u32[]{:S(2)}) copy-start(bf16[256,2048]{1,0:T(8,128)(2,1)} %param.25) | copy-start | bytes 3145732
  6.5 39.7 %all-gather.10.cloned.1.call-start = ((), (), s32[]{:S(2)}) async-start(), calls=%async_computation.8 | async-start | bytes 2359296 | tf_op jit(solution)/shard_map/all_gather | solution.py:200
  8.5 76.8 %all-gather.6.cloned.1.call-start = ((), (), s32[]{:S(2)}) async-start(), calls=%async_computation.4 | async-start | bytes 2228224 | tf_op jit(solution)/shard_map/all_gather | solution.py:225
  27.0 14.7 %copy-start.6 = (f32[4,15,31]{2,0,1:T(4,128)S(1)}, f32[4,15,31]{2,0,1:T(4,128)}, u32[]{:S(2)}) copy-start(f32[4,15,31]{2,0,1:T(4,128)} %param.26) | copy-start | bytes 22324
  37.9 7.5 %copy-start.7 = (f32[4]{0:T(128)S(1)}, f32[4]{0:T(128)}, u32[]{:S(2)}) copy-start(f32[4]{0:T(128)} %param.27) | copy-start | bytes 52
  40.9 71.2 %all-gather.8.cloned.1.call-start = ((), (), s32[]{:S(2)}) async-start(), calls=%async_computation.7 | async-start | bytes 2359296 | tf_op jit(solution)/shard_map/all_gather | solution.py:200
  41.6 108.3 %reduce-scatter.5.cloned.1.call-start = ((), (), s32[]{:S(2)}) async-start(), calls=%async_computation.6 | async-start | bytes 2359296 | tf_op jit(solution)/shard_map/reduce_scatter | solution.py:257
  54.2 34.2 %collective-permute-start.2 = (bf16[256,512]{1,0:T(8,128)(2,1)S(1)}, bf16[256,512]{1,0:T(8,128)(2,1)S(1)}, u32[]{:S(2)}, u32[]{:S(2)}) collective-permute-start(bf16[256,512]{1,0:T(8,128)(2,1)S(1)} %slice.63), channel_id=1, source_target_pairs={{0,8},{8,16},{16,24},{24,32},{32,40},{40,48},{48,56},{56,64},{64,7... | collective-permute-start | bytes 786440 | tf_op jit(solution)/shard_map/ppermute | solution.py:243
  56.7 31.7 %collective-permute-start.3 = (bf16[192,512]{1,0:T(8,128)(2,1)S(1)}, bf16[192,512]{1,0:T(8,128)(2,1)S(1)}, u32[]{:S(2)}, u32[]{:S(2)}) collective-permute-start(bf16[192,512]{1,0:T(8,128)(2,1)S(1)} %slice.64), channel_id=1, source_target_pairs={{8,0},{16,8},{24,16},{32,24},{40,32},{48,40},{56,48},{64,56},{72,6... | collective-permute-start | bytes 589832 | tf_op jit(solution)/shard_map/ppermute | solution.py:244
  88.4 0.7 copy-start.4
  88.4 0.8 copy-start.2
  106.0 79.7 %reduce-scatter.3.cloned.1.call-start = ((), (), s32[]{:S(2)}) async-start(), calls=%async_computation.5 | async-start | bytes 2359296 | tf_op jit(solution)/shard_map/reduce_scatter | solution.py:257
  119.1 13.2 %collective-permute-start = (bf16[256,512]{1,0:T(8,128)(2,1)S(1)}, bf16[256,512]{1,0:T(8,128)(2,1)S(1)}, u32[]{:S(2)}, u32[]{:S(2)}) collective-permute-start(bf16[256,512]{1,0:T(8,128)(2,1)S(1)} %slice.54), channel_id=1, source_target_pairs={{0,8},{8,16},{16,24},{24,32},{32,40},{40,48},{48,56},{56,64},{64,7... | collective-permute-start | bytes 786440 | tf_op jit(solution)/shard_map/ppermute | solution.py:243
  123.4 8.8 %collective-permute-start.1 = (bf16[192,512]{1,0:T(8,128)(2,1)S(1)}, bf16[192,512]{1,0:T(8,128)(2,1)S(1)}, u32[]{:S(2)}, u32[]{:S(2)}) collective-permute-start(bf16[192,512]{1,0:T(8,128)(2,1)S(1)} %slice.55), channel_id=1, source_target_pairs={{8,0},{16,8},{24,16},{32,24},{40,32},{48,40},{56,48},{64,56},{72,6... | collective-permute-start | bytes 589832 | tf_op jit(solution)/shard_map/ppermute | solution.py:244
  132.3 0.7 copy-start.5
  132.3 0.8 copy-start.3
  146.8 38.9 %copy-start.1 = (bf16[2,64,2048]{2,1,0:T(8,128)(2,1)S(1)}, bf16[2,64,2048]{2,1,0:T(8,128)(2,1)}, u32[]{:S(2)}) copy-start(bf16[2,64,2048]{2,1,0:T(8,128)(2,1)} %param.14) | copy-start | bytes 1572868
  186.9 0.8 copy-start.8
Sparse Core Ops, SparseCore 0:
  9.0 27.3 all-gather.9
  41.0 44.2 all-gather.5
  87.1 24.9 all-gather.7
  114.3 34.4 reduce-scatter.4
  151.1 34.6 reduce-scatter.2

commit v2 on v1

v2 whole, which is shorter than its diff:
```python
import jax
import jax.numpy as jnp
from jax import lax
from jax.experimental import pallas as pl
from jax.experimental.pallas import tpu as pltpu
from jax.sharding import PartitionSpec as P

HEAD_DIM = 64
GRID_W = 64
WIN_ROWS = 8
WIN_COLS = 16
EPSILON = 1e-06
MASKED = -1e30
REACH = WIN_ROWS // 2
BIAS_BLOCKS = 7


def copy_for_each(shard, axis):
    length = lax.axis_size(axis)
    return lax.all_to_all(
        jnp.broadcast_to(shard[None], (length, *shard.shape)), axis, 0, 0, tiled=True
    )


def silu_rows(values):
    return jax.nn.silu(values.astype(jnp.float32)).astype(jnp.bfloat16)


def modulation_parts(place, cond, ctx_cond, weights, copies):
    samples = cond.shape[0]
    rows, cols = weights[0].shape

    def body(place_ref, cond_ref, ctx_ref, shift_ref, scale_ref, gate_ref, out_ref):
        at = pl.multiple_of(place_ref[0] * rows, rows)
        ada = silu_rows(cond_ref[:, pl.ds(at, rows)])
        ada_ctx = silu_rows(ctx_ref[:, pl.ds(at, rows)])
        both = jnp.concatenate([ada.astype(jnp.float32), ada_ctx.astype(jnp.float32)], axis=0)
        both = both.astype(jnp.bfloat16)
        result = jnp.concatenate(
            [
                jnp.dot(both, shift_ref[...], preferred_element_type=jnp.float32),
                jnp.dot(both, scale_ref[...], preferred_element_type=jnp.float32),
                jnp.dot(ada, gate_ref[...], preferred_element_type=jnp.float32),
            ],
            axis=0,
        )
        for copy in range(copies):
            out_ref[copy] = result

    return pl.pallas_call(
        body,
        in_specs=[pl.BlockSpec(memory_space=pltpu.SMEM)]
        + [pl.BlockSpec(memory_space=pltpu.VMEM)] * 5,
        out_shape=jax.ShapeDtypeStruct((copies, 3 * samples + 2, cols), jnp.float32),
        name="modulation_parts",
    )(place, cond, ctx_cond, *weights)


def whole(shape):
    return pl.BlockSpec(shape, lambda *_: (0,) * len(shape))


def project(rows, sample, gain, shift, scale, weights, block, ends):
    _, count, width = rows.shape
    cols = weights[0].shape[1]
    first, last = ends if ends else (0, 0)
    steps = count // block

    def body(rows_ref, gain_ref, shift_ref, scale_ref, *refs):
        weight_refs, out_refs = refs[: len(weights)], refs[len(weights) :]
        step = pl.program_id(0)
        floats = rows_ref[0].astype(jnp.float32)
        inverse = lax.rsqrt(jnp.mean(floats * floats, axis=-1, keepdims=True) + EPSILON)
        factor = gain_ref[...] * (1.0 + scale_ref[...])
        hidden = (floats * inverse * factor + shift_ref[...]).astype(jnp.bfloat16)
        pair = [
            jnp.dot(hidden, ref[...], preferred_element_type=jnp.float32).astype(jnp.bfloat16)
            for ref in weight_refs[:2]
        ]
        out_refs[0][:, :cols] = pair[0]
        out_refs[0][:, cols:] = pair[1]
        if ends:
            query = jnp.dot(hidden, weight_refs[2][...], preferred_element_type=jnp.float32)
            query = query.astype(jnp.bfloat16).astype(jnp.float32) * HEAD_DIM**-0.5
            out_refs[1][...] = query.astype(jnp.bfloat16)
            for number in range(steps):
                low = number * block
                for out_ref, start, stop in (
                    (out_refs[2], 0, first),
                    (out_refs[3], count - last, count),
                ):
                    lo, hi = max(low, start), min(low + block, stop)
                    if lo < hi:

                        @pl.when(step == number)
                        def _(out_ref=out_ref, start=start, lo=lo, hi=hi, low=low):
                            for index in range(2):
                                out_ref[
                                    lo - start : hi - start, index * cols : (index + 1) * cols
                                ] = pair[index][lo - low : hi - low]

    out_specs = [pl.BlockSpec((block, 2 * cols), lambda i: (i, 0))]
    out_shape = [jax.ShapeDtypeStruct((count, 2 * cols), jnp.bfloat16)]
    if ends:
        out_specs += [pl.BlockSpec((block, cols), lambda i: (i, 0))]
        out_shape += [jax.ShapeDtypeStruct((count, cols), jnp.bfloat16)]
        for length in ends:
            out_specs += [whole((length, 2 * cols))]
            out_shape += [jax.ShapeDtypeStruct((length, 2 * cols), jnp.bfloat16)]
    return pl.pallas_call(
        body,
        grid=(steps,),
        in_specs=[pl.BlockSpec((1, block, width), lambda i: (sample, i, 0))]
        + [whole((1, width))] * 3
        + [whole(weight.shape) for weight in weights],
        out_specs=out_specs,
        out_shape=out_shape,
        name="project",
    )(rows, gain, shift, scale, *weights)


def bias_table(rel_bias):
    heads, offsets, spread = rel_bias.shape
    slots = 2 * BIAS_BLOCKS + 2
    padded = jnp.pad(rel_bias, ((0, 0), (0, slots - offsets), (0, 128 - spread)))
    padded = padded.reshape(heads * slots, 128)

    def body(rel_ref, out_ref):
        query = lax.broadcasted_iota(jnp.int32, (GRID_W, 128), 0)
        lane = lax.broadcasted_iota(jnp.int32, (GRID_W, 128), 1)
        low = lane < GRID_W
        key = jnp.where(low, lane, lane - GRID_W)
        start = jnp.clip(query - WIN_COLS // 2, 0, GRID_W - WIN_COLS)
        inside = (key >= start) & (key < start + WIN_COLS)

        def diagonal(head, slot, move):
            row = jnp.broadcast_to(rel_ref[pl.ds(head * slots + slot, 1), :], (GRID_W, 128))
            return pltpu.roll(row, (128 - (WIN_COLS - 1) + move) % 128, 1, stride=1, stride_axis=0)

        for parity in range(2):
            for head in range(heads):
                for block in range(BIAS_BLOCKS):
                    slot = 2 * block + parity
                    both = jnp.where(
                        low, diagonal(head, slot, 0), diagonal(head, slot + 1, GRID_W)
                    )
                    out_ref[
                        parity, head * GRID_W : (head + 1) * GRID_W, block * 128 : (block + 1) * 128
                    ] = jnp.where(inside, both, MASKED)

    return pl.pallas_call(
        body,
        out_shape=jax.ShapeDtypeStruct((2, heads * GRID_W, BIAS_BLOCKS * 128), jnp.float32),
        name="bias_table",
    )(padded)


def attend(place, sample, query, before, pair, after, ctx_keys, ctx_values, table, ctx_bias, rows_all, per):
    tokens, cols = query.shape
    heads = cols // HEAD_DIM
    rows_dev = tokens // GRID_W
    near_keys = WIN_ROWS * GRID_W
    ahead, behind = before.shape[0], after.shape[0]
    padded = ahead + tokens + behind
    lanes = -(-padded // 128) * 128
    groups, members, _, ctx_rows, _ = (len(ctx_keys), *ctx_keys[0].shape)
    ctx_count = groups * members * ctx_rows
    queries = heads * GRID_W
    bf16, f32 = jnp.bfloat16, jnp.float32

    def body(place_ref, q_ref, before_ref, pair_ref, after_ref, *refs):
        key_refs, value_refs = refs[:groups], refs[groups : groups + members]
        table_ref, cb_ref, out_ref, near_t, far_t, values, far_values = refs[groups + members :]
        step = pl.program_id(0)

        @pl.when(step == 0)
        def _():
            values[0:ahead] = before_ref[:, cols:]
            values[ahead : ahead + tokens] = pair_ref[:, cols:]
            values[ahead + tokens : padded] = after_ref[:, cols:]
            for group in range(groups):
                block = jnp.concatenate([key_refs[group][m, 0] for m in range(members)], axis=0)
                size = members * ctx_rows
                far_t[:, group * size : (group + 1) * size] = block.T
                for member in range(members):
                    at = (group * members + member) * ctx_rows
                    far_values[at : at + ctx_rows] = value_refs[member][group, 0]
            fill = jnp.zeros((lanes - padded, cols), bf16)
            near_t[0, :, :ahead] = before_ref[:, :cols].T
            near_t[0, :, ahead : ahead + tokens] = pair_ref[:, :cols].T
            near_t[0, :, ahead + tokens :] = jnp.concatenate(
                [after_ref[:, :cols], fill], axis=0
            ).T
            near_t[1] = jnp.concatenate(
                [
                    before_ref[GRID_W:, :cols],
                    pair_ref[:, :cols],
                    after_ref[:, :cols],
                    fill,
                    jnp.zeros((GRID_W, cols), bf16),
                ],
                axis=0,
            ).T

        base = place_ref[0] * rows_dev
        lane = lax.broadcasted_iota(jnp.int32, (GRID_W, cols), 1)
        masks = [(lane >= h * HEAD_DIM) & (lane < (h + 1) * HEAD_DIM) for h in range(heads)]
        cb = cb_ref[...]
        spreads, nears, starts = [], [], []
        for r in range(per):
            actual = base + step * per + r
            start = jnp.clip(actual - REACH, 0, rows_all - WIN_ROWS)
            local = start - base + REACH
            offset = start - actual + WIN_ROWS - 1
            q = q_ref[r * GRID_W : (r + 1) * GRID_W]
            spread = jnp.concatenate(
                [jnp.where(mask, q, jnp.zeros_like(q)) for mask in masks], axis=0
            )
            spreads.append(spread)
            column = pl.multiple_of((local // 2) * 128, 128)
            keys_t = near_t[local % 2, :, pl.ds(column, near_keys)]
            bias_at = pl.multiple_of((offset // 2) * 128, 128)
            nears.append(
                jnp.dot(spread, keys_t, preferred_element_type=f32)
                + table_ref[offset % 2, :, pl.ds(bias_at, near_keys)]
            )
            starts.append(pl.multiple_of(local * GRID_W, GRID_W))
        for r in range(per):
            near = nears[r]
            far = jnp.dot(spreads[r], far_t[...], preferred_element_type=f32)
            top = jnp.maximum(
                jnp.max(near, axis=-1, keepdims=True), jnp.max(far, axis=-1, keepdims=True) + cb
            )
            near_exp = jnp.exp(near - top)
            far_exp = jnp.exp(far - (top - cb))
            total = jnp.sum(near_exp, axis=-1, keepdims=True) + jnp.sum(
                far_exp, axis=-1, keepdims=True
            )
            mixed = jnp.dot(
                near_exp.astype(bf16),
                values[pl.ds(starts[r], near_keys), :],
                preferred_element_type=f32,
            ) + jnp.dot(far_exp.astype(bf16), far_values[...], preferred_element_type=f32)
            mixed = mixed * (1.0 / total)
            result = jnp.where(masks[0], mixed[:GRID_W], 0.0)
            for h in range(1, heads):
                result = jnp.where(masks[h], mixed[h * GRID_W : (h + 1) * GRID_W], result)
            out_ref[r] = result.astype(bf16)

    far_spec = pl.BlockSpec((members, 1, ctx_rows, cols), lambda i: (0, sample, 0, 0))
    return pl.pallas_call(
        body,
        grid=(rows_dev // per,),
        in_specs=[
            pl.BlockSpec(memory_space=pltpu.SMEM),
            pl.BlockSpec((per * GRID_W, cols), lambda i: (i, 0)),
            whole(before.shape),
            whole(pair.shape),
            whole(after.shape),
        ]
        + [far_spec] * (groups + members)
        + [whole(table.shape), whole((queries, 1))],
        out_specs=pl.BlockSpec((per, GRID_W, cols), lambda i: (i, 0, 0)),
        out_shape=jax.ShapeDtypeStruct((rows_dev, GRID_W, cols), bf16),
        scratch_shapes=[
            pltpu.VMEM((2, cols, lanes), bf16),
            pltpu.VMEM((cols, ctx_count), bf16),
            pltpu.VMEM((padded, cols), bf16),
            pltpu.VMEM((ctx_count, cols), bf16),
        ],
        name="attend",
    )(place, query, before, pair, after, *ctx_keys, *ctx_values, table, ctx_bias)


def finish(attended, w_out, latent, gate, block):
    groups, rows, cols = attended.shape
    samples, tokens, width = latent.shape

    def body(att_ref, w_ref, latent_ref, gate_ref, out_ref):
        update = jnp.dot(att_ref[0], w_ref[:cols], preferred_element_type=jnp.float32)
        for group in range(1, groups):
            update += jnp.dot(
                att_ref[group],
                w_ref[group * cols : (group + 1) * cols],
                preferred_element_type=jnp.float32,
            )
        for s in range(samples):
            part = update[s * tokens : (s + 1) * tokens]
            mixed = latent_ref[s].astype(jnp.float32) + gate_ref[s : s + 1] * part
            out_ref[s] = mixed.astype(jnp.bfloat16)

    return pl.pallas_call(
        body,
        grid=(width // block,),
        in_specs=[
            whole(attended.shape),
            pl.BlockSpec((width, block), lambda i: (0, i)),
            pl.BlockSpec((samples, tokens, block), lambda i: (0, 0, i)),
            pl.BlockSpec((samples, block), lambda i: (0, i)),
        ],
        out_specs=pl.BlockSpec((samples, tokens, block), lambda i: (0, 0, i)),
        out_shape=jax.ShapeDtypeStruct(latent.shape, latent.dtype),
        name="finish",
    )(attended, w_out, latent, gate)


def shifted(axis, digits, digit, value):
    size_z, size_x = digits
    pairs = []
    for z in range(size_z):
        for x in range(size_x):
            to_z = (z + value) % size_z if digit == 0 else z
            to_x = (x + value) % size_x if digit == 1 else x
            pairs.append((z * size_x + x, to_z * size_x + to_x))
    return pairs


def everywhere(block, digits, order):
    for digit in order:
        block = [block] + [
            lax.ppermute(block, "sp", shifted("sp", digits, digit, value))
            for value in range(1, digits[digit])
        ]
        if digit != order[-1]:
            block = jnp.stack(block)
    return block


def on_device(
    latent,
    context,
    cond,
    ctx_cond,
    w_shift,
    w_scale,
    w_gate,
    norm_gain,
    w_query,
    w_key,
    w_value,
    w_out,
    rel_bias,
    ctx_bias,
):
    samples, tokens_dev, width = latent.shape
    local_cols = w_shift.shape[1]
    sp_index = lax.axis_index("sp")
    sp_size, tp_size = lax.axis_size("sp"), lax.axis_size("tp")
    digits = (4, sp_size // 4)
    place = jnp.full((1,), sp_index, jnp.int32)
    gathered = lax.all_gather(latent, "tp", axis=1, tiled=True)
    parts = modulation_parts(place, cond, ctx_cond[None], (w_shift, w_scale, w_gate), sp_size)
    parts, w_out_own = lax.optimization_barrier((parts, w_out))
    w_out_all = lax.all_gather(w_out_own, "tp", axis=0, tiled=True)
    summed = jnp.sum(lax.all_to_all(parts, "sp", 0, 0, tiled=True), axis=0)
    tiles = copy_for_each(summed, "tp")
    modulation = jnp.moveaxis(tiles, 0, 1).reshape(-1, width)
    every = samples + 1
    shift, scale = modulation[:every], modulation[every : 2 * every]
    gate = modulation[2 * every :]

    gain = norm_gain[None, :]
    table = bias_table(rel_bias)
    ctx_rows = context.shape[1]
    (ctx_pair,) = project(
        context.reshape(1, samples * ctx_rows, width),
        0,
        gain,
        shift[samples:],
        scale[samples:],
        (w_key, w_value),
        samples * ctx_rows,
        None,
    )
    ctx_keys = ctx_pair[:, :local_cols].reshape(samples, ctx_rows, local_cols)
    ctx_values = ctx_pair[:, local_cols:].reshape(samples, ctx_rows, local_cols)
    ctx_keys = everywhere(ctx_keys, digits, (1, 0))
    ctx_values = everywhere(ctx_values, digits, (0, 1))
    cb = jnp.repeat(ctx_bias, GRID_W)[:, None]
    up = [(i, i + 1) for i in range(sp_size - 1)]
    down = [(j, i) for i, j in up]
    attended = []
    for s in range(samples):
        pair, query, first, last = project(
            gathered,
            s,
            gain,
            shift[s : s + 1],
            scale[s : s + 1],
            (w_key, w_value, w_query),
            128,
            ((WIN_ROWS - REACH - 1) * GRID_W, REACH * GRID_W),
        )
        before = lax.ppermute(last, "sp", up)
        after = lax.ppermute(first, "sp", down)
        rows_all = pair.shape[0] // GRID_W * sp_size
        attended.append(
            attend(
                place, s, query, before, pair, after, ctx_keys, ctx_values, table, cb, rows_all, 2
            )
        )
    attended = jnp.concatenate(attended, axis=1)
    attended = lax.all_to_all(attended, "tp", 0, 0, tiled=True)
    return finish(attended, w_out_all, latent, gate, 256)


def solution(mesh):
    return jax.shard_map(
        on_device,
        mesh=mesh,
        in_specs=(
            P(None, ("sp", "tp"), None),
            P(None, "sp", None),
            P(),
            P(),
            P("sp", "tp"),
            P("sp", "tp"),
            P("sp", "tp"),
            P(),
            P(None, "tp"),
            P(None, "tp"),
            P(None, "tp"),
            P("tp", None),
            P("tp", None, None),
            P("tp"),
        ),
        out_specs=P(None, ("sp", "tp"), None),
        check_vma=False,
    )
```

time: 196 us -> 144 us (0.73)
  waiting for transfers between devices: 70 us -> 10.4 us
  starting transfers between devices: 16.1 us -> 36 us
  matrix products: 8.98 us -> 0 us
  local copies, waits for them, and re-layouts: 14.2 us -> 7.4 us
  Pallas kernels: 45.6 us -> 49 us
    reduce_scatter x2 -> x0, waiting for transfers between devices: 35.8 us -> none  [on_device(): update = lax.psum_scatter(part, 'tp', scatter_dimension=0, tiled=True)]
    all_gather x3 -> x2, waiting for transfers between devices: 29.2 us -> 0.01 us  [the longest x1 0.01 us: on_device(): gathered = lax.all_gather(latent, 'tp', axis=1, tiled=True)]
    ppermute x4 -> x16, starting transfers between devices: 15.9 us -> 32.5 us  [the longest x12 16.9 us: everywhere(): lax.ppermute(block, 'sp', shifted('sp', digits, digit, value))]
    all_to_all x0 -> x1, blocking collectives: none -> 14.2 us  [on_device(): summed = jnp.sum(lax.all_to_all(parts, 'sp', 0, 0, tiled=True), axis=0)]
    all_to_all x2 -> x1, blocking collectives: 24.1 us -> 10.8 us  [copy_for_each(): lax.all_to_all(jnp.broadcast_to(shard[None], (length, *shard.shape)), axi...]
    all_to_all x0 -> x1, waiting for transfers between devices: none -> 9.63 us  [on_device(): attended = lax.all_to_all(attended, 'tp', 0, 0, tiled=True)]
    dot_general x5 -> x0, matrix products: 8.98 us -> none  [the longest x2 6.06 us: on_device(): jnp.dot(attended, w_out, preferred_element_type=jnp.float32)]
    slice x6 -> x3, local copies, waits for them, and re-layouts: 6.44 us -> 2.14 us  [the longest x1 0.88 us: on_device(): ctx_values = ctx_pair[:, local_cols:].reshape(samples, ctx_rows, local_cols)]
  transfers between devices with their start and end apart: 9 -> 19, of which waited for: 4 -> 1; matrix products, arithmetic and copies ran while one was open for 10% -> 5% of each run, Pallas kernels for 23% -> 29%
where the time goes in v2:
time: 144 us; the launch traced here: 143 us
  Pallas kernels  49 us (34%)
  starting transfers between devices  36 us (25%)
  blocking collectives  25 us (17%)
  between operations  13.7 us (10%)
  waiting for transfers between devices  10.4 us (7%)
  local copies, waits for them, and re-layouts  7.4 us (5%)
  other arithmetic  1.87 us (1%)
    pallas_call x2, Pallas kernels, attend(): pl.pallas_call(body, grid=(rows_dev // per,), in_specs=[pl.BlockSpec(memo...  19.6 us
    ppermute x12, starting transfers between devices, everywhere(): lax.ppermute(block, 'sp', shifted('sp', digits, digit, value))  16.9 us
    pallas_call x3, Pallas kernels, project(): pl.pallas_call(body, grid=(steps,), in_specs=[pl.BlockSpec((1, block, wid...  16.6 us
    all_to_all x1, blocking collectives, on_device(): summed = jnp.sum(lax.all_to_all(parts, 'sp', 0, 0, tiled=True), axis=0)  14.2 us
    all_to_all x1, blocking collectives, copy_for_each(): lax.all_to_all(jnp.broadcast_to(shard[None], (length, *shard.shape)), axi...  10.8 us
    all_to_all x1, waiting for transfers between devices, on_device(): attended = lax.all_to_all(attended, 'tp', 0, 0, tiled=True)  9.63 us
    ppermute x2, starting transfers between devices, on_device(): after = lax.ppermute(first, 'sp', down)  9.38 us
    pallas_call x1, Pallas kernels, finish(): pl.pallas_call(body, grid=(width // block,), in_specs=[whole(attended.sha...  8.01 us
  transfers between devices with their start and end apart: 19, of which 1 were waited for; matrix products, arithmetic and copies ran while one was open for 5% of the time, Pallas kernels for 29%

profile of v2, /device:TPU:32, one launch (start us, length us, event | category | flops | bytes accessed | tf_op | source)
XLA Modules:
  0.0 143.4 jit_solution(9486124900482048694)
XLA Ops:
  6.5 0.7 all-gather.3.cloned.1.call-update
  7.3 0.0 all-gather.5.cloned.1.call-start
  7.3 1.3 broadcast_in_dim.20.ctx_ref
  8.6 1.7 %modulation_parts.1 = f32[16,8,256]{2,1,0:T(8,128)} custom-call(s32[1]{0:T(128)} %bitcast.place_ref, bf16[2,2048]{1,0:T(2,128)(2,1)} %cond_ref.1, bf16[1,2048]{1,0:T(2,128)(2,1)} %broadcast_in_dim.20.ctx_ref, bf16[128,256]{1,0:T(8,128)(2,1)} %shift_ref.1, bf16[128,256]{1,0:T(8,128)(2,1)} %scale_ref.1, bf16[128,256]{1,0:T(8,128)(2,1)} %gate_ref.1), custom_call_target="tpu_custom_call" | custom-call | tf_op jit(solution)/shard_map/modulation_parts/pallas_call | solution.py:50
  10.4 0.0 all-gather.5.cloned.1.call-update
  10.4 14.2 %all_to_all.15 = f32[16,8,256]{2,1,0:T(8,128)S(1)} all-to-all(f32[16,8,256]{2,1,0:T(8,128)} %modulation_parts.1), channel_id=1, replica_groups=mesh['sp'=16,'tp'=8] {'sp'}, dimensions={0} | all-to-all | bytes 262144 | tf_op jit(solution)/shard_map/all_to_all | solution.py:355
  24.6 10.8 %all_to_all.16 = f32[8,8,256]{2,1,0:T(8,128)S(1)} all-to-all(f32[8,8,256]{2,1,0:T(8,128)S(1)} %broadcast_in_dim.21), channel_id=1, replica_groups=mesh['sp'=16,'tp'=8] {'tp'}, dimensions={0} | all-to-all | bytes 131072 | tf_op jit(solution)/shard_map/all_to_all | solution.py:20
  35.4 0.7 fusion.1
  36.1 3.0 %project.4 = bf16[128,512]{1,0:T(8,128)(2,1)} custom-call(bf16[1,128,2048]{2,1,0:T(8,128)(2,1)} %bitcast.22, f32[1,2048]{1,0:T(1,128)} %bitcast.34, f32[1,2048]{1,0:T(1,128)} %bitcast.45, f32[1,2048]{1,0:T(1,128)} %bitcast.44, bf16[2048,256]{1,0:T(8,128)(2,1)} %refs_0_.5, bf16[2048,256]{1,0:T(8,128)(2,1)} %refs_1_.5), custom_call_target="tpu_custom_call" | custom-call | tf_op jit(solution)/shard_map/project/pallas_call | solution.py:110
  39.1 0.9 fusion
  40.0 0.7 collective-permute-start.8
  40.7 3.2 %collective-permute-start.9 = (bf16[2,64,256]{2,1,0:T(8,128)(2,1)S(1)}, bf16[2,64,256]{2,1,0:T(8,128)(2,1)S(1)}, u32[]{:S(2)}, u32[]{:S(2)}) collective-permute-start(bf16[2,64,256]{2,1,0:T(8,128)(2,1)S(1)} %bitcast.30), channel_id=1, source_target_pairs={{0,64},{8,72},{16,80},{24,88},{32,96},{40,104},{48,112},{56,120},{... | collective-permute-start | bytes 196616 | tf_op jit(solution)/shard_map/ppermute | solution.py:321
  43.9 0.2 collective-permute-start.10
  44.2 0.6 collective-permute-start.2
  44.8 2.1 %collective-permute-start.3 = (bf16[2,64,256]{2,1,0:T(8,128)(2,1)S(1)}, bf16[2,64,256]{2,1,0:T(8,128)(2,1)S(1)}, u32[]{:S(2)}, u32[]{:S(2)}) collective-permute-start(bf16[2,64,256]{2,1,0:T(8,128)(2,1)S(1)} %bitcast.26), channel_id=1, source_target_pairs={{0,16},{8,24},{16,0},{24,8},{32,48},{40,56},{48,32},{56,40},{64,80... | collective-permute-start | bytes 196616 | tf_op jit(solution)/shard_map/ppermute | solution.py:321
  46.9 1.4 collective-permute-start.4
  48.3 0.0 collective-permute-done.9
  48.4 0.7 collective-permute-start.11
  49.0 1.7 %collective-permute-start.12 = (bf16[4,2,64,256]{3,2,1,0:T(8,128)(2,1)S(1)}, bf16[4,2,64,256]{3,2,1,0:T(8,128)(2,1)S(1)}, u32[]{:S(2)}, u32[]{:S(2)}) collective-permute-start(bf16[4,2,64,256]{3,2,1,0:T(8,128)(2,1)S(1)} %pad_maximum_fusion.2.refs_4_), channel_id=1, source_target_pairs={{0,16},{8,24},{16,0},{24,8},{32,48},{40,56},{48,32},{56,40},{64,80... | collective-permute-start | bytes 786440 | tf_op jit(solution)/shard_map/ppermute | solution.py:321
  50.8 2.3 %collective-permute-start.13 = (bf16[4,2,64,256]{3,2,1,0:T(8,128)(2,1)S(1)}, bf16[4,2,64,256]{3,2,1,0:T(8,128)(2,1)S(1)}, u32[]{:S(2)}, u32[]{:S(2)}) collective-permute-start(bf16[4,2,64,256]{3,2,1,0:T(8,128)(2,1)S(1)} %pad_maximum_fusion.2.refs_4_), channel_id=1, source_target_pairs={{0,24},{8,0},{16,8},{24,16},{32,56},{40,32},{48,40},{56,48},{64,88... | collective-permute-start | bytes 786440 | tf_op jit(solution)/shard_map/ppermute | solution.py:321
  53.2 1.9 %collective-permute-start.5 = (bf16[4,2,64,256]{3,2,1,0:T(8,128)(2,1)S(1)}, bf16[4,2,64,256]{3,2,1,0:T(8,128)(2,1)S(1)}, u32[]{:S(2)}, u32[]{:S(2)}) collective-permute-start(bf16[4,2,64,256]{3,2,1,0:T(8,128)(2,1)S(1)} %pad_maximum_fusion.1.refs_0_), channel_id=1, source_target_pairs={{0,32},{8,40},{16,48},{24,56},{32,64},{40,72},{48,80},{56,88},{64,... | collective-permute-start | bytes 786440 | tf_op jit(solution)/shard_map/ppermute | solution.py:321
  55.0 1.5 %collective-permute-start.6 = (bf16[4,2,64,256]{3,2,1,0:T(8,128)(2,1)S(1)}, bf16[4,2,64,256]{3,2,1,0:T(8,128)(2,1)S(1)}, u32[]{:S(2)}, u32[]{:S(2)}) collective-permute-start(bf16[4,2,64,256]{3,2,1,0:T(8,128)(2,1)S(1)} %pad_maximum_fusion.1.refs_0_), channel_id=1, source_target_pairs={{0,64},{8,72},{16,80},{24,88},{32,96},{40,104},{48,112},{56,120},{... | collective-permute-start | bytes 786440 | tf_op jit(solution)/shard_map/ppermute | solution.py:321
  56.5 7.0 %project.3 = (bf16[512,512]{1,0:T(8,128)(2,1)}, bf16[512,256]{1,0:T(8,128)(2,1)}, bf16[192,512]{1,0:T(8,128)(2,1)}, bf16[256,512]{1,0:T(8,128)(2,1)}) custom-call(bf16[2,512,2048]{2,1,0:T(8,128)(2,1)} %all-gather.3.cloned.1.call-done.rows_ref, f32[1,2048]{1,0:T(1,128)} %bitcast.35, f32[1,2048]{1,0:T(1,128)} %bitcast.49, f32[1,2048]{1,0:T(1,128)} %bitcast.48, ...), custom_call_target="tpu_custom_call" | custom-call | tf_op jit(solution)/shard_map/project/pallas_call | solution.py:110
  63.5 0.0 copy-start.14
  63.6 0.5 collective-permute-start.7
  64.1 4.3 %collective-permute-start = (bf16[256,512]{1,0:T(8,128)(2,1)}, bf16[256,512]{1,0:T(8,128)(2,1)S(1)}, u32[]{:S(2)}, u32[]{:S(2)}) collective-permute-start(bf16[256,512]{1,0:T(8,128)(2,1)} %get-tuple-element.17), channel_id=1, source_target_pairs={{0,8},{8,16},{16,24},{24,32},{32,40},{40,48},{48,56},{56,64},{64,7... | collective-permute-start | bytes 786440 | tf_op jit(solution)/shard_map/ppermute | solution.py:394
  68.3 0.0 copy-start.15
  68.3 6.6 %project.5 = (bf16[512,512]{1,0:T(8,128)(2,1)}, bf16[512,256]{1,0:T(8,128)(2,1)}, bf16[192,512]{1,0:T(8,128)(2,1)}, bf16[256,512]{1,0:T(8,128)(2,1)}) custom-call(bf16[2,512,2048]{2,1,0:T(8,128)(2,1)} %all-gather.3.cloned.1.call-done.rows_ref, f32[1,2048]{1,0:T(1,128)} %bitcast.36, f32[1,2048]{1,0:T(1,128)} %bitcast.47, f32[1,2048]{1,0:T(1,128)} %bitcast.46, ...), custom_call_target="tpu_custom_call" | custom-call | tf_op jit(solution)/shard_map/project/pallas_call | solution.py:110
  75.0 1.9 %collective-permute-start.14 = (bf16[256,512]{1,0:T(8,128)(2,1)}, bf16[256,512]{1,0:T(8,128)(2,1)S(1)}, u32[]{:S(2)}, u32[]{:S(2)}) collective-permute-start(bf16[256,512]{1,0:T(8,128)(2,1)} %get-tuple-element.21), channel_id=1, source_target_pairs={{0,8},{8,16},{16,24},{24,32},{32,40},{40,48},{48,56},{56,64},{64,7... | collective-permute-start | bytes 786440 | tf_op jit(solution)/shard_map/ppermute | solution.py:394
  76.9 6.0 %collective-permute-start.1 = (bf16[192,512]{1,0:T(8,128)(2,1)S(1)}, bf16[192,512]{1,0:T(8,128)(2,1)S(1)}, u32[]{:S(2)}, u32[]{:S(2)}) collective-permute-start(bf16[192,512]{1,0:T(8,128)(2,1)S(1)} %copy-done.16), channel_id=1, source_target_pairs={{8,0},{16,8},{24,16},{32,24},{40,32},{48,40},{56,48},{64,56},{72,6... | collective-permute-start | bytes 589832 | tf_op jit(solution)/shard_map/ppermute | solution.py:395
  83.0 3.4 %collective-permute-start.15 = (bf16[192,512]{1,0:T(8,128)(2,1)}, bf16[192,512]{1,0:T(8,128)(2,1)S(1)}, u32[]{:S(2)}, u32[]{:S(2)}) collective-permute-start(bf16[192,512]{1,0:T(8,128)(2,1)} %get-tuple-element.23), channel_id=1, source_target_pairs={{8,0},{16,8},{24,16},{32,24},{40,32},{48,40},{56,48},{64,56},{72,6... | collective-permute-start | bytes 589832 | tf_op jit(solution)/shard_map/ppermute | solution.py:395
  86.4 0.6 pad.4.clone
  87.0 3.0 %bias_table.1.refs_8_ = f32[2,256,896]{2,1,0:T(8,128)} custom-call(f32[64,128]{1,0:T(8,128)} %bitcast.33), custom_call_target="tpu_custom_call" | custom-call | tf_op jit(solution)/shard_map/bias_table/pallas_call | solution.py:151
  90.0 0.1 broadcast_in_dim.22
  90.1 0.8 broadcast_in_dim_reshape.4.refs_9_
  91.0 0.6 copy-done.8
  91.6 0.1 copy-done.13
  91.7 0.1 copy-done.11
  91.8 9.8 %attend.2 = bf16[8,64,256]{2,1,0:T(8,128)(2,1)} custom-call(s32[1]{0:T(128)} %bitcast.place_ref, bf16[512,256]{1,0:T(8,128)(2,1)} %get-tuple-element.16.q_ref, bf16[256,512]{1,0:T(8,128)(2,1)} %copy-done.11, bf16[512,512]{1,0:T(8,128)(2,1)} %get-tuple-element.18.pair_ref, bf16[192,512]{1,0:T(8,128)(2,1)} %copy-done.13, bf16[4,2,64,256]{3,2,1,0:T(8,128)(2,1)} %copy-done.1, ...), custom_call_target="tpu_custom_call" | custom-call | tf_op jit(solution)/shard_map/attend/pallas_call | solution.py:251
  101.6 0.6 copy-done.12
  102.3 0.1 copy-done.10
  102.4 9.8 %attend.3 = bf16[8,64,256]{2,1,0:T(8,128)(2,1)} custom-call(s32[1]{0:T(128)} %bitcast.place_ref, bf16[512,256]{1,0:T(8,128)(2,1)} %get-tuple-element.20.q_ref, bf16[256,512]{1,0:T(8,128)(2,1)} %copy-done.10, bf16[512,512]{1,0:T(8,128)(2,1)} %get-tuple-element.22.pair_ref, bf16[192,512]{1,0:T(8,128)(2,1)} %copy-done.12, bf16[4,2,64,256]{3,2,1,0:T(8,128)(2,1)} %copy-done.1, ...), custom_call_target="tpu_custom_call" | custom-call | tf_op jit(solution)/shard_map/attend/pallas_call | solution.py:251
  112.2 1.8 %pad_maximum_fusion = bf16[8,128,256]{2,1,0:T(8,128)(2,1)} fusion(bf16[8,64,256]{2,1,0:T(8,128)(2,1)} %attend.3, bf16[8,64,256]{2,1,0:T(8,128)(2,1)S(1)} %copy-done.9), kind=kLoop, calls=%fused_computation | loop fusion | flops 1048576 | bytes 1048576 | tf_op jit(solution)/shard_map/concatenate | solution.py:402
  114.0 3.5 %all-to-all-start.2 = ((bf16[8,128,256]{2,1,0:T(8,128)(2,1)}), bf16[8,128,256]{2,1,0:T(8,128)(2,1)S(1)}, u32[]{:S(2)}, u32[]{:S(2)}) async-start(bf16[8,128,256]{2,1,0:T(8,128)(2,1)} %pad_maximum_fusion), calls=%async_computation.2 | async-start | bytes 1048576 | tf_op jit(solution)/shard_map/all_to_all | solution.py:403
  117.5 0.6 slice.82
  118.1 9.6 %all-to-all-done.2.att_ref = bf16[8,128,256]{2,1,0:T(8,128)(2,1)S(1)} async-done(((bf16[8,128,256]{2,1,0:T(8,128)(2,1)}), bf16[8,128,256]{2,1,0:T(8,128)(2,1)S(1)}, u32[]{:S(2)}, u32[]{:S(2)}) %all-to-all-start.2) | async-done | bytes 524320 | tf_op jit(solution)/shard_map/all_to_all | solution.py:403
  127.7 0.8 copy-done.2
  128.6 8.0 %finish.1 = bf16[2,64,2048]{2,1,0:T(8,128)(2,1)} custom-call(bf16[8,128,256]{2,1,0:T(8,128)(2,1)} %copy-done.2, bf16[2048,2048]{1,0:T(8,128)(2,1)} %all-gather.5.cloned.1.call-done.w_ref, bf16[2,64,2048]{2,1,0:T(8,128)(2,1)} %latent_ref.1, f32[2,2048]{1,0:T(2,128)} %bitcast.37), custom_call_target="tpu_custom_call" | custom-call | tf_op jit(solution)/shard_map/finish/pallas_call | solution.py:292
  (49 shorter events, 0.2 us)
Async XLA Ops:
  6.5 50.0 %all-gather.3.cloned.1.call-start = ((), (), s32[]{:S(2)}) async-start(), calls=%async_computation.3 | async-start | bytes 4718592 | tf_op jit(solution)/shard_map/all_gather | solution.py:351
  7.3 120.5 %all-gather.5.cloned.1.call-start = ((), (), s32[]{:S(2)}) async-start(), calls=%async_computation.4 | async-start | bytes 9437184 | tf_op jit(solution)/shard_map/all_gather | solution.py:354
  40.0 6.9 %collective-permute-start.8 = (bf16[2,64,256]{2,1,0:T(8,128)(2,1)S(1)}, bf16[2,64,256]{2,1,0:T(8,128)(2,1)S(1)}, u32[]{:S(2)}, u32[]{:S(2)}) collective-permute-start(bf16[2,64,256]{2,1,0:T(8,128)(2,1)S(1)} %bitcast.29), channel_id=1, source_target_pairs={{0,32},{8,40},{16,48},{24,56},{32,64},{40,72},{48,80},{56,88},{64,... | collective-permute-start | bytes 196616 | tf_op jit(solution)/shard_map/ppermute | solution.py:321
  40.7 7.6 %collective-permute-start.9 = (bf16[2,64,256]{2,1,0:T(8,128)(2,1)S(1)}, bf16[2,64,256]{2,1,0:T(8,128)(2,1)S(1)}, u32[]{:S(2)}, u32[]{:S(2)}) collective-permute-start(bf16[2,64,256]{2,1,0:T(8,128)(2,1)S(1)} %bitcast.30), channel_id=1, source_target_pairs={{0,64},{8,72},{16,80},{24,88},{32,96},{40,104},{48,112},{56,120},{... | collective-permute-start | bytes 196616 | tf_op jit(solution)/shard_map/ppermute | solution.py:321
  43.9 4.4 %collective-permute-start.10 = (bf16[2,64,256]{2,1,0:T(8,128)(2,1)S(1)}, bf16[2,64,256]{2,1,0:T(8,128)(2,1)S(1)}, u32[]{:S(2)}, u32[]{:S(2)}) collective-permute-start(bf16[2,64,256]{2,1,0:T(8,128)(2,1)S(1)} %bitcast.31), channel_id=1, source_target_pairs={{0,96},{8,104},{16,112},{24,120},{32,0},{40,8},{48,16},{56,24},{64... | collective-permute-start | bytes 196616 | tf_op jit(solution)/shard_map/ppermute | solution.py:321
  44.2 6.6 %collective-permute-start.2 = (bf16[2,64,256]{2,1,0:T(8,128)(2,1)S(1)}, bf16[2,64,256]{2,1,0:T(8,128)(2,1)S(1)}, u32[]{:S(2)}, u32[]{:S(2)}) collective-permute-start(bf16[2,64,256]{2,1,0:T(8,128)(2,1)S(1)} %bitcast.25), channel_id=1, source_target_pairs={{0,8},{8,16},{16,24},{24,0},{32,40},{40,48},{48,56},{56,32},{64,72... | collective-permute-start | bytes 196616 | tf_op jit(solution)/shard_map/ppermute | solution.py:321
  44.8 8.3 %collective-permute-start.3 = (bf16[2,64,256]{2,1,0:T(8,128)(2,1)S(1)}, bf16[2,64,256]{2,1,0:T(8,128)(2,1)S(1)}, u32[]{:S(2)}, u32[]{:S(2)}) collective-permute-start(bf16[2,64,256]{2,1,0:T(8,128)(2,1)S(1)} %bitcast.26), channel_id=1, source_target_pairs={{0,16},{8,24},{16,0},{24,8},{32,48},{40,56},{48,32},{56,40},{64,80... | collective-permute-start | bytes 196616 | tf_op jit(solution)/shard_map/ppermute | solution.py:321
  46.9 6.2 %collective-permute-start.4 = (bf16[2,64,256]{2,1,0:T(8,128)(2,1)S(1)}, bf16[2,64,256]{2,1,0:T(8,128)(2,1)S(1)}, u32[]{:S(2)}, u32[]{:S(2)}) collective-permute-start(bf16[2,64,256]{2,1,0:T(8,128)(2,1)S(1)} %bitcast.27), channel_id=1, source_target_pairs={{0,24},{8,0},{16,8},{24,16},{32,56},{40,32},{48,40},{56,48},{64,88... | collective-permute-start | bytes 196616 | tf_op jit(solution)/shard_map/ppermute | solution.py:321
  48.4 26.6 %copy-start = (bf16[4,2,64,256]{3,2,1,0:T(8,128)(2,1)}, bf16[4,2,64,256]{3,2,1,0:T(8,128)(2,1)S(1)}, u32[]{:S(2)}) copy-start(bf16[4,2,64,256]{3,2,1,0:T(8,128)(2,1)S(1)} %pad_maximum_fusion.2.refs_4_) | copy-start | bytes 786436
  48.4 15.2 %collective-permute-start.11 = (bf16[4,2,64,256]{3,2,1,0:T(8,128)(2,1)S(1)}, bf16[4,2,64,256]{3,2,1,0:T(8,128)(2,1)S(1)}, u32[]{:S(2)}, u32[]{:S(2)}) collective-permute-start(bf16[4,2,64,256]{3,2,1,0:T(8,128)(2,1)S(1)} %pad_maximum_fusion.2.refs_4_), channel_id=1, source_target_pairs={{0,8},{8,16},{16,24},{24,0},{32,40},{40,48},{48,56},{56,32},{64,72... | collective-permute-start | bytes 786440 | tf_op jit(solution)/shard_map/ppermute | solution.py:321
  49.0 15.0 %collective-permute-start.12 = (bf16[4,2,64,256]{3,2,1,0:T(8,128)(2,1)S(1)}, bf16[4,2,64,256]{3,2,1,0:T(8,128)(2,1)S(1)}, u32[]{:S(2)}, u32[]{:S(2)}) collective-permute-start(bf16[4,2,64,256]{3,2,1,0:T(8,128)(2,1)S(1)} %pad_maximum_fusion.2.refs_4_), channel_id=1, source_target_pairs={{0,16},{8,24},{16,0},{24,8},{32,48},{40,56},{48,32},{56,40},{64,80... | collective-permute-start | bytes 786440 | tf_op jit(solution)/shard_map/ppermute | solution.py:321
  50.8 24.2 %collective-permute-start.13 = (bf16[4,2,64,256]{3,2,1,0:T(8,128)(2,1)S(1)}, bf16[4,2,64,256]{3,2,1,0:T(8,128)(2,1)S(1)}, u32[]{:S(2)}, u32[]{:S(2)}) collective-permute-start(bf16[4,2,64,256]{3,2,1,0:T(8,128)(2,1)S(1)} %pad_maximum_fusion.2.refs_4_), channel_id=1, source_target_pairs={{0,24},{8,0},{16,8},{24,16},{32,56},{40,32},{48,40},{56,48},{64,88... | collective-permute-start | bytes 786440 | tf_op jit(solution)/shard_map/ppermute | solution.py:321
  53.1 21.8 %copy-start.1 = (bf16[4,2,64,256]{3,2,1,0:T(8,128)(2,1)}, bf16[4,2,64,256]{3,2,1,0:T(8,128)(2,1)S(1)}, u32[]{:S(2)}) copy-start(bf16[4,2,64,256]{3,2,1,0:T(8,128)(2,1)S(1)} %pad_maximum_fusion.1.refs_0_) | copy-start | bytes 786436
  53.2 23.7 %collective-permute-start.5 = (bf16[4,2,64,256]{3,2,1,0:T(8,128)(2,1)S(1)}, bf16[4,2,64,256]{3,2,1,0:T(8,128)(2,1)S(1)}, u32[]{:S(2)}, u32[]{:S(2)}) collective-permute-start(bf16[4,2,64,256]{3,2,1,0:T(8,128)(2,1)S(1)} %pad_maximum_fusion.1.refs_0_), channel_id=1, source_target_pairs={{0,32},{8,40},{16,48},{24,56},{32,64},{40,72},{48,80},{56,88},{64,... | collective-permute-start | bytes 786440 | tf_op jit(solution)/shard_map/ppermute | solution.py:321
  55.0 28.0 %collective-permute-start.6 = (bf16[4,2,64,256]{3,2,1,0:T(8,128)(2,1)S(1)}, bf16[4,2,64,256]{3,2,1,0:T(8,128)(2,1)S(1)}, u32[]{:S(2)}, u32[]{:S(2)}) collective-permute-start(bf16[4,2,64,256]{3,2,1,0:T(8,128)(2,1)S(1)} %pad_maximum_fusion.1.refs_0_), channel_id=1, source_target_pairs={{0,64},{8,72},{16,80},{24,88},{32,96},{40,104},{48,112},{56,120},{... | collective-permute-start | bytes 786440 | tf_op jit(solution)/shard_map/ppermute | solution.py:321
  63.5 13.4 %copy-start.16 = (bf16[192,512]{1,0:T(8,128)(2,1)S(1)}, bf16[192,512]{1,0:T(8,128)(2,1)}, u32[]{:S(2)}) copy-start(bf16[192,512]{1,0:T(8,128)(2,1)} %get-tuple-element.19) | copy-start | bytes 589828
  63.5 22.8 %copy-start.14 = (f32[4,15,31]{2,0,1:T(4,128)S(1)}, f32[4,15,31]{2,0,1:T(4,128)}, u32[]{:S(2)}) copy-start(f32[4,15,31]{2,0,1:T(4,128)} %param.26) | copy-start | bytes 22324
  63.6 26.4 %copy-start.3 = (bf16[4,2,64,256]{3,2,1,0:T(8,128)(2,1)}, bf16[4,2,64,256]{3,2,1,0:T(8,128)(2,1)S(1)}, u32[]{:S(2)}) copy-start(bf16[4,2,64,256]{3,2,1,0:T(8,128)(2,1)S(1)} %collective-permute-done.11.refs_5_) | copy-start | bytes 786436
  63.6 27.3 %collective-permute-start.7 = (bf16[4,2,64,256]{3,2,1,0:T(8,128)(2,1)S(1)}, bf16[4,2,64,256]{3,2,1,0:T(8,128)(2,1)S(1)}, u32[]{:S(2)}, u32[]{:S(2)}) collective-permute-start(bf16[4,2,64,256]{3,2,1,0:T(8,128)(2,1)S(1)} %pad_maximum_fusion.1.refs_0_), channel_id=1, source_target_pairs={{0,96},{8,104},{16,112},{24,120},{32,0},{40,8},{48,16},{56,24},{64... | collective-permute-start | bytes 786440 | tf_op jit(solution)/shard_map/ppermute | solution.py:321
  64.0 26.0 %copy-start.4 = (bf16[4,2,64,256]{3,2,1,0:T(8,128)(2,1)}, bf16[4,2,64,256]{3,2,1,0:T(8,128)(2,1)S(1)}, u32[]{:S(2)}) copy-start(bf16[4,2,64,256]{3,2,1,0:T(8,128)(2,1)S(1)} %collective-permute-done.12.refs_6_) | copy-start | bytes 786436
  64.1 26.9 %collective-permute-start = (bf16[256,512]{1,0:T(8,128)(2,1)}, bf16[256,512]{1,0:T(8,128)(2,1)S(1)}, u32[]{:S(2)}, u32[]{:S(2)}) collective-permute-start(bf16[256,512]{1,0:T(8,128)(2,1)} %get-tuple-element.17), channel_id=1, source_target_pairs={{0,8},{8,16},{16,24},{24,32},{32,40},{40,48},{48,56},{56,64},{64,7... | collective-permute-start | bytes 786440 | tf_op jit(solution)/shard_map/ppermute | solution.py:394
  68.3 21.7 %copy-start.15 = (f32[4]{0:T(128)S(1)}, f32[4]{0:T(128)}, u32[]{:S(2)}) copy-start(f32[4]{0:T(128)} %param.27) | copy-start | bytes 52
  74.9 16.0 %copy-start.5 = (bf16[4,2,64,256]{3,2,1,0:T(8,128)(2,1)}, bf16[4,2,64,256]{3,2,1,0:T(8,128)(2,1)S(1)}, u32[]{:S(2)}) copy-start(bf16[4,2,64,256]{3,2,1,0:T(8,128)(2,1)S(1)} %collective-permute-done.13.refs_7_) | copy-start | bytes 786436
  75.0 26.6 %collective-permute-start.14 = (bf16[256,512]{1,0:T(8,128)(2,1)}, bf16[256,512]{1,0:T(8,128)(2,1)S(1)}, u32[]{:S(2)}, u32[]{:S(2)}) collective-permute-start(bf16[256,512]{1,0:T(8,128)(2,1)} %get-tuple-element.21), channel_id=1, source_target_pairs={{0,8},{8,16},{16,24},{24,32},{32,40},{40,48},{48,56},{56,64},{64,7... | collective-permute-start | bytes 786440 | tf_op jit(solution)/shard_map/ppermute | solution.py:394
  76.9 14.0 %copy-start.6 = (bf16[4,2,64,256]{3,2,1,0:T(8,128)(2,1)}, bf16[4,2,64,256]{3,2,1,0:T(8,128)(2,1)S(1)}, u32[]{:S(2)}) copy-start(bf16[4,2,64,256]{3,2,1,0:T(8,128)(2,1)S(1)} %collective-permute-done.5.refs_1_) | copy-start | bytes 786436
  76.9 14.0 %collective-permute-start.1 = (bf16[192,512]{1,0:T(8,128)(2,1)S(1)}, bf16[192,512]{1,0:T(8,128)(2,1)S(1)}, u32[]{:S(2)}, u32[]{:S(2)}) collective-permute-start(bf16[192,512]{1,0:T(8,128)(2,1)S(1)} %copy-done.16), channel_id=1, source_target_pairs={{8,0},{16,8},{24,16},{32,24},{40,32},{48,40},{56,48},{64,56},{72,6... | collective-permute-start | bytes 589832 | tf_op jit(solution)/shard_map/ppermute | solution.py:395
  83.0 8.0 %copy-start.7 = (bf16[4,2,64,256]{3,2,1,0:T(8,128)(2,1)}, bf16[4,2,64,256]{3,2,1,0:T(8,128)(2,1)S(1)}, u32[]{:S(2)}) copy-start(bf16[4,2,64,256]{3,2,1,0:T(8,128)(2,1)S(1)} %collective-permute-done.6.refs_2_) | copy-start | bytes 786436
  83.0 18.6 %collective-permute-start.15 = (bf16[192,512]{1,0:T(8,128)(2,1)}, bf16[192,512]{1,0:T(8,128)(2,1)S(1)}, u32[]{:S(2)}, u32[]{:S(2)}) collective-permute-start(bf16[192,512]{1,0:T(8,128)(2,1)} %get-tuple-element.23), channel_id=1, source_target_pairs={{8,0},{16,8},{24,16},{32,24},{40,32},{48,40},{56,48},{64,56},{72,6... | collective-permute-start | bytes 589832 | tf_op jit(solution)/shard_map/ppermute | solution.py:395
  90.9 0.7 copy-start.8
  90.9 0.8 copy-start.13
  90.9 0.8 copy-start.11
  101.6 10.6 %copy-start.9 = (bf16[8,64,256]{2,1,0:T(8,128)(2,1)S(1)}, bf16[8,64,256]{2,1,0:T(8,128)(2,1)}, u32[]{:S(2)}) copy-start(bf16[8,64,256]{2,1,0:T(8,128)(2,1)} %attend.2) | copy-start | bytes 786436
  101.6 0.7 copy-start.12
  101.6 0.8 copy-start.10
  114.0 13.7 %all-to-all-start.2 = ((bf16[8,128,256]{2,1,0:T(8,128)(2,1)}), bf16[8,128,256]{2,1,0:T(8,128)(2,1)S(1)}, u32[]{:S(2)}, u32[]{:S(2)}) async-start(bf16[8,128,256]{2,1,0:T(8,128)(2,1)} %pad_maximum_fusion), calls=%async_computation.2 | async-start | bytes 1048576 | tf_op jit(solution)/shard_map/all_to_all | solution.py:403
  127.7 0.8 copy-start.2
Sparse Core Ops, SparseCore 0:
  9.0 34.7 all-gather.2
  45.5 49.5 all-gather.4

commit v3 on v2

v3 whole, which is shorter than its diff:
```python
import jax
import jax.numpy as jnp
from jax import lax
from jax.experimental import pallas as pl
from jax.experimental.pallas import tpu as pltpu
from jax.sharding import PartitionSpec as P


HEAD_DIM = 64
GRID_W = 64
WIN_ROWS = 8
WIN_COLS = 16
EPSILON = 1e-06
MASKED = -1e30
REACH = WIN_ROWS // 2
BIAS_BLOCKS = 7


def copy_for_each(shard, axis):
    length = lax.axis_size(axis)
    return lax.all_to_all(
        jnp.broadcast_to(shard[None], (length, *shard.shape)), axis, 0, 0, tiled=True
    )


def silu_rows(values):
    return jax.nn.silu(values.astype(jnp.float32)).astype(jnp.bfloat16)


def modulation_parts(place, cond, ctx_cond, weights, copies):
    samples = cond.shape[0]
    rows, cols = weights[0].shape

    def body(place_ref, cond_ref, ctx_ref, shift_ref, scale_ref, gate_ref, out_ref):
        at = pl.multiple_of(place_ref[0] * rows, rows)
        ada = silu_rows(cond_ref[:, pl.ds(at, rows)])
        ada_ctx = silu_rows(ctx_ref[:, pl.ds(at, rows)])
        both = jnp.concatenate([ada.astype(jnp.float32), ada_ctx.astype(jnp.float32)], axis=0)
        both = both.astype(jnp.bfloat16)
        result = jnp.concatenate(
            [
                jnp.dot(both, shift_ref[...], preferred_element_type=jnp.float32),
                jnp.dot(both, scale_ref[...], preferred_element_type=jnp.float32),
                jnp.dot(ada, gate_ref[...], preferred_element_type=jnp.float32),
            ],
            axis=0,
        )
        for copy in range(copies):
            out_ref[copy] = result

    return pl.pallas_call(
        body,
        in_specs=[pl.BlockSpec(memory_space=pltpu.SMEM)]
        + [pl.BlockSpec(memory_space=pltpu.VMEM)] * 5,
        out_shape=jax.ShapeDtypeStruct((copies, 3 * samples + 2, cols), jnp.float32),
        name="modulation_parts",
    )(place, cond, ctx_cond, *weights)


def whole(shape):
    return pl.BlockSpec(shape, lambda *_: (0,) * len(shape))


def modulation_row(tiles, row):
    return jnp.concatenate([tiles[tile, row : row + 1, :] for tile in range(tiles.shape[0])], axis=1)


def project(rows, gain, modulation, weights, row_of, block, ends):
    samples, count, width = rows.shape
    every = modulation.shape[1] // 3 + 1
    cols = weights[0].shape[1]
    first, last = ends if ends else (0, 0)
    steps = count // block

    def body(rows_ref, gain_ref, tiles_ref, *refs):
        weight_refs, out_refs = refs[: len(weights)], refs[len(weights) : -2]
        factor_ref, shift_ref = refs[-2:]
        sample, step = pl.program_id(0), pl.program_id(1)

        for number in range(samples):

            @pl.when((sample == number) & (step == 0))
            def _(number=number):
                row = row_of + number
                factor_ref[...] = gain_ref[...] * (1.0 + modulation_row(tiles_ref, every + row))
                shift_ref[...] = modulation_row(tiles_ref, row)

        floats = rows_ref[0].astype(jnp.float32)
        inverse = lax.rsqrt(jnp.mean(floats * floats, axis=-1, keepdims=True) + EPSILON)
        hidden = (floats * inverse * factor_ref[...] + shift_ref[...]).astype(jnp.bfloat16)
        pair = [
            jnp.dot(hidden, ref[...], preferred_element_type=jnp.float32).astype(jnp.bfloat16)
            for ref in weight_refs[:2]
        ]
        if not ends:
            out_refs[0][0] = pair[0]
            out_refs[1][0] = pair[1]
            return
        out_refs[0][0, :, :cols] = pair[0]
        out_refs[0][0, :, cols:] = pair[1]
        query = jnp.dot(hidden, weight_refs[2][...], preferred_element_type=jnp.float32)
        query = query.astype(jnp.bfloat16).astype(jnp.float32) * HEAD_DIM**-0.5
        out_refs[1][0] = query.astype(jnp.bfloat16)
        for number in range(steps):
            low = number * block
            for out_ref, start, stop in (
                (out_refs[2], 0, first),
                (out_refs[3], count - last, count),
            ):
                lo, hi = max(low, start), min(low + block, stop)
                if lo < hi:

                    @pl.when(step == number)
                    def _(out_ref=out_ref, start=start, lo=lo, hi=hi, low=low):
                        for index in range(2):
                            out_ref[
                                0, lo - start : hi - start, index * cols : (index + 1) * cols
                            ] = pair[index][lo - low : hi - low]

    def blocks(size):
        return pl.BlockSpec((1, block, size), lambda s, i: (s, i, 0))

    if ends:
        out_specs = [blocks(2 * cols), blocks(cols)]
        out_shape = [(samples, count, 2 * cols), (samples, count, cols)]
        for length in ends:
            out_specs += [pl.BlockSpec((1, length, 2 * cols), lambda s, i: (s, 0, 0))]
            out_shape += [(samples, length, 2 * cols)]
    else:
        out_specs = [blocks(cols)] * 2
        out_shape = [(samples, count, cols)] * 2
    return pl.pallas_call(
        body,
        grid=(samples, steps),
        in_specs=[blocks(width), whole((1, width)), whole(modulation.shape)]
        + [whole(weight.shape) for weight in weights],
        out_specs=out_specs,
        out_shape=[jax.ShapeDtypeStruct(shape, jnp.bfloat16) for shape in out_shape],
        scratch_shapes=[pltpu.VMEM((1, width), jnp.float32)] * 2,
        name="project",
    )(rows, gain, modulation, *weights)


def bias_table(rel_bias):
    heads, offsets, spread = rel_bias.shape
    slots = 2 * BIAS_BLOCKS + 2
    padded = jnp.pad(rel_bias, ((0, 0), (0, slots - offsets), (0, 128 - spread)))
    padded = padded.reshape(heads * slots, 128)

    def body(rel_ref, out_ref):
        query = lax.broadcasted_iota(jnp.int32, (GRID_W, 128), 0)
        lane = lax.broadcasted_iota(jnp.int32, (GRID_W, 128), 1)
        low = lane < GRID_W
        key = jnp.where(low, lane, lane - GRID_W)
        start = jnp.clip(query - WIN_COLS // 2, 0, GRID_W - WIN_COLS)
        inside = (key >= start) & (key < start + WIN_COLS)

        def diagonal(head, slot, move):
            row = jnp.broadcast_to(rel_ref[pl.ds(head * slots + slot, 1), :], (GRID_W, 128))
            return pltpu.roll(row, (128 - (WIN_COLS - 1) + move) % 128, 1, stride=1, stride_axis=0)

        for parity in range(2):
            for head in range(heads):
                for block in range(BIAS_BLOCKS):
                    slot = 2 * block + parity
                    both = jnp.where(
                        low, diagonal(head, slot, 0), diagonal(head, slot + 1, GRID_W)
                    )
                    out_ref[
                        parity, head * GRID_W : (head + 1) * GRID_W, block * 128 : (block + 1) * 128
                    ] = jnp.where(inside, both, MASKED)

    return pl.pallas_call(
        body,
        out_shape=jax.ShapeDtypeStruct((2, heads * GRID_W, BIAS_BLOCKS * 128), jnp.float32),
        name="bias_table",
    )(padded)


def attend(place, query, before, pair, after, ctx_keys, ctx_values, table, ctx_bias, rows_all, per):
    samples, tokens, cols = query.shape
    heads = cols // HEAD_DIM
    rows_dev = tokens // GRID_W
    near_keys = WIN_ROWS * GRID_W
    ahead, behind = before.shape[1], after.shape[1]
    padded = ahead + tokens + behind
    lanes = -(-padded // 128) * 128
    groups, members, _, ctx_rows, _ = (len(ctx_keys), *ctx_keys[0].shape)
    ctx_count = groups * members * ctx_rows
    queries = heads * GRID_W
    bf16, f32 = jnp.bfloat16, jnp.float32

    def body(place_ref, q_ref, before_ref, pair_ref, after_ref, *refs):
        key_refs, value_refs = refs[:groups], refs[groups : groups + members]
        table_ref, cb_ref, out_ref, near_t, far_t, values, far_values = refs[groups + members :]
        step = pl.program_id(1)

        @pl.when(step == 0)
        def _():
            values[0:ahead] = before_ref[0, :, cols:]
            values[ahead : ahead + tokens] = pair_ref[0, :, cols:]
            values[ahead + tokens : padded] = after_ref[0, :, cols:]
            for group in range(groups):
                block = jnp.concatenate([key_refs[group][m, 0] for m in range(members)], axis=0)
                size = members * ctx_rows
                far_t[:, group * size : (group + 1) * size] = block.T
                for member in range(members):
                    at = (group * members + member) * ctx_rows
                    far_values[at : at + ctx_rows] = value_refs[member][group, 0]
            fill = jnp.zeros((lanes - padded, cols), bf16)
            near_t[0, :, :ahead] = before_ref[0, :, :cols].T
            near_t[0, :, ahead : ahead + tokens] = pair_ref[0, :, :cols].T
            near_t[0, :, ahead + tokens :] = jnp.concatenate(
                [after_ref[0, :, :cols], fill], axis=0
            ).T
            near_t[1] = jnp.concatenate(
                [
                    before_ref[0, GRID_W:, :cols],
                    pair_ref[0, :, :cols],
                    after_ref[0, :, :cols],
                    fill,
                    jnp.zeros((GRID_W, cols), bf16),
                ],
                axis=0,
            ).T

        base = place_ref[0] * rows_dev
        lane = lax.broadcasted_iota(jnp.int32, (GRID_W, cols), 1)
        masks = [(lane >= h * HEAD_DIM) & (lane < (h + 1) * HEAD_DIM) for h in range(heads)]
        cb = cb_ref[...]
        spreads, nears, starts = [], [], []
        for r in range(per):
            actual = base + step * per + r
            start = jnp.clip(actual - REACH, 0, rows_all - WIN_ROWS)
            local = start - base + REACH
            offset = start - actual + WIN_ROWS - 1
            q = q_ref[0, r * GRID_W : (r + 1) * GRID_W]
            spread = jnp.concatenate(
                [jnp.where(mask, q, jnp.zeros_like(q)) for mask in masks], axis=0
            )
            spreads.append(spread)
            column = pl.multiple_of((local // 2) * 128, 128)
            keys_t = near_t[local % 2, :, pl.ds(column, near_keys)]
            bias_at = pl.multiple_of((offset // 2) * 128, 128)
            nears.append(
                jnp.dot(spread, keys_t, preferred_element_type=f32)
                + table_ref[offset % 2, :, pl.ds(bias_at, near_keys)]
            )
            starts.append(pl.multiple_of(local * GRID_W, GRID_W))
        for r in range(per):
            near = nears[r]
            far = jnp.dot(spreads[r], far_t[...], preferred_element_type=f32)
            top = jnp.maximum(
                jnp.max(near, axis=-1, keepdims=True), jnp.max(far, axis=-1, keepdims=True) + cb
            )
            near_exp = jnp.exp(near - top)
            far_exp = jnp.exp(far - (top - cb))
            total = jnp.sum(near_exp, axis=-1, keepdims=True) + jnp.sum(
                far_exp, axis=-1, keepdims=True
            )
            mixed = jnp.dot(
                near_exp.astype(bf16),
                values[pl.ds(starts[r], near_keys), :],
                preferred_element_type=f32,
            ) + jnp.dot(far_exp.astype(bf16), far_values[...], preferred_element_type=f32)
            mixed = mixed * (1.0 / total)
            result = jnp.where(masks[0], mixed[:GRID_W], 0.0)
            for h in range(1, heads):
                result = jnp.where(masks[h], mixed[h * GRID_W : (h + 1) * GRID_W], result)
            out_ref[r, 0] = result.astype(bf16)

    def of_sample(array):
        return pl.BlockSpec((1, *array.shape[1:]), lambda s, i: (s, 0, 0))

    far_spec = pl.BlockSpec((members, 1, ctx_rows, cols), lambda s, i: (0, s, 0, 0))
    return pl.pallas_call(
        body,
        grid=(samples, rows_dev // per),
        in_specs=[
            pl.BlockSpec(memory_space=pltpu.SMEM),
            pl.BlockSpec((1, per * GRID_W, cols), lambda s, i: (s, i, 0)),
            of_sample(before),
            of_sample(pair),
            of_sample(after),
        ]
        + [far_spec] * (groups + members)
        + [whole(table.shape), whole((queries, 1))],
        out_specs=pl.BlockSpec((per, 1, GRID_W, cols), lambda s, i: (i, s, 0, 0)),
        out_shape=jax.ShapeDtypeStruct((rows_dev, samples, GRID_W, cols), bf16),
        scratch_shapes=[
            pltpu.VMEM((2, cols, lanes), bf16),
            pltpu.VMEM((cols, ctx_count), bf16),
            pltpu.VMEM((padded, cols), bf16),
            pltpu.VMEM((ctx_count, cols), bf16),
        ],
        name="attend",
    )(place, query, before, pair, after, *ctx_keys, *ctx_values, table, ctx_bias)


def finish(attended, w_out, latent, modulation):
    groups, _, _ = attended.shape
    samples, tokens, width = latent.shape
    block = modulation.shape[2]
    first = modulation.shape[1] - samples

    def body(att_ref, w_ref, latent_ref, tile_ref, out_ref):
        everything = jnp.concatenate([att_ref[group] for group in range(groups)], axis=1)
        update = jnp.dot(everything, w_ref[...], preferred_element_type=jnp.float32)
        for s in range(samples):
            gate = tile_ref[0, first + s : first + s + 1, :]
            part = update[s * tokens : (s + 1) * tokens]
            out_ref[s] = (latent_ref[s].astype(jnp.float32) + gate * part).astype(jnp.bfloat16)

    return pl.pallas_call(
        body,
        grid=(width // block,),
        in_specs=[
            whole(attended.shape),
            pl.BlockSpec((width, block), lambda i: (0, i)),
            pl.BlockSpec((samples, tokens, block), lambda i: (0, 0, i)),
            pl.BlockSpec((1, *modulation.shape[1:]), lambda i: (i, 0, 0)),
        ],
        out_specs=pl.BlockSpec((samples, tokens, block), lambda i: (0, 0, i)),
        out_shape=jax.ShapeDtypeStruct(latent.shape, latent.dtype),
        name="finish",
    )(attended, w_out, latent, modulation)


def shifted(size, side, stride, value):
    span = side * stride
    return [(i, i // span * span + (i + value * stride) % span) for i in range(size)]


def from_line(block, axis, side, stride):
    size = lax.axis_size(axis)
    return [block] + [
        lax.ppermute(block, axis, shifted(size, side, stride, value)) for value in range(1, side)
    ]


def computation(
    latent,
    context,
    cond,
    ctx_cond,
    w_shift,
    w_scale,
    w_gate,
    norm_gain,
    w_query,
    w_key,
    w_value,
    w_out,
    rel_bias,
    ctx_bias,
):
    samples, tokens_dev, width = latent.shape
    local_cols = w_shift.shape[1]
    sp_index = lax.axis_index("sp")
    sp_size, tp_size = lax.axis_size("sp"), lax.axis_size("tp")
    place = jnp.full((1,), sp_index, jnp.int32)
    gathered = lax.all_gather(latent, "tp", axis=1, tiled=True)
    parts = modulation_parts(place, cond, ctx_cond[None], (w_shift, w_scale, w_gate), sp_size)
    parts, w_out_own = lax.optimization_barrier((parts, w_out))
    w_out_all = lax.all_gather(w_out_own, "tp", axis=0, tiled=True)
    table = bias_table(rel_bias)
    cb = jnp.repeat(ctx_bias, GRID_W)[:, None]
    summed = jnp.sum(lax.all_to_all(parts, "sp", 0, 0, tiled=True), axis=0)
    summed, table, cb = lax.optimization_barrier((summed, table, cb))
    modulation = copy_for_each(summed, "tp")

    gain = norm_gain[None, :]
    ctx_rows = context.shape[1]
    ctx_keys, ctx_values = project(
        context.reshape(1, samples * ctx_rows, width),
        gain,
        modulation,
        (w_key, w_value),
        samples,
        samples * ctx_rows,
        None,
    )
    ctx_keys = ctx_keys.reshape(samples, ctx_rows, local_cols)
    ctx_values = ctx_values.reshape(samples, ctx_rows, local_cols)
    ctx_keys = jnp.stack(from_line(ctx_keys, "sp", 4, 1))
    ctx_values = jnp.stack(from_line(ctx_values, "sp", 4, 4))
    gathered, ctx_keys, ctx_values = lax.optimization_barrier((gathered, ctx_keys, ctx_values))
    ctx_keys = from_line(ctx_keys, "sp", 4, 4)
    ctx_values = from_line(ctx_values, "sp", 4, 1)
    up = [(i, i + 1) for i in range(sp_size - 1)]
    down = [(j, i) for i, j in up]
    pair, query, first, last = project(
        gathered,
        gain,
        modulation,
        (w_key, w_value, w_query),
        0,
        256,
        ((WIN_ROWS - REACH - 1) * GRID_W, REACH * GRID_W),
    )
    before = lax.ppermute(last, "sp", up)
    after = lax.ppermute(first, "sp", down)
    rows_all = pair.shape[1] // GRID_W * sp_size
    attended = attend(
        place, query, before, pair, after, ctx_keys, ctx_values, table, cb, rows_all, 2
    )
    attended = attended.reshape(tp_size, samples * tokens_dev, local_cols)
    attended = lax.all_to_all(attended, "tp", 0, 0, tiled=True)
    return finish(attended, w_out_all, latent, modulation)


def solution(mesh):
    return jax.shard_map(
        computation,
        mesh=mesh,
        in_specs=(
            P(None, ("sp", "tp"), None),
            P(None, "sp", None),
            P(),
            P(),
            P("sp", "tp"),
            P("sp", "tp"),
            P("sp", "tp"),
            P(),
            P(None, "tp"),
            P(None, "tp"),
            P(None, "tp"),
            P("tp", None),
            P("tp", None, None),
            P("tp"),
        ),
        out_specs=P(None, ("sp", "tp"), None),
        check_vma=False,
    )
```

time: 144 us -> 142 us (0.986)
  the two profiles are of different devices: /device:TPU:32 before, /device:TPU:1 now
where the time goes in v3:
time: 142 us; the launch traced here: 141 us
  Pallas kernels  41.8 us (29%)
  starting transfers between devices  29.7 us (21%)
  blocking collectives  26 us (18%)
  waiting for transfers between devices  23.8 us (17%)
  between operations  13.6 us (10%)
  local copies, waits for them, and re-layouts  4.58 us (3%)
  other arithmetic  1.77 us (1%)
    ppermute x12, waiting for transfers between devices, from_line(): lax.ppermute(block, axis, shifted(size, side, stride, value))  20.7 us
    ppermute x12, starting transfers between devices, from_line(): lax.ppermute(block, axis, shifted(size, side, stride, value))  18.1 us
    pallas_call x1, Pallas kernels, attend(): pl.pallas_call(body, grid=(samples, rows_dev // per), in_specs=[pl.BlockS...  17.1 us
    all_to_all x1, blocking collectives, computation(): attended = lax.all_to_all(attended, 'tp', 0, 0, tiled=True)  14 us
    all_to_all x1, blocking collectives, copy_for_each(): lax.all_to_all(jnp.broadcast_to(shard[None], (length, *shard.shape)), axi...  12 us
    pallas_call x2, Pallas kernels, project(): pl.pallas_call(body, grid=(samples, steps), in_specs=[blocks(width), whol...  11.9 us
    all_to_all x1, starting transfers between devices, computation(): summed = jnp.sum(lax.all_to_all(parts, 'sp', 0, 0, tiled=True), axis=0)  8.43 us
    pallas_call x1, Pallas kernels, finish(): pl.pallas_call(body, grid=(width // block,), in_specs=[whole(attended.sha...  8.03 us
  transfers between devices with their start and end apart: 17, of which 6 were waited for; matrix products, arithmetic and copies ran while one was open for 4% of the time, Pallas kernels for 24%

profile of v3, /device:TPU:1, one launch (start us, length us, event | category | flops | bytes accessed | tf_op | source)
XLA Modules:
  0.0 141.1 jit_solution(5776920279049326010)
XLA Ops:
  6.5 0.7 all-gather.3.cloned.1.call-update
  7.3 0.0 all-gather.5.cloned.1.call-start
  7.3 1.3 broadcast_in_dim.20.ctx_ref
  8.6 1.7 %modulation_parts.1 = f32[16,8,256]{2,1,0:T(8,128)} custom-call(s32[1]{0:T(128)} %bitcast.place_ref, bf16[2,2048]{1,0:T(2,128)(2,1)} %cond_ref.1, bf16[1,2048]{1,0:T(2,128)(2,1)} %broadcast_in_dim.20.ctx_ref, bf16[128,256]{1,0:T(8,128)(2,1)} %shift_ref.1, bf16[128,256]{1,0:T(8,128)(2,1)} %scale_ref.1, bf16[128,256]{1,0:T(8,128)(2,1)} %gate_ref.1), custom_call_target="tpu_custom_call" | custom-call | tf_op jit(solution)/shard_map/modulation_parts/pallas_call | solution.py:51
  10.3 0.0 all-gather.5.cloned.1.call-update
  10.4 8.4 %all-to-all-start = ((f32[16,8,256]{2,1,0:T(8,128)}), f32[16,8,256]{2,1,0:T(8,128)S(1)}, u32[]{:S(2)}, u32[]{:S(2)}) async-start(f32[16,8,256]{2,1,0:T(8,128)} %modulation_parts.1), calls=%async_computation | async-start | bytes 262144 | tf_op jit(solution)/shard_map/all_to_all | solution.py:368
  18.8 0.8 copy.18
  19.6 0.6 pad.4.clone
  20.2 3.0 %bias_table.1.refs_8_ = f32[2,256,896]{2,1,0:T(8,128)} custom-call(f32[64,128]{1,0:T(8,128)} %bitcast.17), custom_call_target="tpu_custom_call" | custom-call | tf_op jit(solution)/shard_map/bias_table/pallas_call | solution.py:173
  23.2 0.1 broadcast_in_dim.21
  23.3 0.1 broadcast_in_dim_reshape.3
  23.3 2.3 %all-to-all-done = f32[16,8,256]{2,1,0:T(8,128)S(1)} async-done(((f32[16,8,256]{2,1,0:T(8,128)}), f32[16,8,256]{2,1,0:T(8,128)S(1)}, u32[]{:S(2)}, u32[]{:S(2)}) %all-to-all-start) | async-done | bytes 131104 | tf_op jit(solution)/shard_map/all_to_all | solution.py:368
  25.7 12.0 %all_to_all.15.tiles_ref.tile_ref = f32[8,8,256]{2,1,0:T(8,128)} all-to-all(f32[8,8,256]{2,1,0:T(8,128)S(1)} %broadcast_in_dim.22), channel_id=1, replica_groups=mesh['sp'=16,'tp'=8] {'tp'}, dimensions={0} | all-to-all | bytes 131072 | tf_op jit(solution)/shard_map/all_to_all | solution.py:21
  37.7 3.0 %project.2 = (bf16[1,128,256]{2,1,0:T(8,128)(2,1)}, bf16[1,128,256]{2,1,0:T(8,128)(2,1)}) custom-call(bf16[1,128,2048]{2,1,0:T(8,128)(2,1)} %bitcast.16, f32[1,2048]{1,0:T(1,128)} %bitcast.32, f32[8,8,256]{2,1,0:T(8,128)} %all_to_all.15.tiles_ref.tile_ref, bf16[2048,256]{1,0:T(8,128)(2,1)} %refs_0_.3, bf16[2048,256]{1,0:T(8,128)(2,1)} %refs_1_.3), custom_call_target="tpu_custom_call" | custom-call | tf_op jit(solution)/shard_map/project/pallas_call | solution.py:132
  40.8 0.0 collective-permute-start.3
  40.8 1.7 %collective-permute-start.4 = (bf16[2,64,256]{2,1,0:T(8,128)(2,1)}, bf16[2,64,256]{2,1,0:T(8,128)(2,1)S(1)}, u32[]{:S(2)}, u32[]{:S(2)}) collective-permute-start(bf16[2,64,256]{2,1,0:T(8,128)(2,1)} %bitcast.23), channel_id=1, source_target_pairs={{0,64},{8,72},{16,80},{24,88},{32,96},{40,104},{48,112},{56,120},{... | collective-permute-start | bytes 196616 | tf_op jit(solution)/shard_map/ppermute | solution.py:337
  42.5 1.0 collective-permute-start.5
  43.5 0.3 collective-permute-start
  43.8 2.3 %collective-permute-start.1 = (bf16[2,64,256]{2,1,0:T(8,128)(2,1)}, bf16[2,64,256]{2,1,0:T(8,128)(2,1)S(1)}, u32[]{:S(2)}, u32[]{:S(2)}) collective-permute-start(bf16[2,64,256]{2,1,0:T(8,128)(2,1)} %bitcast.19), channel_id=1, source_target_pairs={{0,16},{8,24},{16,0},{24,8},{32,48},{40,56},{48,32},{56,40},{64,80... | collective-permute-start | bytes 196616 | tf_op jit(solution)/shard_map/ppermute | solution.py:337
  46.1 0.0 collective-permute-done.3
  46.1 1.2 collective-permute-start.2
  47.3 0.9 pad_maximum_fusion.1.refs_4_
  48.2 0.5 collective-permute-done.1
  48.7 0.7 collective-permute-done.2
  49.4 0.9 pad_maximum_fusion.refs_0_
  50.3 0.0 all-gather.3.cloned.1.call-done.rows_ref
  50.4 0.8 collective-permute-start.10
  51.1 0.8 collective-permute-start.11
  51.9 2.5 %collective-permute-start.12 = (bf16[4,2,64,256]{3,2,1,0:T(8,128)(2,1)S(1)}, bf16[4,2,64,256]{3,2,1,0:T(8,128)(2,1)S(1)}, u32[]{:S(2)}, u32[]{:S(2)}) collective-permute-start(bf16[4,2,64,256]{3,2,1,0:T(8,128)(2,1)S(1)} %pad_maximum_fusion.1.refs_4_), channel_id=1, source_target_pairs={{0,16},{8,24},{16,0},{24,8},{32,48},{40,56},{48,32},{56,40},{64,80... | collective-permute-start | bytes 786440 | tf_op jit(solution)/shard_map/ppermute | solution.py:337
  54.4 8.9 %project.3 = (bf16[2,512,512]{2,1,0:T(8,128)(2,1)}, bf16[2,512,256]{2,1,0:T(8,128)(2,1)}, bf16[2,192,512]{2,1,0:T(8,128)(2,1)}, bf16[2,256,512]{2,1,0:T(8,128)(2,1)}) custom-call(bf16[2,512,2048]{2,1,0:T(8,128)(2,1)} %all-gather.3.cloned.1.call-done.rows_ref, f32[1,2048]{1,0:T(1,128)} %bitcast.33, f32[8,8,256]{2,1,0:T(8,128)} %all_to_all.15.tiles_ref.tile_ref, ...), custom_call_target="tpu_custom_call" | custom-call | tf_op jit(solution)/shard_map/project/pallas_call | solution.py:132
  63.3 1.8 %collective-permute-start.6 = (bf16[2,256,512]{2,1,0:T(8,128)(2,1)}, bf16[2,256,512]{2,1,0:T(8,128)(2,1)S(1)}, u32[]{:S(2)}, u32[]{:S(2)}) collective-permute-start(bf16[2,256,512]{2,1,0:T(8,128)(2,1)} %get-tuple-element.25), channel_id=1, source_target_pairs={{0,8},{8,16},{16,24},{24,32},{32,40},{40,48},{48,56},{56,64},{64,7... | collective-permute-start | bytes 1572872 | tf_op jit(solution)/shard_map/ppermute | solution.py:401
  65.1 1.3 collective-permute-start.7
  66.4 4.2 %collective-permute-start.13 = (bf16[4,2,64,256]{3,2,1,0:T(8,128)(2,1)S(1)}, bf16[4,2,64,256]{3,2,1,0:T(8,128)(2,1)S(1)}, u32[]{:S(2)}, u32[]{:S(2)}) collective-permute-start(bf16[4,2,64,256]{3,2,1,0:T(8,128)(2,1)S(1)} %pad_maximum_fusion.1.refs_4_), channel_id=1, source_target_pairs={{0,24},{8,0},{16,8},{24,16},{32,56},{40,32},{48,40},{56,48},{64,88... | collective-permute-start | bytes 786440 | tf_op jit(solution)/shard_map/ppermute | solution.py:337
  70.7 1.3 collective-permute-start.8
  71.9 0.0 collective-permute-done.12.refs_6_
  71.9 2.1 %collective-permute-start.9 = (bf16[4,2,64,256]{3,2,1,0:T(8,128)(2,1)S(1)}, bf16[4,2,64,256]{3,2,1,0:T(8,128)(2,1)S(1)}, u32[]{:S(2)}, u32[]{:S(2)}) collective-permute-start(bf16[4,2,64,256]{3,2,1,0:T(8,128)(2,1)S(1)} %pad_maximum_fusion.refs_0_), channel_id=1, source_target_pairs={{0,64},{8,72},{16,80},{24,88},{32,96},{40,104},{48,112},{56,120},{... | collective-permute-start | bytes 786440 | tf_op jit(solution)/shard_map/ppermute | solution.py:337
  74.0 0.8 copy.17.refs_9_
  74.8 4.6 %collective-permute-done.13.refs_7_ = bf16[4,2,64,256]{3,2,1,0:T(8,128)(2,1)S(1)} collective-permute-done((bf16[4,2,64,256]{3,2,1,0:T(8,128)(2,1)S(1)}, bf16[4,2,64,256]{3,2,1,0:T(8,128)(2,1)S(1)}, u32[]{:S(2)}, u32[]{:S(2)}) %collective-permute-start.13) | collective-permute-done | bytes 262176 | tf_op jit(solution)/shard_map/ppermute | solution.py:337
  79.4 6.4 %collective-permute-done.8.refs_1_ = bf16[4,2,64,256]{3,2,1,0:T(8,128)(2,1)S(1)} collective-permute-done((bf16[4,2,64,256]{3,2,1,0:T(8,128)(2,1)S(1)}, bf16[4,2,64,256]{3,2,1,0:T(8,128)(2,1)S(1)}, u32[]{:S(2)}, u32[]{:S(2)}) %collective-permute-start.8) | collective-permute-done | bytes 262176 | tf_op jit(solution)/shard_map/ppermute | solution.py:337
  85.8 8.4 %collective-permute-done.9.refs_2_ = bf16[4,2,64,256]{3,2,1,0:T(8,128)(2,1)S(1)} collective-permute-done((bf16[4,2,64,256]{3,2,1,0:T(8,128)(2,1)S(1)}, bf16[4,2,64,256]{3,2,1,0:T(8,128)(2,1)S(1)}, u32[]{:S(2)}, u32[]{:S(2)}) %collective-permute-start.9) | collective-permute-done | bytes 262176 | tf_op jit(solution)/shard_map/ppermute | solution.py:337
  94.2 0.0 collective-permute-done.7.after_ref
  94.2 0.0 collective-permute-done.6.before_ref
  94.3 0.6 copy-done.9
  94.9 0.2 copy-done.3
  95.1 0.1 copy-done.2
  95.2 17.1 %attend.1 = bf16[8,2,64,256]{3,2,1,0:T(8,128)(2,1)} custom-call(s32[1]{0:T(128)} %bitcast.place_ref, bf16[2,512,256]{2,1,0:T(8,128)(2,1)} %get-tuple-element.24.q_ref, bf16[2,256,512]{2,1,0:T(8,128)(2,1)} %copy-done.2, bf16[2,512,512]{2,1,0:T(8,128)(2,1)} %get-tuple-element.26.pair_ref, bf16[2,192,512]{2,1,0:T(8,128)(2,1)} %copy-done.3, ...), custom_call_target="tpu_custom_call" | custom-call | tf_op jit(solution)/shard_map/attend/pallas_call | solution.py:276
  112.3 14.0 %all_to_all.16.att_ref = bf16[8,128,256]{2,1,0:T(8,128)(2,1)} all-to-all(bf16[8,128,256]{2,1,0:T(8,128)(2,1)} %bitcast.15), channel_id=1, replica_groups=mesh['sp'=16,'tp'=8] {'tp'}, dimensions={0} | all-to-all | bytes 1048576 | tf_op jit(solution)/shard_map/all_to_all | solution.py:408
  126.3 8.0 %finish.1 = bf16[2,64,2048]{2,1,0:T(8,128)(2,1)} custom-call(bf16[8,128,256]{2,1,0:T(8,128)(2,1)} %all_to_all.16.att_ref, bf16[2048,2048]{1,0:T(8,128)(2,1)} %all-gather.5.cloned.1.call-done.w_ref, bf16[2,64,2048]{2,1,0:T(8,128)(2,1)} %latent_ref.1, f32[8,8,256]{2,1,0:T(8,128)} %all_to_all.15.tiles_ref.tile_ref), custom_call_target="tpu_custom_call" | custom-call | tf_op jit(solution)/shard_map/finish/pallas_call | solution.py:314
  (28 shorter events, 0.1 us)
Async XLA Ops:
  6.5 16.7 %copy-start.10 = (f32[4]{0:T(128)S(1)}, f32[4]{0:T(128)}, u32[]{:S(2)}) copy-start(f32[4]{0:T(128)} %param.27) | copy-start | bytes 52
  6.5 43.8 %all-gather.3.cloned.1.call-start = ((), (), s32[]{:S(2)}) async-start(), calls=%async_computation.3 | async-start | bytes 4718592 | tf_op jit(solution)/shard_map/all_gather | solution.py:362
  7.3 119.0 %all-gather.5.cloned.1.call-start = ((), (), s32[]{:S(2)}) async-start(), calls=%async_computation.4 | async-start | bytes 9437184 | tf_op jit(solution)/shard_map/all_gather | solution.py:365
  10.4 15.3 %all-to-all-start = ((f32[16,8,256]{2,1,0:T(8,128)}), f32[16,8,256]{2,1,0:T(8,128)S(1)}, u32[]{:S(2)}, u32[]{:S(2)}) async-start(f32[16,8,256]{2,1,0:T(8,128)} %modulation_parts.1), calls=%async_computation | async-start | bytes 262144 | tf_op jit(solution)/shard_map/all_to_all | solution.py:368
  40.8 5.3 %collective-permute-start.3 = (bf16[2,64,256]{2,1,0:T(8,128)(2,1)}, bf16[2,64,256]{2,1,0:T(8,128)(2,1)S(1)}, u32[]{:S(2)}, u32[]{:S(2)}) collective-permute-start(bf16[2,64,256]{2,1,0:T(8,128)(2,1)} %bitcast.22), channel_id=1, source_target_pairs={{0,32},{8,40},{16,48},{24,56},{32,64},{40,72},{48,80},{56,88},{64,... | collective-permute-start | bytes 196616 | tf_op jit(solution)/shard_map/ppermute | solution.py:337
  40.8 6.5 %collective-permute-start.4 = (bf16[2,64,256]{2,1,0:T(8,128)(2,1)}, bf16[2,64,256]{2,1,0:T(8,128)(2,1)S(1)}, u32[]{:S(2)}, u32[]{:S(2)}) collective-permute-start(bf16[2,64,256]{2,1,0:T(8,128)(2,1)} %bitcast.23), channel_id=1, source_target_pairs={{0,64},{8,72},{16,80},{24,88},{32,96},{40,104},{48,112},{56,120},{... | collective-permute-start | bytes 196616 | tf_op jit(solution)/shard_map/ppermute | solution.py:337
  42.5 4.9 %collective-permute-start.5 = (bf16[2,64,256]{2,1,0:T(8,128)(2,1)}, bf16[2,64,256]{2,1,0:T(8,128)(2,1)S(1)}, u32[]{:S(2)}, u32[]{:S(2)}) collective-permute-start(bf16[2,64,256]{2,1,0:T(8,128)(2,1)} %bitcast.24), channel_id=1, source_target_pairs={{0,96},{8,104},{16,112},{24,120},{32,0},{40,8},{48,16},{56,24},{64... | collective-permute-start | bytes 196616 | tf_op jit(solution)/shard_map/ppermute | solution.py:337
  43.5 4.7 %collective-permute-start = (bf16[2,64,256]{2,1,0:T(8,128)(2,1)}, bf16[2,64,256]{2,1,0:T(8,128)(2,1)S(1)}, u32[]{:S(2)}, u32[]{:S(2)}) collective-permute-start(bf16[2,64,256]{2,1,0:T(8,128)(2,1)} %bitcast.18), channel_id=1, source_target_pairs={{0,8},{8,16},{16,24},{24,0},{32,40},{40,48},{48,56},{56,32},{64,72... | collective-permute-start | bytes 196616 | tf_op jit(solution)/shard_map/ppermute | solution.py:337
  43.8 4.9 %collective-permute-start.1 = (bf16[2,64,256]{2,1,0:T(8,128)(2,1)}, bf16[2,64,256]{2,1,0:T(8,128)(2,1)S(1)}, u32[]{:S(2)}, u32[]{:S(2)}) collective-permute-start(bf16[2,64,256]{2,1,0:T(8,128)(2,1)} %bitcast.19), channel_id=1, source_target_pairs={{0,16},{8,24},{16,0},{24,8},{32,48},{40,56},{48,32},{56,40},{64,80... | collective-permute-start | bytes 196616 | tf_op jit(solution)/shard_map/ppermute | solution.py:337
  46.1 3.3 %collective-permute-start.2 = (bf16[2,64,256]{2,1,0:T(8,128)(2,1)}, bf16[2,64,256]{2,1,0:T(8,128)(2,1)S(1)}, u32[]{:S(2)}, u32[]{:S(2)}) collective-permute-start(bf16[2,64,256]{2,1,0:T(8,128)(2,1)} %bitcast.20), channel_id=1, source_target_pairs={{0,24},{8,0},{16,8},{24,16},{32,56},{40,32},{48,40},{56,48},{64,88... | collective-permute-start | bytes 196616 | tf_op jit(solution)/shard_map/ppermute | solution.py:337
  48.2 46.0 %copy-start = (bf16[4,2,64,256]{3,2,1,0:T(8,128)(2,1)}, bf16[4,2,64,256]{3,2,1,0:T(8,128)(2,1)S(1)}, u32[]{:S(2)}) copy-start(bf16[4,2,64,256]{3,2,1,0:T(8,128)(2,1)S(1)} %pad_maximum_fusion.1.refs_4_) | copy-start | bytes 786436
  50.3 43.9 %copy-start.1 = (bf16[4,2,64,256]{3,2,1,0:T(8,128)(2,1)}, bf16[4,2,64,256]{3,2,1,0:T(8,128)(2,1)S(1)}, u32[]{:S(2)}) copy-start(bf16[4,2,64,256]{3,2,1,0:T(8,128)(2,1)S(1)} %pad_maximum_fusion.refs_0_) | copy-start | bytes 786436
  50.4 16.0 %collective-permute-start.10 = (bf16[4,2,64,256]{3,2,1,0:T(8,128)(2,1)S(1)}, bf16[4,2,64,256]{3,2,1,0:T(8,128)(2,1)S(1)}, u32[]{:S(2)}, u32[]{:S(2)}) collective-permute-start(bf16[4,2,64,256]{3,2,1,0:T(8,128)(2,1)S(1)} %pad_maximum_fusion.refs_0_), channel_id=1, source_target_pairs={{0,96},{8,104},{16,112},{24,120},{32,0},{40,8},{48,16},{56,24},{64... | collective-permute-start | bytes 786440 | tf_op jit(solution)/shard_map/ppermute | solution.py:337
  51.1 19.5 %collective-permute-start.11 = (bf16[4,2,64,256]{3,2,1,0:T(8,128)(2,1)S(1)}, bf16[4,2,64,256]{3,2,1,0:T(8,128)(2,1)S(1)}, u32[]{:S(2)}, u32[]{:S(2)}) collective-permute-start(bf16[4,2,64,256]{3,2,1,0:T(8,128)(2,1)S(1)} %pad_maximum_fusion.1.refs_4_), channel_id=1, source_target_pairs={{0,8},{8,16},{16,24},{24,0},{32,40},{40,48},{48,56},{56,32},{64,72... | collective-permute-start | bytes 786440 | tf_op jit(solution)/shard_map/ppermute | solution.py:337
  51.9 20.0 %collective-permute-start.12 = (bf16[4,2,64,256]{3,2,1,0:T(8,128)(2,1)S(1)}, bf16[4,2,64,256]{3,2,1,0:T(8,128)(2,1)S(1)}, u32[]{:S(2)}, u32[]{:S(2)}) collective-permute-start(bf16[4,2,64,256]{3,2,1,0:T(8,128)(2,1)S(1)} %pad_maximum_fusion.1.refs_4_), channel_id=1, source_target_pairs={{0,16},{8,24},{16,0},{24,8},{32,48},{40,56},{48,32},{56,40},{64,80... | collective-permute-start | bytes 786440 | tf_op jit(solution)/shard_map/ppermute | solution.py:337
  63.3 30.9 %collective-permute-start.6 = (bf16[2,256,512]{2,1,0:T(8,128)(2,1)}, bf16[2,256,512]{2,1,0:T(8,128)(2,1)S(1)}, u32[]{:S(2)}, u32[]{:S(2)}) collective-permute-start(bf16[2,256,512]{2,1,0:T(8,128)(2,1)} %get-tuple-element.25), channel_id=1, source_target_pairs={{0,8},{8,16},{16,24},{24,32},{32,40},{40,48},{48,56},{56,64},{64,7... | collective-permute-start | bytes 1572872 | tf_op jit(solution)/shard_map/ppermute | solution.py:401
  65.1 29.1 %collective-permute-start.7 = (bf16[2,192,512]{2,1,0:T(8,128)(2,1)}, bf16[2,192,512]{2,1,0:T(8,128)(2,1)S(1)}, u32[]{:S(2)}, u32[]{:S(2)}) collective-permute-start(bf16[2,192,512]{2,1,0:T(8,128)(2,1)} %get-tuple-element.27), channel_id=1, source_target_pairs={{8,0},{16,8},{24,16},{32,24},{40,32},{48,40},{56,48},{64,56},{72,6... | collective-permute-start | bytes 1179656 | tf_op jit(solution)/shard_map/ppermute | solution.py:402
  66.4 27.8 %copy-start.4 = (bf16[4,2,64,256]{3,2,1,0:T(8,128)(2,1)}, bf16[4,2,64,256]{3,2,1,0:T(8,128)(2,1)S(1)}, u32[]{:S(2)}) copy-start(bf16[4,2,64,256]{3,2,1,0:T(8,128)(2,1)S(1)} %collective-permute-done.10.refs_3_) | copy-start | bytes 786436
  66.4 13.0 %collective-permute-start.13 = (bf16[4,2,64,256]{3,2,1,0:T(8,128)(2,1)S(1)}, bf16[4,2,64,256]{3,2,1,0:T(8,128)(2,1)S(1)}, u32[]{:S(2)}, u32[]{:S(2)}) collective-permute-start(bf16[4,2,64,256]{3,2,1,0:T(8,128)(2,1)S(1)} %pad_maximum_fusion.1.refs_4_), channel_id=1, source_target_pairs={{0,24},{8,0},{16,8},{24,16},{32,56},{40,32},{48,40},{56,48},{64,88... | collective-permute-start | bytes 786440 | tf_op jit(solution)/shard_map/ppermute | solution.py:337
  70.6 23.6 %copy-start.5 = (bf16[4,2,64,256]{3,2,1,0:T(8,128)(2,1)}, bf16[4,2,64,256]{3,2,1,0:T(8,128)(2,1)S(1)}, u32[]{:S(2)}) copy-start(bf16[4,2,64,256]{3,2,1,0:T(8,128)(2,1)S(1)} %collective-permute-done.11.refs_5_) | copy-start | bytes 786436
  70.7 15.1 %collective-permute-start.8 = (bf16[4,2,64,256]{3,2,1,0:T(8,128)(2,1)S(1)}, bf16[4,2,64,256]{3,2,1,0:T(8,128)(2,1)S(1)}, u32[]{:S(2)}, u32[]{:S(2)}) collective-permute-start(bf16[4,2,64,256]{3,2,1,0:T(8,128)(2,1)S(1)} %pad_maximum_fusion.refs_0_), channel_id=1, source_target_pairs={{0,32},{8,40},{16,48},{24,56},{32,64},{40,72},{48,80},{56,88},{64,... | collective-permute-start | bytes 786440 | tf_op jit(solution)/shard_map/ppermute | solution.py:337
  71.9 22.3 %copy-start.6 = (bf16[4,2,64,256]{3,2,1,0:T(8,128)(2,1)}, bf16[4,2,64,256]{3,2,1,0:T(8,128)(2,1)S(1)}, u32[]{:S(2)}) copy-start(bf16[4,2,64,256]{3,2,1,0:T(8,128)(2,1)S(1)} %collective-permute-done.12.refs_6_) | copy-start | bytes 786436
  71.9 22.3 %collective-permute-start.9 = (bf16[4,2,64,256]{3,2,1,0:T(8,128)(2,1)S(1)}, bf16[4,2,64,256]{3,2,1,0:T(8,128)(2,1)S(1)}, u32[]{:S(2)}, u32[]{:S(2)}) collective-permute-start(bf16[4,2,64,256]{3,2,1,0:T(8,128)(2,1)S(1)} %pad_maximum_fusion.refs_0_), channel_id=1, source_target_pairs={{0,64},{8,72},{16,80},{24,88},{32,96},{40,104},{48,112},{56,120},{... | collective-permute-start | bytes 786440 | tf_op jit(solution)/shard_map/ppermute | solution.py:337
  79.4 14.9 %copy-start.7 = (bf16[4,2,64,256]{3,2,1,0:T(8,128)(2,1)}, bf16[4,2,64,256]{3,2,1,0:T(8,128)(2,1)S(1)}, u32[]{:S(2)}) copy-start(bf16[4,2,64,256]{3,2,1,0:T(8,128)(2,1)S(1)} %collective-permute-done.13.refs_7_) | copy-start | bytes 786436
  85.8 8.5 %copy-start.8 = (bf16[4,2,64,256]{3,2,1,0:T(8,128)(2,1)}, bf16[4,2,64,256]{3,2,1,0:T(8,128)(2,1)S(1)}, u32[]{:S(2)}) copy-start(bf16[4,2,64,256]{3,2,1,0:T(8,128)(2,1)S(1)} %collective-permute-done.8.refs_1_) | copy-start | bytes 786436
  94.2 0.7 copy-start.9
  94.2 0.9 copy-start.3
  94.2 1.0 copy-start.2
Sparse Core Ops, SparseCore 0:
  9.0 36.3 all-gather.2
  47.1 49.6 all-gather.4

commit v4 on v3

--- a/solution.py
+++ b/solution.py
@@ -4,7 +4,6 @@
 from jax.experimental import pallas as pl
 from jax.experimental.pallas import tpu as pltpu
 from jax.sharding import PartitionSpec as P
-
 
 HEAD_DIM = 64
 GRID_W = 64
@@ -65,7 +64,7 @@
     return jnp.concatenate([tiles[tile, row : row + 1, :] for tile in range(tiles.shape[0])], axis=1)
 
 
-def project(rows, gain, modulation, weights, row_of, block, ends):
+def project(rows, gain, modulation, weights, row_of, block, ends, copies=0, copy_samples=1):
     samples, count, width = rows.shape
     every = modulation.shape[1] // 3 + 1
     cols = weights[0].shape[1]
@@ -93,8 +92,12 @@
             for ref in weight_refs[:2]
         ]
         if not ends:
-            out_refs[0][0] = pair[0]
-            out_refs[1][0] = pair[1]
+            for copy in range(copies):
+                for number in range(copy_samples):
+                    size = block // copy_samples
+                    low = number * size
+                    out_refs[0][copy, number, :, :cols] = pair[0][low : low + size]
+                    out_refs[0][copy, number, :, cols:] = pair[1][low : low + size]
             return
         out_refs[0][0, :, :cols] = pair[0]
         out_refs[0][0, :, cols:] = pair[1]
@@ -127,8 +130,8 @@
             out_specs += [pl.BlockSpec((1, length, 2 * cols), lambda s, i: (s, 0, 0))]
             out_shape += [(samples, length, 2 * cols)]
     else:
-        out_specs = [blocks(cols)] * 2
-        out_shape = [(samples, count, cols)] * 2
+        out_shape = [(copies, copy_samples, count // copy_samples, 2 * cols)]
+        out_specs = [whole(out_shape[0])]
     return pl.pallas_call(
         body,
         grid=(samples, steps),
@@ -177,22 +180,43 @@
     )(padded)
 
 
-def attend(place, query, before, pair, after, ctx_keys, ctx_values, table, ctx_bias, rows_all, per):
+def head_masks(cols):
+    lane = lax.broadcasted_iota(jnp.int32, (GRID_W, cols), 1)
+    return [(lane >= low) & (lane < low + HEAD_DIM) for low in range(0, cols, HEAD_DIM)]
+
+
+def spread_heads(query, masks):
+    return jnp.concatenate(
+        [jnp.where(mask, query, jnp.zeros_like(query)) for mask in masks], axis=0
+    )
+
+
+def gather_heads(values, masks):
+    result = jnp.where(masks[0], values[:GRID_W], 0.0)
+    for h in range(1, len(masks)):
+        result = jnp.where(masks[h], values[h * GRID_W : (h + 1) * GRID_W], result)
+    return result
+
+
+def weighed(scores, values, masks):
+    top = jnp.max(scores, axis=-1, keepdims=True)
+    exps = jnp.exp(scores - top)
+    total = jnp.sum(exps, axis=-1, keepdims=True)
+    mixed = jnp.dot(exps.astype(jnp.bfloat16), values, preferred_element_type=jnp.float32)
+    return [gather_heads(array, masks) for array in (mixed, top, total)]
+
+
+def attend_near(place, query, before, pair, after, table, rows_all, per):
     samples, tokens, cols = query.shape
-    heads = cols // HEAD_DIM
     rows_dev = tokens // GRID_W
     near_keys = WIN_ROWS * GRID_W
     ahead, behind = before.shape[1], after.shape[1]
     padded = ahead + tokens + behind
     lanes = -(-padded // 128) * 128
-    groups, members, _, ctx_rows, _ = (len(ctx_keys), *ctx_keys[0].shape)
-    ctx_count = groups * members * ctx_rows
-    queries = heads * GRID_W
     bf16, f32 = jnp.bfloat16, jnp.float32
 
-    def body(place_ref, q_ref, before_ref, pair_ref, after_ref, *refs):
-        key_refs, value_refs = refs[:groups], refs[groups : groups + members]
-        table_ref, cb_ref, out_ref, near_t, far_t, values, far_values = refs[groups + members :]
+    def body(place_ref, q_ref, before_ref, pair_ref, after_ref, table_ref, *refs):
+        out_refs, (near_t, values) = refs[:3], refs[3:]
         step = pl.program_id(1)
 
         @pl.when(step == 0)
@@ -200,13 +224,6 @@
             values[0:ahead] = before_ref[0, :, cols:]
             values[ahead : ahead + tokens] = pair_ref[0, :, cols:]
             values[ahead + tokens : padded] = after_ref[0, :, cols:]
-            for group in range(groups):
-                block = jnp.concatenate([key_refs[group][m, 0] for m in range(members)], axis=0)
-                size = members * ctx_rows
-                far_t[:, group * size : (group + 1) * size] = block.T
-                for member in range(members):
-                    at = (group * members + member) * ctx_rows
-                    far_values[at : at + ctx_rows] = value_refs[member][group, 0]
             fill = jnp.zeros((lanes - padded, cols), bf16)
             near_t[0, :, :ahead] = before_ref[0, :, :cols].T
             near_t[0, :, ahead : ahead + tokens] = pair_ref[0, :, :cols].T
@@ -225,80 +242,113 @@
             ).T
 
         base = place_ref[0] * rows_dev
-        lane = lax.broadcasted_iota(jnp.int32, (GRID_W, cols), 1)
-        masks = [(lane >= h * HEAD_DIM) & (lane < (h + 1) * HEAD_DIM) for h in range(heads)]
-        cb = cb_ref[...]
-        spreads, nears, starts = [], [], []
+        masks = head_masks(cols)
+        scores, starts = [], []
         for r in range(per):
             actual = base + step * per + r
             start = jnp.clip(actual - REACH, 0, rows_all - WIN_ROWS)
             local = start - base + REACH
             offset = start - actual + WIN_ROWS - 1
-            q = q_ref[0, r * GRID_W : (r + 1) * GRID_W]
-            spread = jnp.concatenate(
-                [jnp.where(mask, q, jnp.zeros_like(q)) for mask in masks], axis=0
-            )
-            spreads.append(spread)
+            spread = spread_heads(q_ref[0, r * GRID_W : (r + 1) * GRID_W], masks)
             column = pl.multiple_of((local // 2) * 128, 128)
             keys_t = near_t[local % 2, :, pl.ds(column, near_keys)]
             bias_at = pl.multiple_of((offset // 2) * 128, 128)
-            nears.append(
+            scores.append(
                 jnp.dot(spread, keys_t, preferred_element_type=f32)
                 + table_ref[offset % 2, :, pl.ds(bias_at, near_keys)]
             )
             starts.append(pl.multiple_of(local * GRID_W, GRID_W))
         for r in range(per):
-            near = nears[r]
-            far = jnp.dot(spreads[r], far_t[...], preferred_element_type=f32)
-            top = jnp.maximum(
-                jnp.max(near, axis=-1, keepdims=True), jnp.max(far, axis=-1, keepdims=True) + cb
-            )
-            near_exp = jnp.exp(near - top)
-            far_exp = jnp.exp(far - (top - cb))
-            total = jnp.sum(near_exp, axis=-1, keepdims=True) + jnp.sum(
-                far_exp, axis=-1, keepdims=True
-            )
-            mixed = jnp.dot(
-                near_exp.astype(bf16),
-                values[pl.ds(starts[r], near_keys), :],
-                preferred_element_type=f32,
-            ) + jnp.dot(far_exp.astype(bf16), far_values[...], preferred_element_type=f32)
-            mixed = mixed * (1.0 / total)
-            result = jnp.where(masks[0], mixed[:GRID_W], 0.0)
-            for h in range(1, heads):
-                result = jnp.where(masks[h], mixed[h * GRID_W : (h + 1) * GRID_W], result)
-            out_ref[r, 0] = result.astype(bf16)
+            parts = weighed(scores[r], values[pl.ds(starts[r], near_keys), :], masks)
+            for out_ref, part in zip(out_refs, parts):
+                out_ref[0, r * GRID_W : (r + 1) * GRID_W] = part
 
     def of_sample(array):
         return pl.BlockSpec((1, *array.shape[1:]), lambda s, i: (s, 0, 0))
 
-    far_spec = pl.BlockSpec((members, 1, ctx_rows, cols), lambda s, i: (0, s, 0, 0))
+    rows_spec = pl.BlockSpec((1, per * GRID_W, cols), lambda s, i: (s, i, 0))
     return pl.pallas_call(
         body,
         grid=(samples, rows_dev // per),
         in_specs=[
             pl.BlockSpec(memory_space=pltpu.SMEM),
-            pl.BlockSpec((1, per * GRID_W, cols), lambda s, i: (s, i, 0)),
+            rows_spec,
             of_sample(before),
             of_sample(pair),
             of_sample(after),
+            whole(table.shape),
+        ],
+        out_specs=[rows_spec] * 3,
+        out_shape=[jax.ShapeDtypeStruct((samples, tokens, cols), f32)] * 3,
+        scratch_shapes=[
+            pltpu.VMEM((2, cols, lanes), bf16),
+            pltpu.VMEM((padded, cols), bf16),
+        ],
+        name="attend_near",
+    )(place, query, before, pair, after, table)
+
+
+def attend_far(query, ctx_pair, ctx_bias, near, per):
+    samples, tokens, cols = query.shape
+    rows_dev = tokens // GRID_W
+    owners, _, ctx_rows, _ = ctx_pair.shape
+    ctx_count = owners * ctx_rows
+    bf16, f32 = jnp.bfloat16, jnp.float32
+
+    def body(q_ref, ctx_ref, cb_ref, mixed_ref, top_ref, total_ref, out_ref, far_t, values):
+        @pl.when(pl.program_id(1) == 0)
+        def _():
+            for owner in range(owners):
+                values[owner * ctx_rows : (owner + 1) * ctx_rows] = ctx_ref[owner, 0, :, cols:]
+            for first in range(0, owners, 2):
+                block = jnp.concatenate(
+                    [ctx_ref[first, 0, :, :cols], ctx_ref[first + 1, 0, :, :cols]], axis=0
+                )
+                far_t[:, first * ctx_rows : (first + 2) * ctx_rows] = block.T
+
+        masks = head_masks(cols)
+        scores = [
+            jnp.dot(
+                spread_heads(q_ref[0, r * GRID_W : (r + 1) * GRID_W], masks),
+                far_t[...],
+                preferred_element_type=f32,
+            )
+            for r in range(per)
         ]
-        + [far_spec] * (groups + members)
-        + [whole(table.shape), whole((queries, 1))],
+        for r in range(per):
+            mixed, top, total = weighed(scores[r], values[...], masks)
+            at = slice(r * GRID_W, (r + 1) * GRID_W)
+            top = top + cb_ref[...]
+            near_top = top_ref[0, at]
+            highest = jnp.maximum(top, near_top)
+            far_part = jnp.exp(top - highest)
+            near_part = jnp.exp(near_top - highest)
+            total = total * far_part + total_ref[0, at] * near_part
+            mixed = mixed * far_part + mixed_ref[0, at] * near_part
+            out_ref[r, 0] = (mixed / total).astype(bf16)
+
+    rows_spec = pl.BlockSpec((1, per * GRID_W, cols), lambda s, i: (s, i, 0))
+    return pl.pallas_call(
+        body,
+        grid=(samples, rows_dev // per),
+        in_specs=[
+            rows_spec,
+            pl.BlockSpec((owners, 1, ctx_rows, 2 * cols), lambda s, i: (0, s, 0, 0)),
+            whole(ctx_bias.shape),
+        ]
+        + [rows_spec] * 3,
         out_specs=pl.BlockSpec((per, 1, GRID_W, cols), lambda s, i: (i, s, 0, 0)),
         out_shape=jax.ShapeDtypeStruct((rows_dev, samples, GRID_W, cols), bf16),
         scratch_shapes=[
-            pltpu.VMEM((2, cols, lanes), bf16),
             pltpu.VMEM((cols, ctx_count), bf16),
-            pltpu.VMEM((padded, cols), bf16),
             pltpu.VMEM((ctx_count, cols), bf16),
         ],
-        name="attend",
-    )(place, query, before, pair, after, *ctx_keys, *ctx_values, table, ctx_bias)
+        name="attend_far",
+    )(query, ctx_pair, ctx_bias, *near)
 
 
 def finish(attended, w_out, latent, modulation):
-    groups, _, _ = attended.shape
+    groups, rows, cols = attended.shape
     samples, tokens, width = latent.shape
     block = modulation.shape[2]
     first = modulation.shape[1] - samples
@@ -326,19 +376,7 @@
     )(attended, w_out, latent, modulation)
 
 
-def shifted(size, side, stride, value):
-    span = side * stride
-    return [(i, i // span * span + (i + value * stride) % span) for i in range(size)]
-
-
-def from_line(block, axis, side, stride):
-    size = lax.axis_size(axis)
-    return [block] + [
-        lax.ppermute(block, axis, shifted(size, side, stride, value)) for value in range(1, side)
-    ]
-
-
-def computation(
+def on_device(
     latent,
     context,
     cond,
@@ -364,14 +402,14 @@
     parts, w_out_own = lax.optimization_barrier((parts, w_out))
     w_out_all = lax.all_gather(w_out_own, "tp", axis=0, tiled=True)
     table = bias_table(rel_bias)
-    cb = jnp.repeat(ctx_bias, GRID_W)[:, None]
+    cb = jnp.repeat(ctx_bias, HEAD_DIM)[None, :]
     summed = jnp.sum(lax.all_to_all(parts, "sp", 0, 0, tiled=True), axis=0)
     summed, table, cb = lax.optimization_barrier((summed, table, cb))
     modulation = copy_for_each(summed, "tp")
 
     gain = norm_gain[None, :]
     ctx_rows = context.shape[1]
-    ctx_keys, ctx_values = project(
+    (ctx_pair,) = project(
         context.reshape(1, samples * ctx_rows, width),
         gain,
         modulation,
@@ -379,14 +417,10 @@
         samples,
         samples * ctx_rows,
         None,
+        sp_size,
+        samples,
     )
-    ctx_keys = ctx_keys.reshape(samples, ctx_rows, local_cols)
-    ctx_values = ctx_values.reshape(samples, ctx_rows, local_cols)
-    ctx_keys = jnp.stack(from_line(ctx_keys, "sp", 4, 1))
-    ctx_values = jnp.stack(from_line(ctx_values, "sp", 4, 4))
-    gathered, ctx_keys, ctx_values = lax.optimization_barrier((gathered, ctx_keys, ctx_values))
-    ctx_keys = from_line(ctx_keys, "sp", 4, 4)
-    ctx_values = from_line(ctx_values, "sp", 4, 1)
+    ctx_pair = lax.all_to_all(ctx_pair, "sp", 0, 0, tiled=True)
     up = [(i, i + 1) for i in range(sp_size - 1)]
     down = [(j, i) for i, j in up]
     pair, query, first, last = project(
@@ -401,9 +435,8 @@
     before = lax.ppermute(last, "sp", up)
     after = lax.ppermute(first, "sp", down)
     rows_all = pair.shape[1] // GRID_W * sp_size
-    attended = attend(
-        place, query, before, pair, after, ctx_keys, ctx_values, table, cb, rows_all, 2
-    )
+    near = attend_near(place, query, before, pair, after, table, rows_all, 2)
+    attended = attend_far(query, ctx_pair, cb, near, 2)
     attended = attended.reshape(tp_size, samples * tokens_dev, local_cols)
     attended = lax.all_to_all(attended, "tp", 0, 0, tiled=True)
     return finish(attended, w_out_all, latent, modulation)
@@ -411,7 +444,7 @@
 
 def solution(mesh):
     return jax.shard_map(
-        computation,
+        on_device,
         mesh=mesh,
         in_specs=(
             P(None, ("sp", "tp"), None),

time: 142 us -> 139 us (0.979)
  the two profiles are of different devices: /device:TPU:1 before, /device:TPU:32 now
where the time goes in v4:
time: 139 us; the launch traced here: 137 us
  Pallas kernels  46.4 us (33%)
  waiting for transfers between devices  25.5 us (18%)
  blocking collectives  25.4 us (18%)
  starting transfers between devices  21.2 us (15%)
  between operations  13.5 us (10%)
  local copies, waits for them, and re-layouts  4.78 us (3%)
    ppermute x1, waiting for transfers between devices, on_device(): after = lax.ppermute(first, 'sp', down)  19.4 us
    all_to_all x1, blocking collectives, on_device(): attended = lax.all_to_all(attended, 'tp', 0, 0, tiled=True)  14.5 us
    pallas_call x2, Pallas kernels, project(): pl.pallas_call(body, grid=(samples, steps), in_specs=[blocks(width), whol...  12.5 us
    pallas_call x1, Pallas kernels, attend_far(): pl.pallas_call(body, grid=(samples, rows_dev // per), in_specs=[rows_spec...  11.3 us
    all_to_all x1, blocking collectives, copy_for_each(): lax.all_to_all(jnp.broadcast_to(shard[None], (length, *shard.shape)), axi...  10.9 us
    pallas_call x1, Pallas kernels, attend_near(): pl.pallas_call(body, grid=(samples, rows_dev // per), in_specs=[pl.BlockS...  9.73 us
    pallas_call x1, Pallas kernels, finish(): pl.pallas_call(body, grid=(width // block,), in_specs=[whole(attended.sha...  8.03 us
    all_to_all x1, starting transfers between devices, on_device(): summed = jnp.sum(lax.all_to_all(parts, 'sp', 0, 0, tiled=True), axis=0)  7.91 us
  transfers between devices with their start and end apart: 6, of which 3 were waited for; matrix products, arithmetic and copies ran while one was open for 2% of the time, Pallas kernels for 28%

profile of v4, /device:TPU:32, one launch (start us, length us, event | category | flops | bytes accessed | tf_op | source)
XLA Modules:
  0.0 136.7 jit_solution(12711510471894855064)
XLA Ops:
  6.5 0.0 copy-start.3
  6.5 0.0 copy-start.4
  6.5 0.0 all-gather.3.cloned.1.call-start
  6.5 0.7 all-gather.3.cloned.1.call-update
  7.3 0.0 all-gather.5.cloned.1.call-start
  7.3 1.3 broadcast_in_dim.20.ctx_ref
  8.6 1.7 %modulation_parts.1 = f32[16,8,256]{2,1,0:T(8,128)} custom-call(s32[1]{0:T(128)} %bitcast.1.place_ref, bf16[2,2048]{1,0:T(2,128)(2,1)} %cond_ref.1, bf16[1,2048]{1,0:T(2,128)(2,1)} %broadcast_in_dim.20.ctx_ref, bf16[128,256]{1,0:T(8,128)(2,1)} %shift_ref.1, bf16[128,256]{1,0:T(8,128)(2,1)} %scale_ref.1, bf16[128,256]{1,0:T(8,128)(2,1)} %gate_ref.1), custom_call_target="tpu_custom_call" | custom-call | tf_op jit(solution)/shard_map/modulation_parts/pallas_call | solution.py:50
  10.4 0.0 all-gather.5.cloned.1.call-update
  10.4 7.9 %all-to-all-start = ((f32[16,8,256]{2,1,0:T(8,128)}), f32[16,8,256]{2,1,0:T(8,128)S(1)}, u32[]{:S(2)}, u32[]{:S(2)}) async-start(f32[16,8,256]{2,1,0:T(8,128)} %modulation_parts.1), calls=%async_computation | async-start | bytes 262144 | tf_op jit(solution)/shard_map/all_to_all | solution.py:406
  18.3 0.0 copy-done.3
  18.3 0.6 pad.4.clone
  18.9 3.0 %bias_table.1.table_ref = f32[2,256,896]{2,1,0:T(8,128)} custom-call(f32[64,128]{1,0:T(8,128)} %bitcast.7), custom_call_target="tpu_custom_call" | custom-call | tf_op jit(solution)/shard_map/bias_table/pallas_call | solution.py:176
  21.9 0.0 copy-done.4
  22.0 0.1 broadcast_in_dim.21
  22.0 0.7 broadcast_in_dim_reshape.3.cb_ref
  22.7 1.9 %all-to-all-done = f32[16,8,256]{2,1,0:T(8,128)S(1)} async-done(((f32[16,8,256]{2,1,0:T(8,128)}), f32[16,8,256]{2,1,0:T(8,128)S(1)}, u32[]{:S(2)}, u32[]{:S(2)}) %all-to-all-start) | async-done | bytes 131104 | tf_op jit(solution)/shard_map/all_to_all | solution.py:406
  24.6 10.9 %all_to_all.20.tiles_ref.tile_ref = f32[8,8,256]{2,1,0:T(8,128)} all-to-all(f32[8,8,256]{2,1,0:T(8,128)S(1)} %broadcast_in_dim.22), channel_id=1, replica_groups=mesh['sp'=16,'tp'=8] {'tp'}, dimensions={0} | all-to-all | bytes 131072 | tf_op jit(solution)/shard_map/all_to_all | solution.py:20
  35.5 4.0 %project.3 = bf16[16,2,64,512]{3,2,1,0:T(8,128)(2,1)} custom-call(bf16[1,128,2048]{2,1,0:T(8,128)(2,1)} %bitcast.6, f32[1,2048]{1,0:T(1,128)} %bitcast.8, f32[8,8,256]{2,1,0:T(8,128)} %all_to_all.20.tiles_ref.tile_ref, bf16[2048,256]{1,0:T(8,128)(2,1)} %refs_0_.3, bf16[2048,256]{1,0:T(8,128)(2,1)} %refs_1_.3), custom_call_target="tpu_custom_call" | custom-call | tf_op jit(solution)/shard_map/project/pallas_call | solution.py:135
  39.5 5.3 %all-to-all-start.2 = ((bf16[16,2,64,512]{3,2,1,0:T(8,128)(2,1)}), bf16[16,2,64,512]{3,2,1,0:T(8,128)(2,1)S(1)}, u32[]{:S(2)}, u32[]{:S(2)}) async-start(bf16[16,2,64,512]{3,2,1,0:T(8,128)(2,1)} %project.3), calls=%async_computation.2 | async-start | bytes 4194304 | tf_op jit(solution)/shard_map/all_to_all | solution.py:423
  44.8 0.0 all-gather.3.cloned.1.call-done.rows_ref
  44.8 8.6 %project.2 = (bf16[2,512,512]{2,1,0:T(8,128)(2,1)}, bf16[2,512,256]{2,1,0:T(8,128)(2,1)}, bf16[2,192,512]{2,1,0:T(8,128)(2,1)}, bf16[2,256,512]{2,1,0:T(8,128)(2,1)}) custom-call(bf16[2,512,2048]{2,1,0:T(8,128)(2,1)} %all-gather.3.cloned.1.call-done.rows_ref, f32[1,2048]{1,0:T(1,128)} %bitcast.9, f32[8,8,256]{2,1,0:T(8,128)} %all_to_all.20.tiles_ref.tile_ref, ...), custom_call_target="tpu_custom_call" | custom-call | tf_op jit(solution)/shard_map/project/pallas_call | solution.py:135
  53.4 3.4 %collective-permute-start = (bf16[2,256,512]{2,1,0:T(8,128)(2,1)}, bf16[2,256,512]{2,1,0:T(8,128)(2,1)S(1)}, u32[]{:S(2)}, u32[]{:S(2)}) collective-permute-start(bf16[2,256,512]{2,1,0:T(8,128)(2,1)} %get-tuple-element.21), channel_id=1, source_target_pairs={{0,8},{8,16},{16,24},{24,32},{32,40},{40,48},{48,56},{56,64},{64,7... | collective-permute-start | bytes 1572872 | tf_op jit(solution)/shard_map/ppermute | solution.py:435
  56.7 4.6 %collective-permute-start.1 = (bf16[2,192,512]{2,1,0:T(8,128)(2,1)}, bf16[2,192,512]{2,1,0:T(8,128)(2,1)S(1)}, u32[]{:S(2)}, u32[]{:S(2)}) collective-permute-start(bf16[2,192,512]{2,1,0:T(8,128)(2,1)} %get-tuple-element.23), channel_id=1, source_target_pairs={{8,0},{16,8},{24,16},{32,24},{40,32},{48,40},{56,48},{64,56},{72,6... | collective-permute-start | bytes 1179656 | tf_op jit(solution)/shard_map/ppermute | solution.py:436
  61.3 19.4 %collective-permute-done.1.after_ref = bf16[2,192,512]{2,1,0:T(8,128)(2,1)S(1)} collective-permute-done((bf16[2,192,512]{2,1,0:T(8,128)(2,1)}, bf16[2,192,512]{2,1,0:T(8,128)(2,1)S(1)}, u32[]{:S(2)}, u32[]{:S(2)}) %collective-permute-start.1) | collective-permute-done | bytes 393248 | tf_op jit(solution)/shard_map/ppermute | solution.py:436
  80.7 0.0 copy-start.2
  80.7 3.5 %collective-permute-done.before_ref = bf16[2,256,512]{2,1,0:T(8,128)(2,1)S(1)} collective-permute-done((bf16[2,256,512]{2,1,0:T(8,128)(2,1)}, bf16[2,256,512]{2,1,0:T(8,128)(2,1)S(1)}, u32[]{:S(2)}, u32[]{:S(2)}) %collective-permute-start) | collective-permute-done | bytes 524320 | tf_op jit(solution)/shard_map/ppermute | solution.py:435
  84.2 0.0 copy-start.1
  84.2 0.0 copy-done.2
  84.2 0.8 copy-done.1
  85.0 9.7 %attend_near.1 = (f32[2,512,256]{2,1,0:T(8,128)}, f32[2,512,256]{2,1,0:T(8,128)}, f32[2,512,256]{2,1,0:T(8,128)}) custom-call(s32[1]{0:T(128)} %bitcast.1.place_ref, bf16[2,512,256]{2,1,0:T(8,128)(2,1)} %get-tuple-element.19.q_ref, bf16[2,256,512]{2,1,0:T(8,128)(2,1)} %copy-done.1, bf16[2,512,512]{2,1,0:T(8,128)(2,1)} %get-tuple-element.22.pair_ref, ...), custom_call_target="tpu_custom_call" | custom-call | tf_op jit(solution)/shard_map/attend_near/pallas_call | solution.py:270
  94.7 0.0 all-to-all-done.2.ctx_ref
  94.7 0.0 copy-start
  94.8 1.3 copy-done
  96.1 11.3 %attend_far.1 = bf16[8,2,64,256]{3,2,1,0:T(8,128)(2,1)} custom-call(bf16[2,512,256]{2,1,0:T(8,128)(2,1)} %get-tuple-element.19.q_ref, bf16[16,2,64,512]{3,2,1,0:T(8,128)(2,1)} %copy-done, f32[1,256]{1,0:T(1,128)} %broadcast_in_dim_reshape.3.cb_ref, f32[2,512,256]{2,1,0:T(8,128)} %get-tuple-element.25.mixed_ref, f32[2,512,256]{2,1,0:T(8,128)} %get-tuple-element.26.top_ref, ...), custom_call_target="tpu_custom_call" | custom-call | tf_op jit(solution)/shard_map/attend_far/pallas_call | solution.py:331
  107.4 14.5 %all_to_all.21.att_ref = bf16[8,128,256]{2,1,0:T(8,128)(2,1)} all-to-all(bf16[8,128,256]{2,1,0:T(8,128)(2,1)} %bitcast.5), channel_id=1, replica_groups=mesh['sp'=16,'tp'=8] {'tp'}, dimensions={0} | all-to-all | bytes 1048576 | tf_op jit(solution)/shard_map/all_to_all | solution.py:441
  121.9 0.0 all-gather.5.cloned.1.call-done.w_ref
  121.9 8.0 %finish.1 = bf16[2,64,2048]{2,1,0:T(8,128)(2,1)} custom-call(bf16[8,128,256]{2,1,0:T(8,128)(2,1)} %all_to_all.21.att_ref, bf16[2048,2048]{1,0:T(8,128)(2,1)} %all-gather.5.cloned.1.call-done.w_ref, bf16[2,64,2048]{2,1,0:T(8,128)(2,1)} %latent_ref.1, f32[8,8,256]{2,1,0:T(8,128)} %all_to_all.20.tiles_ref.tile_ref), custom_call_target="tpu_custom_call" | custom-call | tf_op jit(solution)/shard_map/finish/pallas_call | solution.py:364
  (3 shorter events, 0.0 us)
Async XLA Ops:
  6.5 11.8 %copy-start.3 = (f32[4,15,31]{2,0,1:T(4,128)S(1)}, f32[4,15,31]{2,0,1:T(4,128)}, u32[]{:S(2)}) copy-start(f32[4,15,31]{2,0,1:T(4,128)} %param.26) | copy-start | bytes 22324
  6.5 15.4 %copy-start.4 = (f32[4]{0:T(128)S(1)}, f32[4]{0:T(128)}, u32[]{:S(2)}) copy-start(f32[4]{0:T(128)} %param.27) | copy-start | bytes 52
  6.5 38.3 %all-gather.3.cloned.1.call-start = ((), (), s32[]{:S(2)}) async-start(), calls=%async_computation.4 | async-start | bytes 4718592 | tf_op jit(solution)/shard_map/all_gather | solution.py:400
  7.3 114.6 %all-gather.5.cloned.1.call-start = ((), (), s32[]{:S(2)}) async-start(), calls=%async_computation.5 | async-start | bytes 9437184 | tf_op jit(solution)/shard_map/all_gather | solution.py:403
  10.4 14.2 %all-to-all-start = ((f32[16,8,256]{2,1,0:T(8,128)}), f32[16,8,256]{2,1,0:T(8,128)S(1)}, u32[]{:S(2)}, u32[]{:S(2)}) async-start(f32[16,8,256]{2,1,0:T(8,128)} %modulation_parts.1), calls=%async_computation | async-start | bytes 262144 | tf_op jit(solution)/shard_map/all_to_all | solution.py:406
  39.5 55.2 %all-to-all-start.2 = ((bf16[16,2,64,512]{3,2,1,0:T(8,128)(2,1)}), bf16[16,2,64,512]{3,2,1,0:T(8,128)(2,1)S(1)}, u32[]{:S(2)}, u32[]{:S(2)}) async-start(bf16[16,2,64,512]{3,2,1,0:T(8,128)(2,1)} %project.3), calls=%async_computation.2 | async-start | bytes 4194304 | tf_op jit(solution)/shard_map/all_to_all | solution.py:423
  53.4 30.8 %collective-permute-start = (bf16[2,256,512]{2,1,0:T(8,128)(2,1)}, bf16[2,256,512]{2,1,0:T(8,128)(2,1)S(1)}, u32[]{:S(2)}, u32[]{:S(2)}) collective-permute-start(bf16[2,256,512]{2,1,0:T(8,128)(2,1)} %get-tuple-element.21), channel_id=1, source_target_pairs={{0,8},{8,16},{16,24},{24,32},{32,40},{40,48},{48,56},{56,64},{64,7... | collective-permute-start | bytes 1572872 | tf_op jit(solution)/shard_map/ppermute | solution.py:435
  56.7 24.0 %collective-permute-start.1 = (bf16[2,192,512]{2,1,0:T(8,128)(2,1)}, bf16[2,192,512]{2,1,0:T(8,128)(2,1)S(1)}, u32[]{:S(2)}, u32[]{:S(2)}) collective-permute-start(bf16[2,192,512]{2,1,0:T(8,128)(2,1)} %get-tuple-element.23), channel_id=1, source_target_pairs={{8,0},{16,8},{24,16},{32,24},{40,32},{48,40},{56,48},{64,56},{72,6... | collective-permute-start | bytes 1179656 | tf_op jit(solution)/shard_map/ppermute | solution.py:436
  80.7 3.5 %copy-start.2 = (bf16[2,192,512]{2,1,0:T(8,128)(2,1)}, bf16[2,192,512]{2,1,0:T(8,128)(2,1)S(1)}, u32[]{:S(2)}) copy-start(bf16[2,192,512]{2,1,0:T(8,128)(2,1)S(1)} %collective-permute-done.1.after_ref) | copy-start | bytes 1179652
  84.2 0.8 copy-start.1
  94.7 1.3 copy-start
Sparse Core Ops, SparseCore 0:
  9.0 34.7 all-gather.2
  45.6 49.5 all-gather.4

commit v5 on v4

--- a/solution.py
+++ b/solution.py
@@ -4,6 +4,7 @@
 from jax.experimental import pallas as pl
 from jax.experimental.pallas import tpu as pltpu
 from jax.sharding import PartitionSpec as P
+
 
 HEAD_DIM = 64
 GRID_W = 64
@@ -64,7 +65,7 @@
     return jnp.concatenate([tiles[tile, row : row + 1, :] for tile in range(tiles.shape[0])], axis=1)
 
 
-def project(rows, gain, modulation, weights, row_of, block, ends, copies=0, copy_samples=1):
+def project(rows, gain, modulation, weights, row_of, block, ends):
     samples, count, width = rows.shape
     every = modulation.shape[1] // 3 + 1
     cols = weights[0].shape[1]
@@ -92,12 +93,8 @@
             for ref in weight_refs[:2]
         ]
         if not ends:
-            for copy in range(copies):
-                for number in range(copy_samples):
-                    size = block // copy_samples
-                    low = number * size
-                    out_refs[0][copy, number, :, :cols] = pair[0][low : low + size]
-                    out_refs[0][copy, number, :, cols:] = pair[1][low : low + size]
+            out_refs[0][0, :, :cols] = pair[0]
+            out_refs[0][0, :, cols:] = pair[1]
             return
         out_refs[0][0, :, :cols] = pair[0]
         out_refs[0][0, :, cols:] = pair[1]
@@ -130,8 +127,8 @@
             out_specs += [pl.BlockSpec((1, length, 2 * cols), lambda s, i: (s, 0, 0))]
             out_shape += [(samples, length, 2 * cols)]
     else:
-        out_shape = [(copies, copy_samples, count // copy_samples, 2 * cols)]
-        out_specs = [whole(out_shape[0])]
+        out_specs = [blocks(2 * cols)]
+        out_shape = [(samples, count, 2 * cols)]
     return pl.pallas_call(
         body,
         grid=(samples, steps),
@@ -288,23 +285,30 @@
     )(place, query, before, pair, after, table)
 
 
-def attend_far(query, ctx_pair, ctx_bias, near, per):
+def attend_far(query, ctx_pairs, ctx_bias, near, per):
     samples, tokens, cols = query.shape
     rows_dev = tokens // GRID_W
-    owners, _, ctx_rows, _ = ctx_pair.shape
-    ctx_count = owners * ctx_rows
+    lines = len(ctx_pairs)
+    members, _, ctx_rows, _ = ctx_pairs[0].shape
+    ctx_count = lines * members * ctx_rows
     bf16, f32 = jnp.bfloat16, jnp.float32
 
-    def body(q_ref, ctx_ref, cb_ref, mixed_ref, top_ref, total_ref, out_ref, far_t, values):
+    def body(q_ref, *refs):
+        ctx_refs = refs[:lines]
+        cb_ref, mixed_ref, top_ref, total_ref, out_ref, far_t, values = refs[lines:]
+
         @pl.when(pl.program_id(1) == 0)
         def _():
-            for owner in range(owners):
-                values[owner * ctx_rows : (owner + 1) * ctx_rows] = ctx_ref[owner, 0, :, cols:]
-            for first in range(0, owners, 2):
+            size = members * ctx_rows
+            for line, ctx_ref in enumerate(ctx_refs):
+                at = line * size
+                for member in range(members):
+                    low = at + member * ctx_rows
+                    values[low : low + ctx_rows] = ctx_ref[member, 0, :, cols:]
                 block = jnp.concatenate(
-                    [ctx_ref[first, 0, :, :cols], ctx_ref[first + 1, 0, :, :cols]], axis=0
+                    [ctx_ref[member, 0, :, :cols] for member in range(members)], axis=0
                 )
-                far_t[:, first * ctx_rows : (first + 2) * ctx_rows] = block.T
+                far_t[:, at : at + size] = block.T
 
         masks = head_masks(cols)
         scores = [
@@ -333,9 +337,9 @@
         grid=(samples, rows_dev // per),
         in_specs=[
             rows_spec,
-            pl.BlockSpec((owners, 1, ctx_rows, 2 * cols), lambda s, i: (0, s, 0, 0)),
-            whole(ctx_bias.shape),
         ]
+        + [pl.BlockSpec((members, 1, ctx_rows, 2 * cols), lambda s, i: (0, s, 0, 0))] * lines
+        + [whole(ctx_bias.shape)]
         + [rows_spec] * 3,
         out_specs=pl.BlockSpec((per, 1, GRID_W, cols), lambda s, i: (i, s, 0, 0)),
         out_shape=jax.ShapeDtypeStruct((rows_dev, samples, GRID_W, cols), bf16),
@@ -344,20 +348,20 @@
             pltpu.VMEM((ctx_count, cols), bf16),
         ],
         name="attend_far",
-    )(query, ctx_pair, ctx_bias, *near)
-
-
-def finish(attended, w_out, latent, modulation):
-    groups, rows, cols = attended.shape
+    )(query, *ctx_pairs, ctx_bias, *near)
+
+
+def finish(attended, w_out, latent, modulation, tiles):
+    groups, _, _ = attended.shape
     samples, tokens, width = latent.shape
-    block = modulation.shape[2]
+    block = modulation.shape[2] * tiles
     first = modulation.shape[1] - samples
 
     def body(att_ref, w_ref, latent_ref, tile_ref, out_ref):
         everything = jnp.concatenate([att_ref[group] for group in range(groups)], axis=1)
         update = jnp.dot(everything, w_ref[...], preferred_element_type=jnp.float32)
         for s in range(samples):
-            gate = tile_ref[0, first + s : first + s + 1, :]
+            gate = modulation_row(tile_ref, first + s)
             part = update[s * tokens : (s + 1) * tokens]
             out_ref[s] = (latent_ref[s].astype(jnp.float32) + gate * part).astype(jnp.bfloat16)
 
@@ -368,7 +372,7 @@
             whole(attended.shape),
             pl.BlockSpec((width, block), lambda i: (0, i)),
             pl.BlockSpec((samples, tokens, block), lambda i: (0, 0, i)),
-            pl.BlockSpec((1, *modulation.shape[1:]), lambda i: (i, 0, 0)),
+            pl.BlockSpec((tiles, *modulation.shape[1:]), lambda i: (i, 0, 0)),
         ],
         out_specs=pl.BlockSpec((samples, tokens, block), lambda i: (0, 0, i)),
         out_shape=jax.ShapeDtypeStruct(latent.shape, latent.dtype),
@@ -376,7 +380,19 @@
     )(attended, w_out, latent, modulation)
 
 
-def on_device(
+def shifted(size, side, stride, value):
+    span = side * stride
+    return [(i, i // span * span + (i + value * stride) % span) for i in range(size)]
+
+
+def from_line(block, axis, side, stride):
+    size = lax.axis_size(axis)
+    return [block] + [
+        lax.ppermute(block, axis, shifted(size, side, stride, value)) for value in range(1, side)
+    ]
+
+
+def computation(
     latent,
     context,
     cond,
@@ -417,10 +433,9 @@
         samples,
         samples * ctx_rows,
         None,
-        sp_size,
-        samples,
     )
-    ctx_pair = lax.all_to_all(ctx_pair, "sp", 0, 0, tiled=True)
+    ctx_pair = ctx_pair.reshape(samples, ctx_rows, 2 * local_cols)
+    ctx_pairs = from_line(ctx_pair, "sp", 4, 1)
     up = [(i, i + 1) for i in range(sp_size - 1)]
     down = [(j, i) for i, j in up]
     pair, query, first, last = project(
@@ -432,19 +447,22 @@
         256,
         ((WIN_ROWS - REACH - 1) * GRID_W, REACH * GRID_W),
     )
+    ctx_pairs, query = lax.optimization_barrier((ctx_pairs, query))
+    ctx_line = jnp.stack(ctx_pairs)
+    ctx_pairs = from_line(ctx_line, "sp", 4, 4)
     before = lax.ppermute(last, "sp", up)
     after = lax.ppermute(first, "sp", down)
     rows_all = pair.shape[1] // GRID_W * sp_size
     near = attend_near(place, query, before, pair, after, table, rows_all, 2)
-    attended = attend_far(query, ctx_pair, cb, near, 2)
+    attended = attend_far(query, ctx_pairs, cb, near, 2)
     attended = attended.reshape(tp_size, samples * tokens_dev, local_cols)
     attended = lax.all_to_all(attended, "tp", 0, 0, tiled=True)
-    return finish(attended, w_out_all, latent, modulation)
+    return finish(attended, w_out_all, latent, modulation, 4)
 
 
 def solution(mesh):
     return jax.shard_map(
-        on_device,
+        computation,
         mesh=mesh,
         in_specs=(
             P(None, ("sp", "tp"), None),

time: 139 us -> 135 us (0.971)
  the two profiles are of different devices: /device:TPU:32 before, /device:TPU:1 now
where the time goes in v5:
time: 135 us; the launch traced here: 134 us
  Pallas kernels  42.7 us (32%)
  blocking collectives  26.9 us (20%)
  waiting for transfers between devices  25 us (19%)
  starting transfers between devices  20.8 us (15%)
  between operations  13.5 us (10%)
  local copies, waits for them, and re-layouts  5.3 us (4%)
    all_to_all x1, blocking collectives, computation(): attended = lax.all_to_all(attended, 'tp', 0, 0, tiled=True)  14.8 us
    all_to_all x1, blocking collectives, copy_for_each(): lax.all_to_all(jnp.broadcast_to(shard[None], (length, *shard.shape)), axi...  12 us
    pallas_call x2, Pallas kernels, project(): pl.pallas_call(body, grid=(samples, steps), in_specs=[blocks(width), whol...  11.5 us
    pallas_call x1, Pallas kernels, attend_far(): pl.pallas_call(body, grid=(samples, rows_dev // per), in_specs=[rows_spec...  11.4 us
    ppermute x6, waiting for transfers between devices, from_line(): lax.ppermute(block, axis, shifted(size, side, stride, value))  10.6 us
    ppermute x1, waiting for transfers between devices, computation(): after = lax.ppermute(first, 'sp', down)  10.2 us
    pallas_call x1, Pallas kernels, attend_near(): pl.pallas_call(body, grid=(samples, rows_dev // per), in_specs=[pl.BlockS...  9.77 us
    all_to_all x1, starting transfers between devices, computation(): summed = jnp.sum(lax.all_to_all(parts, 'sp', 0, 0, tiled=True), axis=0)  8.43 us
  transfers between devices with their start and end apart: 11, of which 4 were waited for; matrix products, arithmetic and copies ran while one was open for 3% of the time, Pallas kernels for 28%

profile of v5, /device:TPU:1, one launch (start us, length us, event | category | flops | bytes accessed | tf_op | source)
XLA Modules:
  0.0 134.3 jit_solution(7158498010924665861)
XLA Ops:
  6.5 0.0 all-gather.3.cloned.1.call-start
  6.5 0.7 all-gather.3.cloned.1.call-update
  7.3 0.0 all-gather.5.cloned.1.call-start
  7.3 1.3 broadcast_in_dim.20.ctx_ref
  8.6 1.7 %modulation_parts.1 = f32[16,8,256]{2,1,0:T(8,128)} custom-call(s32[1]{0:T(128)} %bitcast.2.place_ref, bf16[2,2048]{1,0:T(2,128)(2,1)} %cond_ref.1, bf16[1,2048]{1,0:T(2,128)(2,1)} %broadcast_in_dim.20.ctx_ref, bf16[128,256]{1,0:T(8,128)(2,1)} %shift_ref.1, bf16[128,256]{1,0:T(8,128)(2,1)} %scale_ref.1, bf16[128,256]{1,0:T(8,128)(2,1)} %gate_ref.1), custom_call_target="tpu_custom_call" | custom-call | tf_op jit(solution)/shard_map/modulation_parts/pallas_call | solution.py:51
  10.3 0.0 all-gather.5.cloned.1.call-update
  10.4 8.4 %all-to-all-start = ((f32[16,8,256]{2,1,0:T(8,128)}), f32[16,8,256]{2,1,0:T(8,128)S(1)}, u32[]{:S(2)}, u32[]{:S(2)}) async-start(f32[16,8,256]{2,1,0:T(8,128)} %modulation_parts.1), calls=%async_computation | async-start | bytes 262144 | tf_op jit(solution)/shard_map/all_to_all | solution.py:422
  18.8 0.8 copy.16
  19.6 0.6 pad.4.clone
  20.2 3.0 %bias_table.1.table_ref = f32[2,256,896]{2,1,0:T(8,128)} custom-call(f32[64,128]{1,0:T(8,128)} %bitcast.16), custom_call_target="tpu_custom_call" | custom-call | tf_op jit(solution)/shard_map/bias_table/pallas_call | solution.py:173
  23.2 0.0 copy-done.7
  23.2 0.1 broadcast_in_dim.21
  23.2 0.7 broadcast_in_dim_reshape.3.refs_4_
  23.9 1.8 %all-to-all-done = f32[16,8,256]{2,1,0:T(8,128)S(1)} async-done(((f32[16,8,256]{2,1,0:T(8,128)}), f32[16,8,256]{2,1,0:T(8,128)S(1)}, u32[]{:S(2)}, u32[]{:S(2)}) %all-to-all-start) | async-done | bytes 131104 | tf_op jit(solution)/shard_map/all_to_all | solution.py:422
  25.7 12.0 %all_to_all.15.tiles_ref.tile_ref = f32[8,8,256]{2,1,0:T(8,128)} all-to-all(f32[8,8,256]{2,1,0:T(8,128)S(1)} %broadcast_in_dim.22), channel_id=1, replica_groups=mesh['sp'=16,'tp'=8] {'tp'}, dimensions={0} | all-to-all | bytes 131072 | tf_op jit(solution)/shard_map/all_to_all | solution.py:21
  37.7 3.0 %project.2 = bf16[1,128,512]{2,1,0:T(8,128)(2,1)} custom-call(bf16[1,128,2048]{2,1,0:T(8,128)(2,1)} %bitcast.11, f32[1,2048]{1,0:T(1,128)} %bitcast.20, f32[8,8,256]{2,1,0:T(8,128)} %all_to_all.15.tiles_ref.tile_ref, bf16[2048,256]{1,0:T(8,128)(2,1)} %refs_0_.3, bf16[2048,256]{1,0:T(8,128)(2,1)} %refs_1_.3), custom_call_target="tpu_custom_call" | custom-call | tf_op jit(solution)/shard_map/project/pallas_call | solution.py:132
  40.8 0.2 collective-permute-start
  41.0 1.6 %collective-permute-start.1 = (bf16[2,64,512]{2,1,0:T(8,128)(2,1)}, bf16[2,64,512]{2,1,0:T(8,128)(2,1)S(1)}, u32[]{:S(2)}, u32[]{:S(2)}) collective-permute-start(bf16[2,64,512]{2,1,0:T(8,128)(2,1)} %bitcast.13), channel_id=1, source_target_pairs={{0,16},{8,24},{16,0},{24,8},{32,48},{40,56},{48,32},{56,40},{64,80... | collective-permute-start | bytes 393224 | tf_op jit(solution)/shard_map/ppermute | solution.py:391
  42.6 1.2 collective-permute-start.2
  43.7 1.7 %all-gather.3.cloned.1.call-done.rows_ref = bf16[2,512,2048]{2,1,0:T(8,128)(2,1)} async-done(((bf16[2,64,2048]{2,1,0:T(8,128)(2,1)}), bf16[2,512,2048]{2,1,0:T(8,128)(2,1)}) %all-gather.3.cloned.1.call-update) | async-done | bytes 4194320 | tf_op jit(solution)/shard_map/all_gather | solution.py:416
  45.4 8.5 %project.3 = (bf16[2,512,512]{2,1,0:T(8,128)(2,1)}, bf16[2,512,256]{2,1,0:T(8,128)(2,1)}, bf16[2,192,512]{2,1,0:T(8,128)(2,1)}, bf16[2,256,512]{2,1,0:T(8,128)(2,1)}) custom-call(bf16[2,512,2048]{2,1,0:T(8,128)(2,1)} %all-gather.3.cloned.1.call-done.rows_ref, f32[1,2048]{1,0:T(1,128)} %bitcast.21, f32[8,8,256]{2,1,0:T(8,128)} %all_to_all.15.tiles_ref.tile_ref, ...), custom_call_target="tpu_custom_call" | custom-call | tf_op jit(solution)/shard_map/project/pallas_call | solution.py:132
  53.9 0.0 collective-permute-done
  53.9 0.0 collective-permute-done.1
  53.9 0.0 collective-permute-done.2
  53.9 3.1 %collective-permute-start.6 = (bf16[2,256,512]{2,1,0:T(8,128)(2,1)}, bf16[2,256,512]{2,1,0:T(8,128)(2,1)S(1)}, u32[]{:S(2)}, u32[]{:S(2)}) collective-permute-start(bf16[2,256,512]{2,1,0:T(8,128)(2,1)} %get-tuple-element.31), channel_id=1, source_target_pairs={{0,8},{8,16},{16,24},{24,32},{32,40},{40,48},{48,56},{56,64},{64,7... | collective-permute-start | bytes 1572872 | tf_op jit(solution)/shard_map/ppermute | solution.py:453
  57.1 0.0 copy-done.2
  57.1 0.1 pad_maximum_fusion.refs_0_
  57.2 0.0 copy-start
  57.2 1.3 collective-permute-start.3
  58.5 2.6 %collective-permute-start.4 = (bf16[4,2,64,512]{3,2,1,0:T(8,128)(2,1)S(1)}, bf16[4,2,64,512]{3,2,1,0:T(8,128)(2,1)S(1)}, u32[]{:S(2)}, u32[]{:S(2)}) collective-permute-start(bf16[4,2,64,512]{3,2,1,0:T(8,128)(2,1)S(1)} %pad_maximum_fusion.refs_0_), channel_id=1, source_target_pairs={{0,64},{8,72},{16,80},{24,88},{32,96},{40,104},{48,112},{56,120},{... | collective-permute-start | bytes 1572872 | tf_op jit(solution)/shard_map/ppermute | solution.py:391
  61.1 1.1 collective-permute-start.5
  62.2 1.3 collective-permute-start.7
  63.5 10.2 %collective-permute-done.7.after_ref = bf16[2,192,512]{2,1,0:T(8,128)(2,1)S(1)} collective-permute-done((bf16[2,192,512]{2,1,0:T(8,128)(2,1)}, bf16[2,192,512]{2,1,0:T(8,128)(2,1)S(1)}, u32[]{:S(2)}, u32[]{:S(2)}) %collective-permute-start.7) | collective-permute-done | bytes 393248 | tf_op jit(solution)/shard_map/ppermute | solution.py:454
  73.7 0.0 collective-permute-done.6.before_ref
  73.7 0.7 copy-done.6
  74.4 0.2 copy-done.1
  74.6 9.8 %attend_near.1 = (f32[2,512,256]{2,1,0:T(8,128)}, f32[2,512,256]{2,1,0:T(8,128)}, f32[2,512,256]{2,1,0:T(8,128)}) custom-call(s32[1]{0:T(128)} %bitcast.2.place_ref, bf16[2,512,256]{2,1,0:T(8,128)(2,1)} %get-tuple-element.25.q_ref, bf16[2,256,512]{2,1,0:T(8,128)(2,1)} %copy-done.1, bf16[2,512,512]{2,1,0:T(8,128)(2,1)} %get-tuple-element.32.pair_ref, ...), custom_call_target="tpu_custom_call" | custom-call | tf_op jit(solution)/shard_map/attend_near/pallas_call | solution.py:267
  84.4 0.0 collective-permute-done.3.refs_1_
  84.4 0.0 copy-start.3
  84.4 10.6 %collective-permute-done.4.refs_2_ = bf16[4,2,64,512]{3,2,1,0:T(8,128)(2,1)S(1)} collective-permute-done((bf16[4,2,64,512]{3,2,1,0:T(8,128)(2,1)S(1)}, bf16[4,2,64,512]{3,2,1,0:T(8,128)(2,1)S(1)}, u32[]{:S(2)}, u32[]{:S(2)}) %collective-permute-start.4) | collective-permute-done | bytes 524320 | tf_op jit(solution)/shard_map/ppermute | solution.py:391
  95.0 0.0 collective-permute-done.5.refs_3_
  95.0 0.0 copy-done
  95.0 0.0 copy-done.3
  95.0 0.8 copy-done.4
  95.8 0.2 copy-done.5
  96.0 11.4 %attend_far.1 = bf16[8,2,64,256]{3,2,1,0:T(8,128)(2,1)} custom-call(bf16[2,512,256]{2,1,0:T(8,128)(2,1)} %get-tuple-element.25.q_ref, bf16[4,2,64,512]{3,2,1,0:T(8,128)(2,1)} %copy-done, bf16[4,2,64,512]{3,2,1,0:T(8,128)(2,1)} %copy-done.3, bf16[4,2,64,512]{3,2,1,0:T(8,128)(2,1)} %copy-done.4, bf16[4,2,64,512]{3,2,1,0:T(8,128)(2,1)} %copy-done.5, ...), custom_call_target="tpu_custom_call" | custom-call | tf_op jit(solution)/shard_map/attend_far/pallas_call | solution.py:335
  107.4 14.8 %all_to_all.16.att_ref = bf16[8,128,256]{2,1,0:T(8,128)(2,1)} all-to-all(bf16[8,128,256]{2,1,0:T(8,128)(2,1)} %bitcast.10), channel_id=1, replica_groups=mesh['sp'=16,'tp'=8] {'tp'}, dimensions={0} | all-to-all | bytes 1048576 | tf_op jit(solution)/shard_map/all_to_all | solution.py:459
  122.2 5.2 %finish.1 = bf16[2,64,2048]{2,1,0:T(8,128)(2,1)} custom-call(bf16[8,128,256]{2,1,0:T(8,128)(2,1)} %all_to_all.16.att_ref, bf16[2048,2048]{1,0:T(8,128)(2,1)} %all-gather.5.cloned.1.call-done.w_ref, bf16[2,64,2048]{2,1,0:T(8,128)(2,1)} %latent_ref.1, f32[8,8,256]{2,1,0:T(8,128)} %all_to_all.15.tiles_ref.tile_ref), custom_call_target="tpu_custom_call" | custom-call | tf_op jit(solution)/shard_map/finish/pallas_call | solution.py:368
  (9 shorter events, 0.0 us)
Async XLA Ops:
  6.5 16.6 %copy-start.7 = (f32[4]{0:T(128)S(1)}, f32[4]{0:T(128)}, u32[]{:S(2)}) copy-start(f32[4]{0:T(128)} %param.27) | copy-start | bytes 52
  6.5 38.9 %all-gather.3.cloned.1.call-start = ((), (), s32[]{:S(2)}) async-start(), calls=%async_computation.3 | async-start | bytes 4718592 | tf_op jit(solution)/shard_map/all_gather | solution.py:416
  7.3 115.0 %all-gather.5.cloned.1.call-start = ((), (), s32[]{:S(2)}) async-start(), calls=%async_computation.4 | async-start | bytes 9437184 | tf_op jit(solution)/shard_map/all_gather | solution.py:419
  10.4 15.3 %all-to-all-start = ((f32[16,8,256]{2,1,0:T(8,128)}), f32[16,8,256]{2,1,0:T(8,128)S(1)}, u32[]{:S(2)}, u32[]{:S(2)}) async-start(f32[16,8,256]{2,1,0:T(8,128)} %modulation_parts.1), calls=%async_computation | async-start | bytes 262144 | tf_op jit(solution)/shard_map/all_to_all | solution.py:422
  40.8 16.3 %copy-start.2 = (bf16[1,128,512]{2,1,0:T(8,128)(2,1)S(1)}, bf16[1,128,512]{2,1,0:T(8,128)(2,1)}, u32[]{:S(2)}) copy-start(bf16[1,128,512]{2,1,0:T(8,128)(2,1)} %project.2) | copy-start | bytes 393220
  40.8 13.1 %collective-permute-start = (bf16[2,64,512]{2,1,0:T(8,128)(2,1)}, bf16[2,64,512]{2,1,0:T(8,128)(2,1)S(1)}, u32[]{:S(2)}, u32[]{:S(2)}) collective-permute-start(bf16[2,64,512]{2,1,0:T(8,128)(2,1)} %bitcast.12), channel_id=1, source_target_pairs={{0,8},{8,16},{16,24},{24,0},{32,40},{40,48},{48,56},{56,32},{64,72... | collective-permute-start | bytes 393224 | tf_op jit(solution)/shard_map/ppermute | solution.py:391
  41.0 12.9 %collective-permute-start.1 = (bf16[2,64,512]{2,1,0:T(8,128)(2,1)}, bf16[2,64,512]{2,1,0:T(8,128)(2,1)S(1)}, u32[]{:S(2)}, u32[]{:S(2)}) collective-permute-start(bf16[2,64,512]{2,1,0:T(8,128)(2,1)} %bitcast.13), channel_id=1, source_target_pairs={{0,16},{8,24},{16,0},{24,8},{32,48},{40,56},{48,32},{56,40},{64,80... | collective-permute-start | bytes 393224 | tf_op jit(solution)/shard_map/ppermute | solution.py:391
  42.6 11.3 %collective-permute-start.2 = (bf16[2,64,512]{2,1,0:T(8,128)(2,1)}, bf16[2,64,512]{2,1,0:T(8,128)(2,1)S(1)}, u32[]{:S(2)}, u32[]{:S(2)}) collective-permute-start(bf16[2,64,512]{2,1,0:T(8,128)(2,1)} %bitcast.14), channel_id=1, source_target_pairs={{0,24},{8,0},{16,8},{24,16},{32,56},{40,32},{48,40},{56,48},{64,88... | collective-permute-start | bytes 393224 | tf_op jit(solution)/shard_map/ppermute | solution.py:391
  53.9 19.7 %collective-permute-start.6 = (bf16[2,256,512]{2,1,0:T(8,128)(2,1)}, bf16[2,256,512]{2,1,0:T(8,128)(2,1)S(1)}, u32[]{:S(2)}, u32[]{:S(2)}) collective-permute-start(bf16[2,256,512]{2,1,0:T(8,128)(2,1)} %get-tuple-element.31), channel_id=1, source_target_pairs={{0,8},{8,16},{16,24},{24,32},{32,40},{40,48},{48,56},{56,64},{64,7... | collective-permute-start | bytes 1572872 | tf_op jit(solution)/shard_map/ppermute | solution.py:453
  57.2 37.9 %copy-start = (bf16[4,2,64,512]{3,2,1,0:T(8,128)(2,1)}, bf16[4,2,64,512]{3,2,1,0:T(8,128)(2,1)S(1)}, u32[]{:S(2)}) copy-start(bf16[4,2,64,512]{3,2,1,0:T(8,128)(2,1)S(1)} %pad_maximum_fusion.refs_0_) | copy-start | bytes 1572868
  57.2 27.2 %collective-permute-start.3 = (bf16[4,2,64,512]{3,2,1,0:T(8,128)(2,1)S(1)}, bf16[4,2,64,512]{3,2,1,0:T(8,128)(2,1)S(1)}, u32[]{:S(2)}, u32[]{:S(2)}) collective-permute-start(bf16[4,2,64,512]{3,2,1,0:T(8,128)(2,1)S(1)} %pad_maximum_fusion.refs_0_), channel_id=1, source_target_pairs={{0,32},{8,40},{16,48},{24,56},{32,64},{40,72},{48,80},{56,88},{64,... | collective-permute-start | bytes 1572872 | tf_op jit(solution)/shard_map/ppermute | solution.py:391
  58.5 36.5 %collective-permute-start.4 = (bf16[4,2,64,512]{3,2,1,0:T(8,128)(2,1)S(1)}, bf16[4,2,64,512]{3,2,1,0:T(8,128)(2,1)S(1)}, u32[]{:S(2)}, u32[]{:S(2)}) collective-permute-start(bf16[4,2,64,512]{3,2,1,0:T(8,128)(2,1)S(1)} %pad_maximum_fusion.refs_0_), channel_id=1, source_target_pairs={{0,64},{8,72},{16,80},{24,88},{32,96},{40,104},{48,112},{56,120},{... | collective-permute-start | bytes 1572872 | tf_op jit(solution)/shard_map/ppermute | solution.py:391
  61.1 33.9 %collective-permute-start.5 = (bf16[4,2,64,512]{3,2,1,0:T(8,128)(2,1)S(1)}, bf16[4,2,64,512]{3,2,1,0:T(8,128)(2,1)S(1)}, u32[]{:S(2)}, u32[]{:S(2)}) collective-permute-start(bf16[4,2,64,512]{3,2,1,0:T(8,128)(2,1)S(1)} %pad_maximum_fusion.refs_0_), channel_id=1, source_target_pairs={{0,96},{8,104},{16,112},{24,120},{32,0},{40,8},{48,16},{56,24},{64... | collective-permute-start | bytes 1572872 | tf_op jit(solution)/shard_map/ppermute | solution.py:391
  62.2 11.5 %collective-permute-start.7 = (bf16[2,192,512]{2,1,0:T(8,128)(2,1)}, bf16[2,192,512]{2,1,0:T(8,128)(2,1)S(1)}, u32[]{:S(2)}, u32[]{:S(2)}) collective-permute-start(bf16[2,192,512]{2,1,0:T(8,128)(2,1)} %get-tuple-element.33), channel_id=1, source_target_pairs={{8,0},{16,8},{24,16},{32,24},{40,32},{48,40},{56,48},{64,56},{72,6... | collective-permute-start | bytes 1179656 | tf_op jit(solution)/shard_map/ppermute | solution.py:454
  73.7 0.8 copy-start.6
  73.7 0.9 copy-start.1
  84.4 10.7 %copy-start.3 = (bf16[4,2,64,512]{3,2,1,0:T(8,128)(2,1)}, bf16[4,2,64,512]{3,2,1,0:T(8,128)(2,1)S(1)}, u32[]{:S(2)}) copy-start(bf16[4,2,64,512]{3,2,1,0:T(8,128)(2,1)S(1)} %collective-permute-done.3.refs_1_) | copy-start | bytes 1572868
  95.0 0.8 copy-start.4
  95.0 1.0 copy-start.5
Sparse Core Ops, SparseCore 0:
  9.0 36.3 all-gather.2
  47.1 49.6 all-gather.4

commit v6 on v3

--- a/solution.py
+++ b/solution.py
@@ -93,8 +93,8 @@
             for ref in weight_refs[:2]
         ]
         if not ends:
-            out_refs[0][0] = pair[0]
-            out_refs[1][0] = pair[1]
+            out_refs[0][0, :, :cols] = pair[0]
+            out_refs[0][0, :, cols:] = pair[1]
             return
         out_refs[0][0, :, :cols] = pair[0]
         out_refs[0][0, :, cols:] = pair[1]
@@ -127,8 +127,8 @@
             out_specs += [pl.BlockSpec((1, length, 2 * cols), lambda s, i: (s, 0, 0))]
             out_shape += [(samples, length, 2 * cols)]
     else:
-        out_specs = [blocks(cols)] * 2
-        out_shape = [(samples, count, cols)] * 2
+        out_specs = [blocks(2 * cols)]
+        out_shape = [(samples, count, 2 * cols)]
     return pl.pallas_call(
         body,
         grid=(samples, steps),
@@ -177,7 +177,7 @@
     )(padded)
 
 
-def attend(place, query, before, pair, after, ctx_keys, ctx_values, table, ctx_bias, rows_all, per):
+def attend(place, query, before, pair, after, ctx_pairs, table, ctx_bias, rows_all, per):
     samples, tokens, cols = query.shape
     heads = cols // HEAD_DIM
     rows_dev = tokens // GRID_W
@@ -185,14 +185,15 @@
     ahead, behind = before.shape[1], after.shape[1]
     padded = ahead + tokens + behind
     lanes = -(-padded // 128) * 128
-    groups, members, _, ctx_rows, _ = (len(ctx_keys), *ctx_keys[0].shape)
-    ctx_count = groups * members * ctx_rows
+    ctx_rows = ctx_pairs[0].shape[2]
+    members = [array.shape[0] for array in ctx_pairs]
+    ctx_count = sum(members) * ctx_rows
     queries = heads * GRID_W
     bf16, f32 = jnp.bfloat16, jnp.float32
 
     def body(place_ref, q_ref, before_ref, pair_ref, after_ref, *refs):
-        key_refs, value_refs = refs[:groups], refs[groups : groups + members]
-        table_ref, cb_ref, out_ref, near_t, far_t, values, far_values = refs[groups + members :]
+        ctx_refs = refs[: len(members)]
+        table_ref, cb_ref, out_ref, near_t, far_t, values, far_values = refs[len(members) :]
         step = pl.program_id(1)
 
         @pl.when(step == 0)
@@ -200,13 +201,17 @@
             values[0:ahead] = before_ref[0, :, cols:]
             values[ahead : ahead + tokens] = pair_ref[0, :, cols:]
             values[ahead + tokens : padded] = after_ref[0, :, cols:]
-            for group in range(groups):
-                block = jnp.concatenate([key_refs[group][m, 0] for m in range(members)], axis=0)
-                size = members * ctx_rows
-                far_t[:, group * size : (group + 1) * size] = block.T
-                for member in range(members):
-                    at = (group * members + member) * ctx_rows
-                    far_values[at : at + ctx_rows] = value_refs[member][group, 0]
+            at = 0
+            for ctx_ref, count in zip(ctx_refs, members):
+                for member in range(count):
+                    low = at + member * ctx_rows
+                    far_values[low : low + ctx_rows] = ctx_ref[member, 0, :, cols:]
+                size = count * ctx_rows
+                block = jnp.concatenate(
+                    [ctx_ref[member, 0, :, :cols] for member in range(count)], axis=0
+                )
+                far_t[:, at : at + size] = block.T
+                at += size
             fill = jnp.zeros((lanes - padded, cols), bf16)
             near_t[0, :, :ahead] = before_ref[0, :, :cols].T
             near_t[0, :, ahead : ahead + tokens] = pair_ref[0, :, :cols].T
@@ -272,7 +277,6 @@
     def of_sample(array):
         return pl.BlockSpec((1, *array.shape[1:]), lambda s, i: (s, 0, 0))
 
-    far_spec = pl.BlockSpec((members, 1, ctx_rows, cols), lambda s, i: (0, s, 0, 0))
     return pl.pallas_call(
         body,
         grid=(samples, rows_dev // per),
@@ -283,7 +287,10 @@
             of_sample(pair),
             of_sample(after),
         ]
-        + [far_spec] * (groups + members)
+        + [
+            pl.BlockSpec((count, 1, ctx_rows, 2 * cols), lambda s, i: (0, s, 0, 0))
+            for count in members
+        ]
         + [whole(table.shape), whole((queries, 1))],
         out_specs=pl.BlockSpec((per, 1, GRID_W, cols), lambda s, i: (i, s, 0, 0)),
         out_shape=jax.ShapeDtypeStruct((rows_dev, samples, GRID_W, cols), bf16),
@@ -294,20 +301,20 @@
             pltpu.VMEM((ctx_count, cols), bf16),
         ],
         name="attend",
-    )(place, query, before, pair, after, *ctx_keys, *ctx_values, table, ctx_bias)
-
-
-def finish(attended, w_out, latent, modulation):
+    )(place, query, before, pair, after, *ctx_pairs, table, ctx_bias)
+
+
+def finish(attended, w_out, latent, modulation, tiles):
     groups, _, _ = attended.shape
     samples, tokens, width = latent.shape
-    block = modulation.shape[2]
+    block = modulation.shape[2] * tiles
     first = modulation.shape[1] - samples
 
     def body(att_ref, w_ref, latent_ref, tile_ref, out_ref):
         everything = jnp.concatenate([att_ref[group] for group in range(groups)], axis=1)
         update = jnp.dot(everything, w_ref[...], preferred_element_type=jnp.float32)
         for s in range(samples):
-            gate = tile_ref[0, first + s : first + s + 1, :]
+            gate = modulation_row(tile_ref, first + s)
             part = update[s * tokens : (s + 1) * tokens]
             out_ref[s] = (latent_ref[s].astype(jnp.float32) + gate * part).astype(jnp.bfloat16)
 
@@ -318,7 +325,7 @@
             whole(attended.shape),
             pl.BlockSpec((width, block), lambda i: (0, i)),
             pl.BlockSpec((samples, tokens, block), lambda i: (0, 0, i)),
-            pl.BlockSpec((1, *modulation.shape[1:]), lambda i: (i, 0, 0)),
+            pl.BlockSpec((tiles, *modulation.shape[1:]), lambda i: (i, 0, 0)),
         ],
         out_specs=pl.BlockSpec((samples, tokens, block), lambda i: (0, 0, i)),
         out_shape=jax.ShapeDtypeStruct(latent.shape, latent.dtype),
@@ -371,7 +378,7 @@
 
     gain = norm_gain[None, :]
     ctx_rows = context.shape[1]
-    ctx_keys, ctx_values = project(
+    (ctx_pair,) = project(
         context.reshape(1, samples * ctx_rows, width),
         gain,
         modulation,
@@ -380,13 +387,8 @@
         samples * ctx_rows,
         None,
     )
-    ctx_keys = ctx_keys.reshape(samples, ctx_rows, local_cols)
-    ctx_values = ctx_values.reshape(samples, ctx_rows, local_cols)
-    ctx_keys = jnp.stack(from_line(ctx_keys, "sp", 4, 1))
-    ctx_values = jnp.stack(from_line(ctx_values, "sp", 4, 4))
-    gathered, ctx_keys, ctx_values = lax.optimization_barrier((gathered, ctx_keys, ctx_values))
-    ctx_keys = from_line(ctx_keys, "sp", 4, 4)
-    ctx_values = from_line(ctx_values, "sp", 4, 1)
+    ctx_pair = ctx_pair.reshape(samples, ctx_rows, 2 * local_cols)
+    ctx_pairs = from_line(ctx_pair, "sp", 4, 1)
     up = [(i, i + 1) for i in range(sp_size - 1)]
     down = [(j, i) for i, j in up]
     pair, query, first, last = project(
@@ -398,15 +400,26 @@
         256,
         ((WIN_ROWS - REACH - 1) * GRID_W, REACH * GRID_W),
     )
+    ctx_pairs, query = lax.optimization_barrier((ctx_pairs, query))
+    ctx_line = jnp.stack(ctx_pairs)
+    below = lax.ppermute(ctx_line, "sp", shifted(sp_size, 4, 4, 1))
+    above = lax.ppermute(ctx_line, "sp", shifted(sp_size, 4, 4, 3))
     before = lax.ppermute(last, "sp", up)
     after = lax.ppermute(first, "sp", down)
     rows_all = pair.shape[1] // GRID_W * sp_size
+    ctx_pairs = [
+        ctx_line,
+        below,
+        above,
+        lax.ppermute(below[:2], "sp", shifted(sp_size, 4, 4, 1)),
+        lax.ppermute(above[2:], "sp", shifted(sp_size, 4, 4, 3)),
+    ]
     attended = attend(
-        place, query, before, pair, after, ctx_keys, ctx_values, table, cb, rows_all, 2
+        place, query, before, pair, after, ctx_pairs, table, cb, rows_all, 2
     )
     attended = attended.reshape(tp_size, samples * tokens_dev, local_cols)
     attended = lax.all_to_all(attended, "tp", 0, 0, tiled=True)
-    return finish(attended, w_out_all, latent, modulation)
+    return finish(attended, w_out_all, latent, modulation, 4)
 
 
 def solution(mesh):

time: 142 us -> 133 us (0.937)
  the two profiles are of different devices: /device:TPU:1 before, /device:TPU:32 now
where the time goes in v6:
time: 133 us; the launch traced here: 131 us
  Pallas kernels  38.5 us (29%)
  blocking collectives  25.4 us (19%)
  waiting for transfers between devices  25.1 us (19%)
  starting transfers between devices  24.3 us (18%)
  between operations  13.5 us (10%)
  local copies, waits for them, and re-layouts  4.31 us (3%)
    pallas_call x1, Pallas kernels, attend(): pl.pallas_call(body, grid=(samples, rows_dev // per), in_specs=[pl.BlockS...  17 us
    ppermute x1, waiting for transfers between devices, computation(): below = lax.ppermute(ctx_line, 'sp', shifted(sp_size, 4, 4, 1))  15.3 us
    all_to_all x1, blocking collectives, computation(): attended = lax.all_to_all(attended, 'tp', 0, 0, tiled=True)  14.5 us
    pallas_call x2, Pallas kernels, project(): pl.pallas_call(body, grid=(samples, steps), in_specs=[blocks(width), whol...  11.5 us
    all_to_all x1, blocking collectives, copy_for_each(): lax.all_to_all(jnp.broadcast_to(shard[None], (length, *shard.shape)), axi...  10.9 us
    all_to_all x1, starting transfers between devices, computation(): summed = jnp.sum(lax.all_to_all(parts, 'sp', 0, 0, tiled=True), axis=0)  7.91 us
    pallas_call x1, Pallas kernels, finish(): pl.pallas_call(body, grid=(width // block,), in_specs=[whole(attended.sha...  5.24 us
    ppermute x1, waiting for transfers between devices, computation(): lax.ppermute(below[:2], 'sp', shifted(sp_size, 4, 4, 1))  4.77 us
  transfers between devices with their start and end apart: 12, of which 5 were waited for; matrix products, arithmetic and copies ran while one was open for 3% of the time, Pallas kernels for 25%

profile of v6, /device:TPU:32, one launch (start us, length us, event | category | flops | bytes accessed | tf_op | source)
XLA Modules:
  0.0 131.3 jit_solution(17855574813863864751)
XLA Ops:
  6.5 0.0 all-gather.3.cloned.1.call-start
  6.5 0.7 all-gather.3.cloned.1.call-update
  7.3 0.0 all-gather.5.cloned.1.call-start
  7.3 1.3 broadcast_in_dim.20.ctx_ref
  8.6 1.7 %modulation_parts.1 = f32[16,8,256]{2,1,0:T(8,128)} custom-call(s32[1]{0:T(128)} %bitcast.place_ref, bf16[2,2048]{1,0:T(2,128)(2,1)} %cond_ref.1, bf16[1,2048]{1,0:T(2,128)(2,1)} %broadcast_in_dim.20.ctx_ref, bf16[128,256]{1,0:T(8,128)(2,1)} %shift_ref.1, bf16[128,256]{1,0:T(8,128)(2,1)} %scale_ref.1, bf16[128,256]{1,0:T(8,128)(2,1)} %gate_ref.1), custom_call_target="tpu_custom_call" | custom-call | tf_op jit(solution)/shard_map/modulation_parts/pallas_call | solution.py:51
  10.3 0.0 all-gather.5.cloned.1.call-update
  10.4 7.9 %all-to-all-start = ((f32[16,8,256]{2,1,0:T(8,128)}), f32[16,8,256]{2,1,0:T(8,128)S(1)}, u32[]{:S(2)}, u32[]{:S(2)}) async-start(f32[16,8,256]{2,1,0:T(8,128)} %modulation_parts.1), calls=%async_computation | async-start | bytes 262144 | tf_op jit(solution)/shard_map/all_to_all | solution.py:375
  18.3 0.8 copy.18
  19.0 0.6 pad.4.clone
  19.6 3.0 %bias_table.1.refs_5_ = f32[2,256,896]{2,1,0:T(8,128)} custom-call(f32[64,128]{1,0:T(8,128)} %bitcast.16), custom_call_target="tpu_custom_call" | custom-call | tf_op jit(solution)/shard_map/bias_table/pallas_call | solution.py:173
  22.6 0.0 copy-done.8
  22.6 0.1 broadcast_in_dim.21
  22.7 0.1 broadcast_in_dim_reshape.3
  22.8 1.8 %all-to-all-done = f32[16,8,256]{2,1,0:T(8,128)S(1)} async-done(((f32[16,8,256]{2,1,0:T(8,128)}), f32[16,8,256]{2,1,0:T(8,128)S(1)}, u32[]{:S(2)}, u32[]{:S(2)}) %all-to-all-start) | async-done | bytes 131104 | tf_op jit(solution)/shard_map/all_to_all | solution.py:375
  24.6 10.9 %all_to_all.15.tiles_ref.tile_ref = f32[8,8,256]{2,1,0:T(8,128)} all-to-all(f32[8,8,256]{2,1,0:T(8,128)S(1)} %broadcast_in_dim.22), channel_id=1, replica_groups=mesh['sp'=16,'tp'=8] {'tp'}, dimensions={0} | all-to-all | bytes 131072 | tf_op jit(solution)/shard_map/all_to_all | solution.py:21
  35.5 3.0 %project.2 = bf16[1,128,512]{2,1,0:T(8,128)(2,1)} custom-call(bf16[1,128,2048]{2,1,0:T(8,128)(2,1)} %bitcast.11, f32[1,2048]{1,0:T(1,128)} %bitcast.20, f32[8,8,256]{2,1,0:T(8,128)} %all_to_all.15.tiles_ref.tile_ref, bf16[2048,256]{1,0:T(8,128)(2,1)} %refs_0_.3, bf16[2048,256]{1,0:T(8,128)(2,1)} %refs_1_.3), custom_call_target="tpu_custom_call" | custom-call | tf_op jit(solution)/shard_map/project/pallas_call | solution.py:132
  38.6 0.5 collective-permute-start
  39.1 2.2 %collective-permute-start.1 = (bf16[2,64,512]{2,1,0:T(8,128)(2,1)}, bf16[2,64,512]{2,1,0:T(8,128)(2,1)S(1)}, u32[]{:S(2)}, u32[]{:S(2)}) collective-permute-start(bf16[2,64,512]{2,1,0:T(8,128)(2,1)} %bitcast.13), channel_id=1, source_target_pairs={{0,16},{8,24},{16,0},{24,8},{32,48},{40,56},{48,32},{56,40},{64,80... | collective-permute-start | bytes 393224 | tf_op jit(solution)/shard_map/ppermute | solution.py:344
  41.3 1.4 %collective-permute-start.2 = (bf16[2,64,512]{2,1,0:T(8,128)(2,1)}, bf16[2,64,512]{2,1,0:T(8,128)(2,1)S(1)}, u32[]{:S(2)}, u32[]{:S(2)}) collective-permute-start(bf16[2,64,512]{2,1,0:T(8,128)(2,1)} %bitcast.14), channel_id=1, source_target_pairs={{0,24},{8,0},{16,8},{24,16},{32,56},{40,32},{48,40},{56,48},{64,88... | collective-permute-start | bytes 393224 | tf_op jit(solution)/shard_map/ppermute | solution.py:344
  42.7 1.1 all-gather.3.cloned.1.call-done.rows_ref
  43.8 8.5 %project.3 = (bf16[2,512,512]{2,1,0:T(8,128)(2,1)}, bf16[2,512,256]{2,1,0:T(8,128)(2,1)}, bf16[2,192,512]{2,1,0:T(8,128)(2,1)}, bf16[2,256,512]{2,1,0:T(8,128)(2,1)}) custom-call(bf16[2,512,2048]{2,1,0:T(8,128)(2,1)} %all-gather.3.cloned.1.call-done.rows_ref, f32[1,2048]{1,0:T(1,128)} %bitcast.21, f32[8,8,256]{2,1,0:T(8,128)} %all_to_all.15.tiles_ref.tile_ref, ...), custom_call_target="tpu_custom_call" | custom-call | tf_op jit(solution)/shard_map/project/pallas_call | solution.py:132
  52.3 0.0 collective-permute-done
  52.3 0.0 collective-permute-done.1
  52.3 0.0 collective-permute-done.2
  52.4 0.0 copy-done.4
  52.4 0.1 pad_maximum_fusion.refs_0_
  52.4 0.0 copy-start
  52.5 1.6 %collective-permute-start.5 = (bf16[4,2,64,512]{3,2,1,0:T(8,128)(2,1)S(1)}, bf16[4,2,64,512]{3,2,1,0:T(8,128)(2,1)S(1)}, u32[]{:S(2)}, u32[]{:S(2)}) collective-permute-start(bf16[4,2,64,512]{3,2,1,0:T(8,128)(2,1)S(1)} %pad_maximum_fusion.refs_0_), channel_id=1, source_target_pairs={{0,32},{8,40},{16,48},{24,56},{32,64},{40,72},{48,80},{56,88},{64,... | collective-permute-start | bytes 1572872 | tf_op jit(solution)/shard_map/ppermute | solution.py:405
  54.1 0.5 collective-permute-start.6
  54.5 3.4 %collective-permute-start.3 = (bf16[2,256,512]{2,1,0:T(8,128)(2,1)}, bf16[2,256,512]{2,1,0:T(8,128)(2,1)S(1)}, u32[]{:S(2)}, u32[]{:S(2)}) collective-permute-start(bf16[2,256,512]{2,1,0:T(8,128)(2,1)} %get-tuple-element.23), channel_id=1, source_target_pairs={{0,8},{8,16},{16,24},{24,32},{32,40},{40,48},{48,56},{56,64},{64,7... | collective-permute-start | bytes 1572872 | tf_op jit(solution)/shard_map/ppermute | solution.py:407
  57.9 4.6 %collective-permute-start.4 = (bf16[2,192,512]{2,1,0:T(8,128)(2,1)}, bf16[2,192,512]{2,1,0:T(8,128)(2,1)S(1)}, u32[]{:S(2)}, u32[]{:S(2)}) collective-permute-start(bf16[2,192,512]{2,1,0:T(8,128)(2,1)} %get-tuple-element.25), channel_id=1, source_target_pairs={{8,0},{16,8},{24,16},{32,24},{40,32},{48,40},{56,48},{64,56},{72,6... | collective-permute-start | bytes 1179656 | tf_op jit(solution)/shard_map/ppermute | solution.py:408
  62.5 15.3 %collective-permute-done.5.refs_1_ = bf16[4,2,64,512]{3,2,1,0:T(8,128)(2,1)S(1)} collective-permute-done((bf16[4,2,64,512]{3,2,1,0:T(8,128)(2,1)S(1)}, bf16[4,2,64,512]{3,2,1,0:T(8,128)(2,1)S(1)}, u32[]{:S(2)}, u32[]{:S(2)}) %collective-permute-start.5) | collective-permute-done | bytes 524320 | tf_op jit(solution)/shard_map/ppermute | solution.py:405
  77.9 1.6 %collective-permute-start.7 = (bf16[2,2,64,512]{3,2,1,0:T(8,128)(2,1)S(1)}, bf16[2,2,64,512]{3,2,1,0:T(8,128)(2,1)S(1)}, u32[]{:S(2)}, u32[]{:S(2)}) collective-permute-start(bf16[2,2,64,512]{3,2,1,0:T(8,128)(2,1)S(1)} %slice.8), channel_id=1, source_target_pairs={{0,32},{8,40},{16,48},{24,56},{32,64},{40,72},{48,80},{56,88},{64,... | collective-permute-start | bytes 786440 | tf_op jit(solution)/shard_map/ppermute | solution.py:414
  79.5 0.0 collective-permute-done.6.refs_2_
  79.5 0.5 collective-permute-start.8
  80.0 0.8 copy.17.refs_6_
  80.8 0.0 collective-permute-done.4.after_ref
  80.8 0.0 collective-permute-done.3.before_ref
  80.8 4.8 %collective-permute-done.7.refs_3_ = bf16[2,2,64,512]{3,2,1,0:T(8,128)(2,1)S(1)} collective-permute-done((bf16[2,2,64,512]{3,2,1,0:T(8,128)(2,1)S(1)}, bf16[2,2,64,512]{3,2,1,0:T(8,128)(2,1)S(1)}, u32[]{:S(2)}, u32[]{:S(2)}) %collective-permute-start.7) | collective-permute-done | bytes 262176 | tf_op jit(solution)/shard_map/ppermute | solution.py:414
  85.6 1.4 %collective-permute-done.8.refs_4_ = bf16[2,2,64,512]{3,2,1,0:T(8,128)(2,1)S(1)} collective-permute-done((bf16[2,2,64,512]{3,2,1,0:T(8,128)(2,1)S(1)}, bf16[2,2,64,512]{3,2,1,0:T(8,128)(2,1)S(1)}, u32[]{:S(2)}, u32[]{:S(2)}) %collective-permute-start.8) | collective-permute-done | bytes 262176 | tf_op jit(solution)/shard_map/ppermute | solution.py:415
  87.0 0.0 copy-done.1
  87.0 0.0 copy-done.5
  87.0 0.0 copy-done.3
  87.0 0.0 copy-done.6
  87.0 0.7 copy-done.7
  87.7 17.0 %attend.1 = bf16[8,2,64,256]{3,2,1,0:T(8,128)(2,1)} custom-call(s32[1]{0:T(128)} %bitcast.place_ref, bf16[2,512,256]{2,1,0:T(8,128)(2,1)} %get-tuple-element.22.q_ref, bf16[2,256,512]{2,1,0:T(8,128)(2,1)} %copy-done.3, bf16[2,512,512]{2,1,0:T(8,128)(2,1)} %get-tuple-element.24.pair_ref, bf16[2,192,512]{2,1,0:T(8,128)(2,1)} %copy-done.5, ...), custom_call_target="tpu_custom_call" | custom-call | tf_op jit(solution)/shard_map/attend/pallas_call | solution.py:280
  104.7 14.5 %all_to_all.16.att_ref = bf16[8,128,256]{2,1,0:T(8,128)(2,1)} all-to-all(bf16[8,128,256]{2,1,0:T(8,128)(2,1)} %bitcast.10), channel_id=1, replica_groups=mesh['sp'=16,'tp'=8] {'tp'}, dimensions={0} | all-to-all | bytes 1048576 | tf_op jit(solution)/shard_map/all_to_all | solution.py:421
  119.2 5.2 %finish.1 = bf16[2,64,2048]{2,1,0:T(8,128)(2,1)} custom-call(bf16[8,128,256]{2,1,0:T(8,128)(2,1)} %all_to_all.16.att_ref, bf16[2048,2048]{1,0:T(8,128)(2,1)} %all-gather.5.cloned.1.call-done.w_ref, bf16[2,64,2048]{2,1,0:T(8,128)(2,1)} %latent_ref.1, f32[8,8,256]{2,1,0:T(8,128)} %all_to_all.15.tiles_ref.tile_ref), custom_call_target="tpu_custom_call" | custom-call | tf_op jit(solution)/shard_map/finish/pallas_call | solution.py:321
  (15 shorter events, 0.1 us)
Async XLA Ops:
  6.5 16.1 %copy-start.8 = (f32[4]{0:T(128)S(1)}, f32[4]{0:T(128)}, u32[]{:S(2)}) copy-start(f32[4]{0:T(128)} %param.27) | copy-start | bytes 52
  6.5 37.3 %all-gather.3.cloned.1.call-start = ((), (), s32[]{:S(2)}) async-start(), calls=%async_computation.3 | async-start | bytes 4718592 | tf_op jit(solution)/shard_map/all_gather | solution.py:369
  7.3 111.9 %all-gather.5.cloned.1.call-start = ((), (), s32[]{:S(2)}) async-start(), calls=%async_computation.4 | async-start | bytes 9437184 | tf_op jit(solution)/shard_map/all_gather | solution.py:372
  10.4 14.2 %all-to-all-start = ((f32[16,8,256]{2,1,0:T(8,128)}), f32[16,8,256]{2,1,0:T(8,128)S(1)}, u32[]{:S(2)}, u32[]{:S(2)}) async-start(f32[16,8,256]{2,1,0:T(8,128)} %modulation_parts.1), calls=%async_computation | async-start | bytes 262144 | tf_op jit(solution)/shard_map/all_to_all | solution.py:375
  38.6 13.8 %copy-start.4 = (bf16[1,128,512]{2,1,0:T(8,128)(2,1)S(1)}, bf16[1,128,512]{2,1,0:T(8,128)(2,1)}, u32[]{:S(2)}) copy-start(bf16[1,128,512]{2,1,0:T(8,128)(2,1)} %project.2) | copy-start | bytes 393220
  38.6 13.8 %collective-permute-start = (bf16[2,64,512]{2,1,0:T(8,128)(2,1)}, bf16[2,64,512]{2,1,0:T(8,128)(2,1)S(1)}, u32[]{:S(2)}, u32[]{:S(2)}) collective-permute-start(bf16[2,64,512]{2,1,0:T(8,128)(2,1)} %bitcast.12), channel_id=1, source_target_pairs={{0,8},{8,16},{16,24},{24,0},{32,40},{40,48},{48,56},{56,32},{64,72... | collective-permute-start | bytes 393224 | tf_op jit(solution)/shard_map/ppermute | solution.py:344
  39.1 13.3 %collective-permute-start.1 = (bf16[2,64,512]{2,1,0:T(8,128)(2,1)}, bf16[2,64,512]{2,1,0:T(8,128)(2,1)S(1)}, u32[]{:S(2)}, u32[]{:S(2)}) collective-permute-start(bf16[2,64,512]{2,1,0:T(8,128)(2,1)} %bitcast.13), channel_id=1, source_target_pairs={{0,16},{8,24},{16,0},{24,8},{32,48},{40,56},{48,32},{56,40},{64,80... | collective-permute-start | bytes 393224 | tf_op jit(solution)/shard_map/ppermute | solution.py:344
  41.3 11.1 %collective-permute-start.2 = (bf16[2,64,512]{2,1,0:T(8,128)(2,1)}, bf16[2,64,512]{2,1,0:T(8,128)(2,1)S(1)}, u32[]{:S(2)}, u32[]{:S(2)}) collective-permute-start(bf16[2,64,512]{2,1,0:T(8,128)(2,1)} %bitcast.14), channel_id=1, source_target_pairs={{0,24},{8,0},{16,8},{24,16},{32,56},{40,32},{48,40},{56,48},{64,88... | collective-permute-start | bytes 393224 | tf_op jit(solution)/shard_map/ppermute | solution.py:344
  52.4 34.5 %copy-start = (bf16[4,2,64,512]{3,2,1,0:T(8,128)(2,1)}, bf16[4,2,64,512]{3,2,1,0:T(8,128)(2,1)S(1)}, u32[]{:S(2)}) copy-start(bf16[4,2,64,512]{3,2,1,0:T(8,128)(2,1)S(1)} %pad_maximum_fusion.refs_0_) | copy-start | bytes 1572868
  52.5 25.4 %collective-permute-start.5 = (bf16[4,2,64,512]{3,2,1,0:T(8,128)(2,1)S(1)}, bf16[4,2,64,512]{3,2,1,0:T(8,128)(2,1)S(1)}, u32[]{:S(2)}, u32[]{:S(2)}) collective-permute-start(bf16[4,2,64,512]{3,2,1,0:T(8,128)(2,1)S(1)} %pad_maximum_fusion.refs_0_), channel_id=1, source_target_pairs={{0,32},{8,40},{16,48},{24,56},{32,64},{40,72},{48,80},{56,88},{64,... | collective-permute-start | bytes 1572872 | tf_op jit(solution)/shard_map/ppermute | solution.py:405
  54.1 25.4 %collective-permute-start.6 = (bf16[4,2,64,512]{3,2,1,0:T(8,128)(2,1)S(1)}, bf16[4,2,64,512]{3,2,1,0:T(8,128)(2,1)S(1)}, u32[]{:S(2)}, u32[]{:S(2)}) collective-permute-start(bf16[4,2,64,512]{3,2,1,0:T(8,128)(2,1)S(1)} %pad_maximum_fusion.refs_0_), channel_id=1, source_target_pairs={{0,96},{8,104},{16,112},{24,120},{32,0},{40,8},{48,16},{56,24},{64... | collective-permute-start | bytes 1572872 | tf_op jit(solution)/shard_map/ppermute | solution.py:406
  54.5 26.3 %collective-permute-start.3 = (bf16[2,256,512]{2,1,0:T(8,128)(2,1)}, bf16[2,256,512]{2,1,0:T(8,128)(2,1)S(1)}, u32[]{:S(2)}, u32[]{:S(2)}) collective-permute-start(bf16[2,256,512]{2,1,0:T(8,128)(2,1)} %get-tuple-element.23), channel_id=1, source_target_pairs={{0,8},{8,16},{16,24},{24,32},{32,40},{40,48},{48,56},{56,64},{64,7... | collective-permute-start | bytes 1572872 | tf_op jit(solution)/shard_map/ppermute | solution.py:407
  57.9 22.9 %collective-permute-start.4 = (bf16[2,192,512]{2,1,0:T(8,128)(2,1)}, bf16[2,192,512]{2,1,0:T(8,128)(2,1)S(1)}, u32[]{:S(2)}, u32[]{:S(2)}) collective-permute-start(bf16[2,192,512]{2,1,0:T(8,128)(2,1)} %get-tuple-element.25), channel_id=1, source_target_pairs={{8,0},{16,8},{24,16},{32,24},{40,32},{48,40},{56,48},{64,56},{72,6... | collective-permute-start | bytes 1179656 | tf_op jit(solution)/shard_map/ppermute | solution.py:408
  77.8 9.2 %copy-start.1 = (bf16[4,2,64,512]{3,2,1,0:T(8,128)(2,1)}, bf16[4,2,64,512]{3,2,1,0:T(8,128)(2,1)S(1)}, u32[]{:S(2)}) copy-start(bf16[4,2,64,512]{3,2,1,0:T(8,128)(2,1)S(1)} %collective-permute-done.5.refs_1_) | copy-start | bytes 1572868
  77.9 7.8 %collective-permute-start.7 = (bf16[2,2,64,512]{3,2,1,0:T(8,128)(2,1)S(1)}, bf16[2,2,64,512]{3,2,1,0:T(8,128)(2,1)S(1)}, u32[]{:S(2)}, u32[]{:S(2)}) collective-permute-start(bf16[2,2,64,512]{3,2,1,0:T(8,128)(2,1)S(1)} %slice.8), channel_id=1, source_target_pairs={{0,32},{8,40},{16,48},{24,56},{32,64},{40,72},{48,80},{56,88},{64,... | collective-permute-start | bytes 786440 | tf_op jit(solution)/shard_map/ppermute | solution.py:414
  79.5 7.5 %copy-start.2 = (bf16[4,2,64,512]{3,2,1,0:T(8,128)(2,1)}, bf16[4,2,64,512]{3,2,1,0:T(8,128)(2,1)S(1)}, u32[]{:S(2)}) copy-start(bf16[4,2,64,512]{3,2,1,0:T(8,128)(2,1)S(1)} %collective-permute-done.6.refs_2_) | copy-start | bytes 1572868
  79.5 7.5 %collective-permute-start.8 = (bf16[2,2,64,512]{3,2,1,0:T(8,128)(2,1)S(1)}, bf16[2,2,64,512]{3,2,1,0:T(8,128)(2,1)S(1)}, u32[]{:S(2)}, u32[]{:S(2)}) collective-permute-start(bf16[2,2,64,512]{3,2,1,0:T(8,128)(2,1)S(1)} %slice.9), channel_id=1, source_target_pairs={{0,96},{8,104},{16,112},{24,120},{32,0},{40,8},{48,16},{56,24},{64... | collective-permute-start | bytes 786440 | tf_op jit(solution)/shard_map/ppermute | solution.py:415
  80.8 6.2 %copy-start.5 = (bf16[2,192,512]{2,1,0:T(8,128)(2,1)}, bf16[2,192,512]{2,1,0:T(8,128)(2,1)S(1)}, u32[]{:S(2)}) copy-start(bf16[2,192,512]{2,1,0:T(8,128)(2,1)S(1)} %collective-permute-done.4.after_ref) | copy-start | bytes 1179652
  80.8 6.2 %copy-start.3 = (bf16[2,256,512]{2,1,0:T(8,128)(2,1)}, bf16[2,256,512]{2,1,0:T(8,128)(2,1)S(1)}, u32[]{:S(2)}) copy-start(bf16[2,256,512]{2,1,0:T(8,128)(2,1)S(1)} %collective-permute-done.3.before_ref) | copy-start | bytes 1572868
  85.6 1.4 %copy-start.6 = (bf16[2,2,64,512]{3,2,1,0:T(8,128)(2,1)}, bf16[2,2,64,512]{3,2,1,0:T(8,128)(2,1)S(1)}, u32[]{:S(2)}) copy-start(bf16[2,2,64,512]{3,2,1,0:T(8,128)(2,1)S(1)} %collective-permute-done.7.refs_3_) | copy-start | bytes 786436
  87.0 0.7 copy-start.7
Sparse Core Ops, SparseCore 0:
  9.0 34.7 all-gather.2
  45.6 49.5 all-gather.4

commit v7 on v6

--- a/solution.py
+++ b/solution.py
@@ -31,10 +31,11 @@
     samples = cond.shape[0]
     rows, cols = weights[0].shape
 
-    def body(place_ref, cond_ref, ctx_ref, shift_ref, scale_ref, gate_ref, out_ref):
+    def body(place_ref, cond_ref, ctx_ref, shift_ref, scale_ref, gate_ref, out_ref, wide):
         at = pl.multiple_of(place_ref[0] * rows, rows)
         ada = silu_rows(cond_ref[:, pl.ds(at, rows)])
-        ada_ctx = silu_rows(ctx_ref[:, pl.ds(at, rows)])
+        wide[...] = ctx_ref[...].astype(jnp.float32).reshape(1, ctx_ref.shape[0])
+        ada_ctx = silu_rows(wide[:, pl.ds(at, rows)])
         both = jnp.concatenate([ada.astype(jnp.float32), ada_ctx.astype(jnp.float32)], axis=0)
         both = both.astype(jnp.bfloat16)
         result = jnp.concatenate(
@@ -53,6 +54,7 @@
         in_specs=[pl.BlockSpec(memory_space=pltpu.SMEM)]
         + [pl.BlockSpec(memory_space=pltpu.VMEM)] * 5,
         out_shape=jax.ShapeDtypeStruct((copies, 3 * samples + 2, cols), jnp.float32),
+        scratch_shapes=[pltpu.VMEM((1, ctx_cond.shape[0]), jnp.float32)],
         name="modulation_parts",
     )(place, cond, ctx_cond, *weights)
 
@@ -65,21 +67,23 @@
     return jnp.concatenate([tiles[tile, row : row + 1, :] for tile in range(tiles.shape[0])], axis=1)
 
 
-def project(rows, gain, modulation, weights, row_of, block, ends):
+def project(rows, gain, modulation, weights, row_of, block, ends, sample=None, buffers=()):
     samples, count, width = rows.shape
     every = modulation.shape[1] // 3 + 1
+    chosen = range(samples) if sample is None else (sample,)
+    begin = chosen[0]
     cols = weights[0].shape[1]
     first, last = ends if ends else (0, 0)
     steps = count // block
 
     def body(rows_ref, gain_ref, tiles_ref, *refs):
-        weight_refs, out_refs = refs[: len(weights)], refs[len(weights) : -2]
+        weight_refs, out_refs = refs[: len(weights)], refs[len(weights) + len(buffers) : -2]
         factor_ref, shift_ref = refs[-2:]
-        sample, step = pl.program_id(0), pl.program_id(1)
-
-        for number in range(samples):
-
-            @pl.when((sample == number) & (step == 0))
+        turn, step = pl.program_id(0), pl.program_id(1)
+
+        for number in chosen:
+
+            @pl.when((turn == number - begin) & (step == 0))
             def _(number=number):
                 row = row_of + number
                 factor_ref[...] = gain_ref[...] * (1.0 + modulation_row(tiles_ref, every + row))
@@ -118,27 +122,29 @@
                             ] = pair[index][lo - low : hi - low]
 
     def blocks(size):
-        return pl.BlockSpec((1, block, size), lambda s, i: (s, i, 0))
+        return pl.BlockSpec((1, block, size), lambda s, i: (begin + s, i, 0))
 
     if ends:
         out_specs = [blocks(2 * cols), blocks(cols)]
         out_shape = [(samples, count, 2 * cols), (samples, count, cols)]
         for length in ends:
-            out_specs += [pl.BlockSpec((1, length, 2 * cols), lambda s, i: (s, 0, 0))]
+            out_specs += [pl.BlockSpec((1, length, 2 * cols), lambda s, i: (begin + s, 0, 0))]
             out_shape += [(samples, length, 2 * cols)]
     else:
         out_specs = [blocks(2 * cols)]
         out_shape = [(samples, count, 2 * cols)]
     return pl.pallas_call(
         body,
-        grid=(samples, steps),
+        grid=(len(chosen), steps),
         in_specs=[blocks(width), whole((1, width)), whole(modulation.shape)]
-        + [whole(weight.shape) for weight in weights],
+        + [whole(weight.shape) for weight in weights]
+        + [pl.BlockSpec(memory_space=pl.ANY)] * len(buffers),
         out_specs=out_specs,
         out_shape=[jax.ShapeDtypeStruct(shape, jnp.bfloat16) for shape in out_shape],
         scratch_shapes=[pltpu.VMEM((1, width), jnp.float32)] * 2,
+        input_output_aliases={3 + len(weights) + i: i for i in range(len(buffers))},
         name="project",
-    )(rows, gain, modulation, *weights)
+    )(rows, gain, modulation, *weights, *buffers)
 
 
 def bias_table(rel_bias):
@@ -188,7 +194,6 @@
     ctx_rows = ctx_pairs[0].shape[2]
     members = [array.shape[0] for array in ctx_pairs]
     ctx_count = sum(members) * ctx_rows
-    queries = heads * GRID_W
     bf16, f32 = jnp.bfloat16, jnp.float32
 
     def body(place_ref, q_ref, before_ref, pair_ref, after_ref, *refs):
@@ -232,7 +237,9 @@
         base = place_ref[0] * rows_dev
         lane = lax.broadcasted_iota(jnp.int32, (GRID_W, cols), 1)
         masks = [(lane >= h * HEAD_DIM) & (lane < (h + 1) * HEAD_DIM) for h in range(heads)]
-        cb = cb_ref[...]
+        cb = jnp.concatenate(
+            [jnp.full((GRID_W, 1), cb_ref[h], f32) for h in range(heads)], axis=0
+        )
         spreads, nears, starts = [], [], []
         for r in range(per):
             actual = base + step * per + r
@@ -291,7 +298,7 @@
             pl.BlockSpec((count, 1, ctx_rows, 2 * cols), lambda s, i: (0, s, 0, 0))
             for count in members
         ]
-        + [whole(table.shape), whole((queries, 1))],
+        + [whole(table.shape), pl.BlockSpec(memory_space=pltpu.SMEM)],
         out_specs=pl.BlockSpec((per, 1, GRID_W, cols), lambda s, i: (i, s, 0, 0)),
         out_shape=jax.ShapeDtypeStruct((rows_dev, samples, GRID_W, cols), bf16),
         scratch_shapes=[
@@ -367,13 +374,12 @@
     sp_size, tp_size = lax.axis_size("sp"), lax.axis_size("tp")
     place = jnp.full((1,), sp_index, jnp.int32)
     gathered = lax.all_gather(latent, "tp", axis=1, tiled=True)
-    parts = modulation_parts(place, cond, ctx_cond[None], (w_shift, w_scale, w_gate), sp_size)
+    parts = modulation_parts(place, cond, ctx_cond, (w_shift, w_scale, w_gate), sp_size)
     parts, w_out_own = lax.optimization_barrier((parts, w_out))
     w_out_all = lax.all_gather(w_out_own, "tp", axis=0, tiled=True)
     table = bias_table(rel_bias)
-    cb = jnp.repeat(ctx_bias, GRID_W)[:, None]
     summed = jnp.sum(lax.all_to_all(parts, "sp", 0, 0, tiled=True), axis=0)
-    summed, table, cb = lax.optimization_barrier((summed, table, cb))
+    summed, table = lax.optimization_barrier((summed, table))
     modulation = copy_for_each(summed, "tp")
 
     gain = norm_gain[None, :]
@@ -391,19 +397,16 @@
     ctx_pairs = from_line(ctx_pair, "sp", 4, 1)
     up = [(i, i + 1) for i in range(sp_size - 1)]
     down = [(j, i) for i, j in up]
-    pair, query, first, last = project(
-        gathered,
-        gain,
-        modulation,
-        (w_key, w_value, w_query),
-        0,
-        256,
-        ((WIN_ROWS - REACH - 1) * GRID_W, REACH * GRID_W),
-    )
-    ctx_pairs, query = lax.optimization_barrier((ctx_pairs, query))
+    ends = ((WIN_ROWS - REACH - 1) * GRID_W, REACH * GRID_W)
+    w_triple = (w_key, w_value, w_query)
+    outs = project(gathered, gain, modulation, w_triple, 0, 256, ends, 0)
+    ctx_pairs, outs = lax.optimization_barrier((ctx_pairs, outs))
     ctx_line = jnp.stack(ctx_pairs)
     below = lax.ppermute(ctx_line, "sp", shifted(sp_size, 4, 4, 1))
     above = lax.ppermute(ctx_line, "sp", shifted(sp_size, 4, 4, 3))
+    for s in range(1, samples):
+        outs = project(gathered, gain, modulation, w_triple, 0, 256, ends, s, outs)
+    pair, query, first, last = outs
     before = lax.ppermute(last, "sp", up)
     after = lax.ppermute(first, "sp", down)
     rows_all = pair.shape[1] // GRID_W * sp_size
@@ -415,7 +418,7 @@
         lax.ppermute(above[2:], "sp", shifted(sp_size, 4, 4, 3)),
     ]
     attended = attend(
-        place, query, before, pair, after, ctx_pairs, table, cb, rows_all, 2
+        place, query, before, pair, after, ctx_pairs, table, ctx_bias, rows_all, 4
     )
     attended = attended.reshape(tp_size, samples * tokens_dev, local_cols)
     attended = lax.all_to_all(attended, "tp", 0, 0, tiled=True)

time: 133 us -> 126 us (0.947)
  waiting for transfers between devices: 25.1 us -> 18.4 us
  local copies, waits for them, and re-layouts: 4.31 us -> 2.18 us
  Pallas kernels: 38.5 us -> 40.5 us
    ppermute x1, waiting for transfers between devices: 15.3 us -> 0.01 us  [computation(): below = lax.ppermute(ctx_line, 'sp', shifted(sp_size, 4, 4, 1))]
    ppermute x1, waiting for transfers between devices: 0.01 us -> 6.26 us  [computation(): after = lax.ppermute(first, 'sp', down)]
    pallas_call x2 -> x3, Pallas kernels: 11.5 us -> 14.4 us  [project(): pl.pallas_call(body, grid=(len(chosen), steps), in_specs=[blocks(width),...]
    ppermute x1, waiting for transfers between devices: 0.01 us -> 1.58 us  [computation(): before = lax.ppermute(last, 'sp', up)]
    ppermute x1, waiting for transfers between devices: 1.36 us -> 0.01 us  [computation(): lax.ppermute(above[2:], 'sp', shifted(sp_size, 4, 4, 3))]
    broadcast_in_dim x2 -> x0, local copies, waits for them, and re-layouts: 1.35 us -> none  [the longest x1 1.28 us: computation(): ctx_cond[None]]
  transfers between devices with their start and end apart: 12 -> 12, of which waited for: 5 -> 5; matrix products, arithmetic and copies ran while one was open for 3% -> 1% of each run, Pallas kernels for 25% -> 28%
where the time goes in v7:
time: 126 us; the launch traced here: 124 us
  Pallas kernels  40.5 us (32%)
  blocking collectives  25.4 us (20%)
  starting transfers between devices  24.3 us (19%)
  waiting for transfers between devices  18.4 us (15%)
  between operations  13.6 us (11%)
  local copies, waits for them, and re-layouts  2.18 us (2%)
    pallas_call x1, Pallas kernels, attend(): pl.pallas_call(body, grid=(samples, rows_dev // per), in_specs=[pl.BlockS...  16.1 us
    all_to_all x1, blocking collectives, computation(): attended = lax.all_to_all(attended, 'tp', 0, 0, tiled=True)  14.5 us
    pallas_call x3, Pallas kernels, project(): pl.pallas_call(body, grid=(len(chosen), steps), in_specs=[blocks(width),...  14.4 us
    all_to_all x1, blocking collectives, copy_for_each(): lax.all_to_all(jnp.broadcast_to(shard[None], (length, *shard.shape)), axi...  10.9 us
    all_to_all x1, starting transfers between devices, computation(): summed = jnp.sum(lax.all_to_all(parts, 'sp', 0, 0, tiled=True), axis=0)  7.91 us
    ppermute x1, waiting for transfers between devices, computation(): after = lax.ppermute(first, 'sp', down)  6.26 us
    ppermute x1, waiting for transfers between devices, computation(): lax.ppermute(below[:2], 'sp', shifted(sp_size, 4, 4, 1))  5.52 us
    pallas_call x1, Pallas kernels, finish(): pl.pallas_call(body, grid=(width // block,), in_specs=[whole(attended.sha...  5.24 us
  transfers between devices with their start and end apart: 12, of which 5 were waited for; matrix products, arithmetic and copies ran while one was open for 1% of the time, Pallas kernels for 28%

profile of v7, /device:TPU:32, one launch (start us, length us, event | category | flops | bytes accessed | tf_op | source)
XLA Modules:
  0.0 124.5 jit_solution(10442072430723925541)
XLA Ops:
  6.5 0.0 all-gather.3.cloned.1.call-start
  6.5 0.7 all-gather.3.cloned.1.call-update
  7.3 0.0 all-gather.5.cloned.1.call-start
  7.3 1.8 %modulation_parts.1 = f32[16,8,256]{2,1,0:T(8,128)} custom-call(s32[1]{0:T(128)} %bitcast.place_ref, bf16[2,2048]{1,0:T(2,128)(2,1)} %cond_ref.1, bf16[2048]{0:T(1024)(128)(2,1)} %ctx_ref.1, bf16[128,256]{1,0:T(8,128)(2,1)} %shift_ref.1, bf16[128,256]{1,0:T(8,128)(2,1)} %scale_ref.1, bf16[128,256]{1,0:T(8,128)(2,1)} %gate_ref.1), custom_call_target="tpu_custom_call" | custom-call | tf_op jit(solution)/shard_map/modulation_parts/pallas_call | solution.py:52
  9.1 0.0 all-gather.5.cloned.1.call-update
  9.1 7.9 %all-to-all-start = ((f32[16,8,256]{2,1,0:T(8,128)}), f32[16,8,256]{2,1,0:T(8,128)S(1)}, u32[]{:S(2)}, u32[]{:S(2)}) async-start(f32[16,8,256]{2,1,0:T(8,128)} %modulation_parts.1), calls=%async_computation | async-start | bytes 262144 | tf_op jit(solution)/shard_map/all_to_all | solution.py:381
  17.0 0.8 copy.20
  17.8 0.6 pad.4.clone
  18.4 3.0 %bias_table.1.refs_5_ = f32[2,256,896]{2,1,0:T(8,128)} custom-call(f32[64,128]{1,0:T(8,128)} %bitcast.16), custom_call_target="tpu_custom_call" | custom-call | tf_op jit(solution)/shard_map/bias_table/pallas_call | solution.py:179
  21.4 1.9 %all-to-all-done = f32[16,8,256]{2,1,0:T(8,128)S(1)} async-done(((f32[16,8,256]{2,1,0:T(8,128)}), f32[16,8,256]{2,1,0:T(8,128)S(1)}, u32[]{:S(2)}, u32[]{:S(2)}) %all-to-all-start) | async-done | bytes 131104 | tf_op jit(solution)/shard_map/all_to_all | solution.py:381
  23.3 10.9 %all_to_all.15.tiles_ref.tile_ref = f32[8,8,256]{2,1,0:T(8,128)} all-to-all(f32[8,8,256]{2,1,0:T(8,128)S(1)} %broadcast_in_dim.14), channel_id=1, replica_groups=mesh['sp'=16,'tp'=8] {'tp'}, dimensions={0} | all-to-all | bytes 131072 | tf_op jit(solution)/shard_map/all_to_all | solution.py:21
  34.2 3.1 %project.3 = bf16[1,128,512]{2,1,0:T(8,128)(2,1)} custom-call(bf16[1,128,2048]{2,1,0:T(8,128)(2,1)} %bitcast.11, f32[1,2048]{1,0:T(1,128)} %bitcast.20, f32[8,8,256]{2,1,0:T(8,128)} %all_to_all.15.tiles_ref.tile_ref, bf16[2048,256]{1,0:T(8,128)(2,1)} %refs_0_.5, bf16[2048,256]{1,0:T(8,128)(2,1)} %refs_1_.5), custom_call_target="tpu_custom_call" | custom-call | tf_op jit(solution)/shard_map/project/pallas_call | solution.py:136
  37.3 0.0 copy-start.4
  37.3 0.5 collective-permute-start
  37.8 2.2 %collective-permute-start.1 = (bf16[2,64,512]{2,1,0:T(8,128)(2,1)}, bf16[2,64,512]{2,1,0:T(8,128)(2,1)S(1)}, u32[]{:S(2)}, u32[]{:S(2)}) collective-permute-start(bf16[2,64,512]{2,1,0:T(8,128)(2,1)} %bitcast.13), channel_id=1, source_target_pairs={{0,16},{8,24},{16,0},{24,8},{32,48},{40,56},{48,32},{56,40},{64,80... | collective-permute-start | bytes 393224 | tf_op jit(solution)/shard_map/ppermute | solution.py:351
  40.0 1.4 %collective-permute-start.2 = (bf16[2,64,512]{2,1,0:T(8,128)(2,1)}, bf16[2,64,512]{2,1,0:T(8,128)(2,1)S(1)}, u32[]{:S(2)}, u32[]{:S(2)}) collective-permute-start(bf16[2,64,512]{2,1,0:T(8,128)(2,1)} %bitcast.14), channel_id=1, source_target_pairs={{0,24},{8,0},{16,8},{24,16},{32,56},{40,32},{48,40},{56,48},{64,88... | collective-permute-start | bytes 393224 | tf_op jit(solution)/shard_map/ppermute | solution.py:351
  41.4 2.4 %all-gather.3.cloned.1.call-done.rows_ref = bf16[2,512,2048]{2,1,0:T(8,128)(2,1)} async-done(((bf16[2,64,2048]{2,1,0:T(8,128)(2,1)}), bf16[2,512,2048]{2,1,0:T(8,128)(2,1)}) %all-gather.3.cloned.1.call-update) | async-done | bytes 4194320 | tf_op jit(solution)/shard_map/all_gather | solution.py:376
  43.8 5.7 %project.4 = (bf16[2,512,512]{2,1,0:T(8,128)(2,1)}, bf16[2,512,256]{2,1,0:T(8,128)(2,1)}, bf16[2,192,512]{2,1,0:T(8,128)(2,1)}, bf16[2,256,512]{2,1,0:T(8,128)(2,1)}) custom-call(bf16[2,512,2048]{2,1,0:T(8,128)(2,1)} %all-gather.3.cloned.1.call-done.rows_ref, f32[1,2048]{1,0:T(1,128)} %bitcast.21, f32[8,8,256]{2,1,0:T(8,128)} %all_to_all.15.tiles_ref.tile_ref, ...), custom_call_target="tpu_custom_call" | custom-call | tf_op jit(solution)/shard_map/project/pallas_call | solution.py:136
  49.5 0.0 collective-permute-done
  49.5 0.0 collective-permute-done.1
  49.5 0.0 collective-permute-done.2
  49.5 0.0 copy-done.4
  49.5 0.1 pad_maximum_fusion.refs_0_
  49.6 0.0 copy-start
  49.6 1.6 %collective-permute-start.5 = (bf16[4,2,64,512]{3,2,1,0:T(8,128)(2,1)S(1)}, bf16[4,2,64,512]{3,2,1,0:T(8,128)(2,1)S(1)}, u32[]{:S(2)}, u32[]{:S(2)}) collective-permute-start(bf16[4,2,64,512]{3,2,1,0:T(8,128)(2,1)S(1)} %pad_maximum_fusion.refs_0_), channel_id=1, source_target_pairs={{0,32},{8,40},{16,48},{24,56},{32,64},{40,72},{48,80},{56,88},{64,... | collective-permute-start | bytes 1572872 | tf_op jit(solution)/shard_map/ppermute | solution.py:405
  51.2 0.5 collective-permute-start.6
  51.7 5.7 %project.5 = (bf16[2,512,512]{2,1,0:T(8,128)(2,1)}, bf16[2,512,256]{2,1,0:T(8,128)(2,1)}, bf16[2,192,512]{2,1,0:T(8,128)(2,1)}, bf16[2,256,512]{2,1,0:T(8,128)(2,1)}) custom-call(bf16[2,512,2048]{2,1,0:T(8,128)(2,1)} %all-gather.3.cloned.1.call-done.rows_ref, ...), custom_call_target="tpu_custom_call", output_to_operand_aliasing={{0}: (6, {}), {1}: (7, {}), {2}: (8, {}), {3}: (9, {})} | custom-call | tf_op jit(solution)/shard_map/project/pallas_call | solution.py:136
  57.4 0.0 copy-done
  57.4 3.4 %collective-permute-start.3 = (bf16[2,256,512]{2,1,0:T(8,128)(2,1)}, bf16[2,256,512]{2,1,0:T(8,128)(2,1)S(1)}, u32[]{:S(2)}, u32[]{:S(2)}) collective-permute-start(bf16[2,256,512]{2,1,0:T(8,128)(2,1)} %get-tuple-element.36), channel_id=1, source_target_pairs={{0,8},{8,16},{16,24},{24,32},{32,40},{40,48},{48,56},{56,64},{64,7... | collective-permute-start | bytes 1572872 | tf_op jit(solution)/shard_map/ppermute | solution.py:410
  60.8 4.6 %collective-permute-start.4 = (bf16[2,192,512]{2,1,0:T(8,128)(2,1)}, bf16[2,192,512]{2,1,0:T(8,128)(2,1)S(1)}, u32[]{:S(2)}, u32[]{:S(2)}) collective-permute-start(bf16[2,192,512]{2,1,0:T(8,128)(2,1)} %get-tuple-element.38), channel_id=1, source_target_pairs={{8,0},{16,8},{24,16},{32,24},{40,32},{48,40},{56,48},{64,56},{72,6... | collective-permute-start | bytes 1179656 | tf_op jit(solution)/shard_map/ppermute | solution.py:411
  65.4 0.0 collective-permute-done.5.refs_1_
  65.4 0.0 copy-start.1
  65.4 1.6 %collective-permute-start.7 = (bf16[2,2,64,512]{3,2,1,0:T(8,128)(2,1)S(1)}, bf16[2,2,64,512]{3,2,1,0:T(8,128)(2,1)S(1)}, u32[]{:S(2)}, u32[]{:S(2)}) collective-permute-start(bf16[2,2,64,512]{3,2,1,0:T(8,128)(2,1)S(1)} %slice.8), channel_id=1, source_target_pairs={{0,32},{8,40},{16,48},{24,56},{32,64},{40,72},{48,80},{56,88},{64,... | collective-permute-start | bytes 786440 | tf_op jit(solution)/shard_map/ppermute | solution.py:417
  67.0 0.0 collective-permute-done.6.refs_2_
  67.1 0.5 collective-permute-start.8
  67.6 6.3 %collective-permute-done.4.after_ref = bf16[2,192,512]{2,1,0:T(8,128)(2,1)S(1)} collective-permute-done((bf16[2,192,512]{2,1,0:T(8,128)(2,1)}, bf16[2,192,512]{2,1,0:T(8,128)(2,1)S(1)}, u32[]{:S(2)}, u32[]{:S(2)}) %collective-permute-start.4) | collective-permute-done | bytes 393248 | tf_op jit(solution)/shard_map/ppermute | solution.py:411
  73.9 1.6 %collective-permute-done.3.before_ref = bf16[2,256,512]{2,1,0:T(8,128)(2,1)S(1)} collective-permute-done((bf16[2,256,512]{2,1,0:T(8,128)(2,1)}, bf16[2,256,512]{2,1,0:T(8,128)(2,1)S(1)}, u32[]{:S(2)}, u32[]{:S(2)}) %collective-permute-start.3) | collective-permute-done | bytes 524320 | tf_op jit(solution)/shard_map/ppermute | solution.py:410
  75.5 5.5 %collective-permute-done.7.refs_3_ = bf16[2,2,64,512]{3,2,1,0:T(8,128)(2,1)S(1)} collective-permute-done((bf16[2,2,64,512]{3,2,1,0:T(8,128)(2,1)S(1)}, bf16[2,2,64,512]{3,2,1,0:T(8,128)(2,1)S(1)}, u32[]{:S(2)}, u32[]{:S(2)}) %collective-permute-start.7) | collective-permute-done | bytes 262176 | tf_op jit(solution)/shard_map/ppermute | solution.py:417
  81.0 0.0 collective-permute-done.8.refs_4_
  81.0 0.0 copy-done.1
  81.0 0.0 copy-done.2
  81.0 0.0 copy-done.5
  81.0 0.0 copy-done.3
  81.0 0.7 copy-done.6
  81.7 0.1 copy-done.7
  81.8 16.1 %attend.1 = bf16[8,2,64,256]{3,2,1,0:T(8,128)(2,1)} custom-call(s32[1]{0:T(128)} %bitcast.place_ref, bf16[2,512,256]{2,1,0:T(8,128)(2,1)} %get-tuple-element.35.q_ref, bf16[2,256,512]{2,1,0:T(8,128)(2,1)} %copy-done.3, bf16[2,512,512]{2,1,0:T(8,128)(2,1)} %get-tuple-element.37.pair_ref, bf16[2,192,512]{2,1,0:T(8,128)(2,1)} %copy-done.5, ...), custom_call_target="tpu_custom_call" | custom-call | tf_op jit(solution)/shard_map/attend/pallas_call | solution.py:287
  97.9 14.5 %all_to_all.16.att_ref = bf16[8,128,256]{2,1,0:T(8,128)(2,1)} all-to-all(bf16[8,128,256]{2,1,0:T(8,128)(2,1)} %bitcast.10), channel_id=1, replica_groups=mesh['sp'=16,'tp'=8] {'tp'}, dimensions={0} | all-to-all | bytes 1048576 | tf_op jit(solution)/shard_map/all_to_all | solution.py:424
  112.4 5.2 %finish.1 = bf16[2,64,2048]{2,1,0:T(8,128)(2,1)} custom-call(bf16[8,128,256]{2,1,0:T(8,128)(2,1)} %all_to_all.16.att_ref, bf16[2048,2048]{1,0:T(8,128)(2,1)} %all-gather.5.cloned.1.call-done.w_ref, bf16[2,64,2048]{2,1,0:T(8,128)(2,1)} %latent_ref.1, f32[8,8,256]{2,1,0:T(8,128)} %all_to_all.15.tiles_ref.tile_ref), custom_call_target="tpu_custom_call" | custom-call | tf_op jit(solution)/shard_map/finish/pallas_call | solution.py:328
  (10 shorter events, 0.1 us)
Async XLA Ops:
  6.5 37.3 %all-gather.3.cloned.1.call-start = ((), (), s32[]{:S(2)}) async-start(), calls=%async_computation.3 | async-start | bytes 4718592 | tf_op jit(solution)/shard_map/all_gather | solution.py:376
  7.3 105.1 %all-gather.5.cloned.1.call-start = ((), (), s32[]{:S(2)}) async-start(), calls=%async_computation.4 | async-start | bytes 9437184 | tf_op jit(solution)/shard_map/all_gather | solution.py:379
  9.1 14.2 %all-to-all-start = ((f32[16,8,256]{2,1,0:T(8,128)}), f32[16,8,256]{2,1,0:T(8,128)S(1)}, u32[]{:S(2)}, u32[]{:S(2)}) async-start(f32[16,8,256]{2,1,0:T(8,128)} %modulation_parts.1), calls=%async_computation | async-start | bytes 262144 | tf_op jit(solution)/shard_map/all_to_all | solution.py:381
  37.3 12.2 %copy-start.4 = (bf16[1,128,512]{2,1,0:T(8,128)(2,1)S(1)}, bf16[1,128,512]{2,1,0:T(8,128)(2,1)}, u32[]{:S(2)}) copy-start(bf16[1,128,512]{2,1,0:T(8,128)(2,1)} %project.3) | copy-start | bytes 393220
  37.3 12.2 %collective-permute-start = (bf16[2,64,512]{2,1,0:T(8,128)(2,1)}, bf16[2,64,512]{2,1,0:T(8,128)(2,1)S(1)}, u32[]{:S(2)}, u32[]{:S(2)}) collective-permute-start(bf16[2,64,512]{2,1,0:T(8,128)(2,1)} %bitcast.12), channel_id=1, source_target_pairs={{0,8},{8,16},{16,24},{24,0},{32,40},{40,48},{48,56},{56,32},{64,72... | collective-permute-start | bytes 393224 | tf_op jit(solution)/shard_map/ppermute | solution.py:351
  37.8 11.7 %collective-permute-start.1 = (bf16[2,64,512]{2,1,0:T(8,128)(2,1)}, bf16[2,64,512]{2,1,0:T(8,128)(2,1)S(1)}, u32[]{:S(2)}, u32[]{:S(2)}) collective-permute-start(bf16[2,64,512]{2,1,0:T(8,128)(2,1)} %bitcast.13), channel_id=1, source_target_pairs={{0,16},{8,24},{16,0},{24,8},{32,48},{40,56},{48,32},{56,40},{64,80... | collective-permute-start | bytes 393224 | tf_op jit(solution)/shard_map/ppermute | solution.py:351
  40.0 9.5 %collective-permute-start.2 = (bf16[2,64,512]{2,1,0:T(8,128)(2,1)}, bf16[2,64,512]{2,1,0:T(8,128)(2,1)S(1)}, u32[]{:S(2)}, u32[]{:S(2)}) collective-permute-start(bf16[2,64,512]{2,1,0:T(8,128)(2,1)} %bitcast.14), channel_id=1, source_target_pairs={{0,24},{8,0},{16,8},{24,16},{32,56},{40,32},{48,40},{56,48},{64,88... | collective-permute-start | bytes 393224 | tf_op jit(solution)/shard_map/ppermute | solution.py:351
  49.6 7.8 %copy-start = (bf16[4,2,64,512]{3,2,1,0:T(8,128)(2,1)}, bf16[4,2,64,512]{3,2,1,0:T(8,128)(2,1)S(1)}, u32[]{:S(2)}) copy-start(bf16[4,2,64,512]{3,2,1,0:T(8,128)(2,1)S(1)} %pad_maximum_fusion.refs_0_) | copy-start | bytes 1572868
  49.6 15.7 %collective-permute-start.5 = (bf16[4,2,64,512]{3,2,1,0:T(8,128)(2,1)S(1)}, bf16[4,2,64,512]{3,2,1,0:T(8,128)(2,1)S(1)}, u32[]{:S(2)}, u32[]{:S(2)}) collective-permute-start(bf16[4,2,64,512]{3,2,1,0:T(8,128)(2,1)S(1)} %pad_maximum_fusion.refs_0_), channel_id=1, source_target_pairs={{0,32},{8,40},{16,48},{24,56},{32,64},{40,72},{48,80},{56,88},{64,... | collective-permute-start | bytes 1572872 | tf_op jit(solution)/shard_map/ppermute | solution.py:405
  51.2 15.8 %collective-permute-start.6 = (bf16[4,2,64,512]{3,2,1,0:T(8,128)(2,1)S(1)}, bf16[4,2,64,512]{3,2,1,0:T(8,128)(2,1)S(1)}, u32[]{:S(2)}, u32[]{:S(2)}) collective-permute-start(bf16[4,2,64,512]{3,2,1,0:T(8,128)(2,1)S(1)} %pad_maximum_fusion.refs_0_), channel_id=1, source_target_pairs={{0,96},{8,104},{16,112},{24,120},{32,0},{40,8},{48,16},{56,24},{64... | collective-permute-start | bytes 1572872 | tf_op jit(solution)/shard_map/ppermute | solution.py:406
  57.4 18.1 %collective-permute-start.3 = (bf16[2,256,512]{2,1,0:T(8,128)(2,1)}, bf16[2,256,512]{2,1,0:T(8,128)(2,1)S(1)}, u32[]{:S(2)}, u32[]{:S(2)}) collective-permute-start(bf16[2,256,512]{2,1,0:T(8,128)(2,1)} %get-tuple-element.36), channel_id=1, source_target_pairs={{0,8},{8,16},{16,24},{24,32},{32,40},{40,48},{48,56},{56,64},{64,7... | collective-permute-start | bytes 1572872 | tf_op jit(solution)/shard_map/ppermute | solution.py:410
  60.8 13.1 %collective-permute-start.4 = (bf16[2,192,512]{2,1,0:T(8,128)(2,1)}, bf16[2,192,512]{2,1,0:T(8,128)(2,1)S(1)}, u32[]{:S(2)}, u32[]{:S(2)}) collective-permute-start(bf16[2,192,512]{2,1,0:T(8,128)(2,1)} %get-tuple-element.38), channel_id=1, source_target_pairs={{8,0},{16,8},{24,16},{32,24},{40,32},{48,40},{56,48},{64,56},{72,6... | collective-permute-start | bytes 1179656 | tf_op jit(solution)/shard_map/ppermute | solution.py:411
  65.4 15.6 %copy-start.1 = (bf16[4,2,64,512]{3,2,1,0:T(8,128)(2,1)}, bf16[4,2,64,512]{3,2,1,0:T(8,128)(2,1)S(1)}, u32[]{:S(2)}) copy-start(bf16[4,2,64,512]{3,2,1,0:T(8,128)(2,1)S(1)} %collective-permute-done.5.refs_1_) | copy-start | bytes 1572868
  65.4 15.6 %collective-permute-start.7 = (bf16[2,2,64,512]{3,2,1,0:T(8,128)(2,1)S(1)}, bf16[2,2,64,512]{3,2,1,0:T(8,128)(2,1)S(1)}, u32[]{:S(2)}, u32[]{:S(2)}) collective-permute-start(bf16[2,2,64,512]{3,2,1,0:T(8,128)(2,1)S(1)} %slice.8), channel_id=1, source_target_pairs={{0,32},{8,40},{16,48},{24,56},{32,64},{40,72},{48,80},{56,88},{64,... | collective-permute-start | bytes 786440 | tf_op jit(solution)/shard_map/ppermute | solution.py:417
  67.0 13.9 %copy-start.2 = (bf16[4,2,64,512]{3,2,1,0:T(8,128)(2,1)}, bf16[4,2,64,512]{3,2,1,0:T(8,128)(2,1)S(1)}, u32[]{:S(2)}) copy-start(bf16[4,2,64,512]{3,2,1,0:T(8,128)(2,1)S(1)} %collective-permute-done.6.refs_2_) | copy-start | bytes 1572868
  67.1 13.9 %collective-permute-start.8 = (bf16[2,2,64,512]{3,2,1,0:T(8,128)(2,1)S(1)}, bf16[2,2,64,512]{3,2,1,0:T(8,128)(2,1)S(1)}, u32[]{:S(2)}, u32[]{:S(2)}) collective-permute-start(bf16[2,2,64,512]{3,2,1,0:T(8,128)(2,1)S(1)} %slice.9), channel_id=1, source_target_pairs={{0,96},{8,104},{16,112},{24,120},{32,0},{40,8},{48,16},{56,24},{64... | collective-permute-start | bytes 786440 | tf_op jit(solution)/shard_map/ppermute | solution.py:418
  73.9 7.1 %copy-start.5 = (bf16[2,192,512]{2,1,0:T(8,128)(2,1)}, bf16[2,192,512]{2,1,0:T(8,128)(2,1)S(1)}, u32[]{:S(2)}) copy-start(bf16[2,192,512]{2,1,0:T(8,128)(2,1)S(1)} %collective-permute-done.4.after_ref) | copy-start | bytes 1179652
  75.5 5.6 %copy-start.3 = (bf16[2,256,512]{2,1,0:T(8,128)(2,1)}, bf16[2,256,512]{2,1,0:T(8,128)(2,1)S(1)}, u32[]{:S(2)}) copy-start(bf16[2,256,512]{2,1,0:T(8,128)(2,1)S(1)} %collective-permute-done.3.before_ref) | copy-start | bytes 1572868
  81.0 0.7 copy-start.6
  81.0 0.8 copy-start.7
Sparse Core Ops, SparseCore 0:
  9.0 34.7 all-gather.2
  45.6 49.5 all-gather.4

commit v8 on v7

--- a/solution.py
+++ b/solution.py
@@ -14,6 +14,7 @@
 MASKED = -1e30
 REACH = WIN_ROWS // 2
 BIAS_BLOCKS = 7
+RESIDENT = pl.BlockSpec(memory_space=pltpu.VMEM)
 
 
 def copy_for_each(shard, axis):
@@ -55,8 +56,13 @@
         + [pl.BlockSpec(memory_space=pltpu.VMEM)] * 5,
         out_shape=jax.ShapeDtypeStruct((copies, 3 * samples + 2, cols), jnp.float32),
         scratch_shapes=[pltpu.VMEM((1, ctx_cond.shape[0]), jnp.float32)],
+        compiler_params=pltpu.CompilerParams(vmem_limit_bytes=16 * 2**20),
         name="modulation_parts",
     )(place, cond, ctx_cond, *weights)
+
+
+def resident(array):
+    return pltpu.with_memory_space_constraint(array, pltpu.VMEM)
 
 
 def whole(shape):
@@ -136,13 +142,14 @@
     return pl.pallas_call(
         body,
         grid=(len(chosen), steps),
-        in_specs=[blocks(width), whole((1, width)), whole(modulation.shape)]
-        + [whole(weight.shape) for weight in weights]
+        in_specs=[blocks(width), whole((1, width)), RESIDENT]
+        + [RESIDENT] * len(weights)
         + [pl.BlockSpec(memory_space=pl.ANY)] * len(buffers),
         out_specs=out_specs,
         out_shape=[jax.ShapeDtypeStruct(shape, jnp.bfloat16) for shape in out_shape],
         scratch_shapes=[pltpu.VMEM((1, width), jnp.float32)] * 2,
         input_output_aliases={3 + len(weights) + i: i for i in range(len(buffers))},
+        compiler_params=pltpu.CompilerParams(vmem_limit_bytes=24 * 2**20),
         name="project",
     )(rows, gain, modulation, *weights, *buffers)
 
@@ -179,6 +186,7 @@
     return pl.pallas_call(
         body,
         out_shape=jax.ShapeDtypeStruct((2, heads * GRID_W, BIAS_BLOCKS * 128), jnp.float32),
+        compiler_params=pltpu.CompilerParams(vmem_limit_bytes=16 * 2**20),
         name="bias_table",
     )(padded)
 
@@ -199,35 +207,35 @@
     def body(place_ref, q_ref, before_ref, pair_ref, after_ref, *refs):
         ctx_refs = refs[: len(members)]
         table_ref, cb_ref, out_ref, near_t, far_t, values, far_values = refs[len(members) :]
-        step = pl.program_id(1)
+        sample, step = pl.program_id(0), pl.program_id(1)
 
         @pl.when(step == 0)
         def _():
-            values[0:ahead] = before_ref[0, :, cols:]
+            values[0:ahead] = before_ref[sample, :, cols:]
             values[ahead : ahead + tokens] = pair_ref[0, :, cols:]
-            values[ahead + tokens : padded] = after_ref[0, :, cols:]
+            values[ahead + tokens : padded] = after_ref[sample, :, cols:]
             at = 0
             for ctx_ref, count in zip(ctx_refs, members):
                 for member in range(count):
                     low = at + member * ctx_rows
-                    far_values[low : low + ctx_rows] = ctx_ref[member, 0, :, cols:]
+                    far_values[low : low + ctx_rows] = ctx_ref[member, sample, :, cols:]
                 size = count * ctx_rows
                 block = jnp.concatenate(
-                    [ctx_ref[member, 0, :, :cols] for member in range(count)], axis=0
+                    [ctx_ref[member, sample, :, :cols] for member in range(count)], axis=0
                 )
                 far_t[:, at : at + size] = block.T
                 at += size
             fill = jnp.zeros((lanes - padded, cols), bf16)
-            near_t[0, :, :ahead] = before_ref[0, :, :cols].T
+            near_t[0, :, :ahead] = before_ref[sample, :, :cols].T
             near_t[0, :, ahead : ahead + tokens] = pair_ref[0, :, :cols].T
             near_t[0, :, ahead + tokens :] = jnp.concatenate(
-                [after_ref[0, :, :cols], fill], axis=0
+                [after_ref[sample, :, :cols], fill], axis=0
             ).T
             near_t[1] = jnp.concatenate(
                 [
-                    before_ref[0, GRID_W:, :cols],
+                    before_ref[sample, GRID_W:, :cols],
                     pair_ref[0, :, :cols],
-                    after_ref[0, :, :cols],
+                    after_ref[sample, :, :cols],
                     fill,
                     jnp.zeros((GRID_W, cols), bf16),
                 ],
@@ -290,15 +298,12 @@
         in_specs=[
             pl.BlockSpec(memory_space=pltpu.SMEM),
             pl.BlockSpec((1, per * GRID_W, cols), lambda s, i: (s, i, 0)),
-            of_sample(before),
+            RESIDENT,
             of_sample(pair),
-            of_sample(after),
+            RESIDENT,
         ]
-        + [
-            pl.BlockSpec((count, 1, ctx_rows, 2 * cols), lambda s, i: (0, s, 0, 0))
-            for count in members
-        ]
-        + [whole(table.shape), pl.BlockSpec(memory_space=pltpu.SMEM)],
+        + [RESIDENT] * len(members)
+        + [RESIDENT, pl.BlockSpec(memory_space=pltpu.SMEM)],
         out_specs=pl.BlockSpec((per, 1, GRID_W, cols), lambda s, i: (i, s, 0, 0)),
         out_shape=jax.ShapeDtypeStruct((rows_dev, samples, GRID_W, cols), bf16),
         scratch_shapes=[
@@ -307,6 +312,7 @@
             pltpu.VMEM((padded, cols), bf16),
             pltpu.VMEM((ctx_count, cols), bf16),
         ],
+        compiler_params=pltpu.CompilerParams(vmem_limit_bytes=32 * 2**20),
         name="attend",
     )(place, query, before, pair, after, *ctx_pairs, table, ctx_bias)
 
@@ -318,10 +324,13 @@
     first = modulation.shape[1] - samples
 
     def body(att_ref, w_ref, latent_ref, tile_ref, out_ref):
+        low = pl.program_id(0) * tiles
         everything = jnp.concatenate([att_ref[group] for group in range(groups)], axis=1)
         update = jnp.dot(everything, w_ref[...], preferred_element_type=jnp.float32)
         for s in range(samples):
-            gate = modulation_row(tile_ref, first + s)
+            gate = jnp.concatenate(
+                [tile_ref[low + t, first + s : first + s + 1, :] for t in range(tiles)], axis=1
+            )
             part = update[s * tokens : (s + 1) * tokens]
             out_ref[s] = (latent_ref[s].astype(jnp.float32) + gate * part).astype(jnp.bfloat16)
 
@@ -332,10 +341,11 @@
             whole(attended.shape),
             pl.BlockSpec((width, block), lambda i: (0, i)),
             pl.BlockSpec((samples, tokens, block), lambda i: (0, 0, i)),
-            pl.BlockSpec((tiles, *modulation.shape[1:]), lambda i: (i, 0, 0)),
+            RESIDENT,
         ],
         out_specs=pl.BlockSpec((samples, tokens, block), lambda i: (0, 0, i)),
         out_shape=jax.ShapeDtypeStruct(latent.shape, latent.dtype),
+        compiler_params=pltpu.CompilerParams(vmem_limit_bytes=24 * 2**20),
         name="finish",
     )(attended, w_out, latent, modulation)
 
@@ -380,7 +390,9 @@
     table = bias_table(rel_bias)
     summed = jnp.sum(lax.all_to_all(parts, "sp", 0, 0, tiled=True), axis=0)
     summed, table = lax.optimization_barrier((summed, table))
-    modulation = copy_for_each(summed, "tp")
+    modulation = resident(copy_for_each(summed, "tp"))
+    w_query, w_key, w_value = resident(w_query), resident(w_key), resident(w_value)
+    table = resident(table)
 
     gain = norm_gain[None, :]
     ctx_rows = context.shape[1]
@@ -407,8 +419,8 @@
     for s in range(1, samples):
         outs = project(gathered, gain, modulation, w_triple, 0, 256, ends, s, outs)
     pair, query, first, last = outs
-    before = lax.ppermute(last, "sp", up)
-    after = lax.ppermute(first, "sp", down)
+    before = resident(lax.ppermute(last, "sp", up))
+    after = resident(lax.ppermute(first, "sp", down))
     rows_all = pair.shape[1] // GRID_W * sp_size
     ctx_pairs = [
         ctx_line,
@@ -417,6 +429,7 @@
         lax.ppermute(below[:2], "sp", shifted(sp_size, 4, 4, 1)),
         lax.ppermute(above[2:], "sp", shifted(sp_size, 4, 4, 3)),
     ]
+    ctx_pairs = [resident(array) for array in ctx_pairs]
     attended = attend(
         place, query, before, pair, after, ctx_pairs, table, ctx_bias, rows_all, 4
     )

time: 126 us -> 125 us (level)
  Pallas kernels: 40.5 us -> 23.8 us
  local copies, waits for them, and re-layouts: 2.18 us -> 12.7 us
  waiting for transfers between devices: 18.4 us -> 23.4 us
  blocking collectives: 25.4 us -> 23.9 us
    ppermute x1, waiting for transfers between devices: 0.01 us -> 11.7 us  [computation(): below = lax.ppermute(ctx_line, 'sp', shifted(sp_size, 4, 4, 1))]
    unnamed x17 -> x33, local copies, waits for them, and re-layouts: 1.53 us -> 12.7 us
    pallas_call x3, Pallas kernels: 14.4 us -> 5.61 us  [project(): pl.pallas_call(body, grid=(len(chosen), steps), in_specs=[blocks(width),...]
    ppermute x2, waiting for transfers between devices: 7.84 us -> 0.01 us  [the longest x1 0.01 us: computation(): after = resident(lax.ppermute(first, 'sp', down))]
    pallas_call x1, Pallas kernels: 16.1 us -> 13.5 us  [attend(): pl.pallas_call(body, grid=(samples, rows_dev // per), in_specs=[pl.BlockS...]
    pallas_call x1, Pallas kernels: 5.24 us -> 2.78 us  [finish(): pl.pallas_call(body, grid=(width // block,), in_specs=[whole(attended.sha...]
    pallas_call x1, Pallas kernels: 2.99 us -> 1 us  [bias_table(): pl.pallas_call(body, out_shape=jax.ShapeDtypeStruct((2, heads * GRID_W, B...]
    all_gather x1, waiting for transfers between devices: 2.4 us -> 0.66 us  [computation(): gathered = lax.all_gather(latent, 'tp', axis=1, tiled=True)]
  transfers between devices with their start and end apart: 12 -> 12, of which waited for: 5 -> 6; matrix products, arithmetic and copies ran while one was open for 1% -> 2% of each run, Pallas kernels for 28% -> 17%
where the time goes in v8:
time: 125 us; the launch traced here: 124 us
  starting transfers between devices  25.4 us (20%)
  blocking collectives  23.9 us (19%)
  Pallas kernels  23.8 us (19%)
  waiting for transfers between devices  23.4 us (19%)
  between operations  13.6 us (11%)
  local copies, waits for them, and re-layouts  12.7 us (10%)
    pallas_call x1, Pallas kernels, attend(): pl.pallas_call(body, grid=(samples, rows_dev // per), in_specs=[pl.BlockS...  13.5 us
    all_to_all x1, blocking collectives, computation(): attended = lax.all_to_all(attended, 'tp', 0, 0, tiled=True)  13.1 us
    unnamed x33, local copies, waits for them, and re-layouts  12.7 us
    ppermute x1, waiting for transfers between devices, computation(): below = lax.ppermute(ctx_line, 'sp', shifted(sp_size, 4, 4, 1))  11.7 us
    all_to_all x1, blocking collectives, copy_for_each(): lax.all_to_all(jnp.broadcast_to(shard[None], (length, *shard.shape)), axi...  10.8 us
    all_to_all x1, starting transfers between devices, computation(): summed = jnp.sum(lax.all_to_all(parts, 'sp', 0, 0, tiled=True), axis=0)  7.91 us
    ppermute x1, starting transfers between devices, computation(): after = resident(lax.ppermute(first, 'sp', down))  5.71 us
    pallas_call x3, Pallas kernels, project(): pl.pallas_call(body, grid=(len(chosen), steps), in_specs=[blocks(width),...  5.61 us
  transfers between devices with their start and end apart: 12, of which 6 were waited for; matrix products, arithmetic and copies ran while one was open for 2% of the time, Pallas kernels for 17%

profile of v8, /device:TPU:32, one launch (start us, length us, event | category | flops | bytes accessed | tf_op | source)
XLA Modules:
  0.0 123.9 jit_solution(17004438289649276917)
XLA Ops:
  6.5 0.0 all-gather.3.cloned.1.call-start
  6.6 0.7 all-gather.3.cloned.1.call-update
  7.3 0.0 all-gather.5.cloned.1.call-start
  7.3 1.0 copy-done.10
  8.3 0.8 copy-done.11
  9.2 0.8 copy-done.12
  10.0 0.7 copy-done.13
  10.7 0.7 copy-done.14
  11.4 0.8 modulation_parts.1
  12.2 0.0 all-gather.5.cloned.1.call-update
  12.3 7.9 %all-to-all-start = ((f32[16,8,256]{2,1,0:T(8,128)}), f32[16,8,256]{2,1,0:T(8,128)S(1)}, u32[]{:S(2)}, u32[]{:S(2)}) async-start(f32[16,8,256]{2,1,0:T(8,128)} %modulation_parts.1), calls=%async_computation | async-start | bytes 262144 | tf_op jit(solution)/shard_map/all_to_all | solution.py:391
  20.2 0.8 copy.20
  20.9 1.0 bias_table.1.refs_5_
  22.0 1.2 copy-done.4
  23.2 3.3 %all-to-all-done = f32[16,8,256]{2,1,0:T(8,128)S(1)} async-done(((f32[16,8,256]{2,1,0:T(8,128)}), f32[16,8,256]{2,1,0:T(8,128)S(1)}, u32[]{:S(2)}, u32[]{:S(2)}) %all-to-all-start) | async-done | bytes 131104 | tf_op jit(solution)/shard_map/all_to_all | solution.py:391
  26.5 10.8 %all_to_all.15.tiles_ref.tile_ref = f32[8,8,256]{2,1,0:T(8,128)S(1)} all-to-all(f32[8,8,256]{2,1,0:T(8,128)S(1)} %broadcast_in_dim.14), channel_id=1, replica_groups=mesh['sp'=16,'tp'=8] {'tp'}, dimensions={0} | all-to-all | bytes 131072 | tf_op jit(solution)/shard_map/all_to_all | solution.py:22
  37.3 0.0 copy-start.8
  37.3 1.0 copy-done.8
  38.4 0.6 project.3
  39.0 0.6 collective-permute-start
  39.6 2.2 %collective-permute-start.1 = (bf16[2,64,512]{2,1,0:T(8,128)(2,1)S(1)}, bf16[2,64,512]{2,1,0:T(8,128)(2,1)}, u32[]{:S(2)}, u32[]{:S(2)}) collective-permute-start(bf16[2,64,512]{2,1,0:T(8,128)(2,1)S(1)} %bitcast.13), channel_id=1, source_target_pairs={{0,16},{8,24},{16,0},{24,8},{32,48},{40,56},{48,32},{56,40},{64,80... | collective-permute-start | bytes 393224 | tf_op jit(solution)/shard_map/ppermute | solution.py:361
  41.8 1.4 %collective-permute-start.2 = (bf16[2,64,512]{2,1,0:T(8,128)(2,1)S(1)}, bf16[2,64,512]{2,1,0:T(8,128)(2,1)}, u32[]{:S(2)}, u32[]{:S(2)}) collective-permute-start(bf16[2,64,512]{2,1,0:T(8,128)(2,1)S(1)} %bitcast.14), channel_id=1, source_target_pairs={{0,24},{8,0},{16,8},{24,16},{32,56},{40,32},{48,40},{56,48},{64,88... | collective-permute-start | bytes 393224 | tf_op jit(solution)/shard_map/ppermute | solution.py:361
  43.2 0.7 all-gather.3.cloned.1.call-done.rows_ref
  43.9 2.2 %copy-done = bf16[2,512,2048]{2,1,0:T(8,128)(2,1)S(1)} copy-done((bf16[2,512,2048]{2,1,0:T(8,128)(2,1)S(1)}, bf16[2,512,2048]{2,1,0:T(8,128)(2,1)}, u32[]{:S(2)}) %copy-start) | copy-done | bytes 4194328
  46.0 2.5 %project.4 = (bf16[2,512,512]{2,1,0:T(8,128)(2,1)S(1)}, bf16[2,512,256]{2,1,0:T(8,128)(2,1)S(1)}, bf16[2,192,512]{2,1,0:T(8,128)(2,1)S(1)}, bf16[2,256,512]{2,1,0:T(8,128)(2,1)S(1)}) custom-call(bf16[2,512,2048]{2,1,0:T(8,128)(2,1)S(1)} %copy-done, f32[1,2048]{1,0:T(1,128)S(1)} %bitcast.18, f32[8,8,256]{2,1,0:T(8,128)S(1)} %all_to_all.15.tiles_ref.tile_ref, ...), custom_call_target="tpu_custom_call" | custom-call | tf_op jit(solution)/shard_map/project/pallas_call | solution.py:142
  48.6 0.0 collective-permute-done
  48.6 0.0 collective-permute-done.1
  48.6 0.2 collective-permute-done.2
  48.7 1.0 pad_maximum_fusion.refs_0_
  49.8 0.0 copy-start.15
  49.8 1.5 %collective-permute-start.5 = (bf16[4,2,64,512]{3,2,1,0:T(8,128)(2,1)S(1)}, bf16[4,2,64,512]{3,2,1,0:T(8,128)(2,1)S(1)}, u32[]{:S(2)}, u32[]{:S(2)}) collective-permute-start(bf16[4,2,64,512]{3,2,1,0:T(8,128)(2,1)S(1)} %pad_maximum_fusion.refs_0_), channel_id=1, source_target_pairs={{0,32},{8,40},{16,48},{24,56},{32,64},{40,72},{48,80},{56,88},{64,... | collective-permute-start | bytes 1572872 | tf_op jit(solution)/shard_map/ppermute | solution.py:417
  51.3 0.6 collective-permute-start.6
  51.9 2.5 %project.5 = (bf16[2,512,512]{2,1,0:T(8,128)(2,1)S(1)}, bf16[2,512,256]{2,1,0:T(8,128)(2,1)S(1)}, bf16[2,192,512]{2,1,0:T(8,128)(2,1)S(1)}, bf16[2,256,512]{2,1,0:T(8,128)(2,1)S(1)}) custom-call(bf16[2,512,2048]{2,1,0:T(8,128)(2,1)S(1)} %copy-done, f32[1,2048]{1,0:T(1,128)S(1)} %bitcast.19, ...), custom_call_target="tpu_custom_call", output_to_operand_aliasing={{0}: (6, {}), {1}: (7, {}), {2}: (8, {}), {3}: (9, {})} | custom-call | tf_op jit(solution)/shard_map/project/pallas_call | solution.py:142
  54.4 3.2 %collective-permute-start.3 = (bf16[2,256,512]{2,1,0:T(8,128)(2,1)S(1)}, bf16[2,256,512]{2,1,0:T(8,128)(2,1)S(1)}, u32[]{:S(2)}, u32[]{:S(2)}) collective-permute-start(bf16[2,256,512]{2,1,0:T(8,128)(2,1)S(1)} %get-tuple-element.36), channel_id=1, source_target_pairs={{0,8},{8,16},{16,24},{24,32},{32,40},{40,48},{48,56},{56,64},{64,7... | collective-permute-start | bytes 1572872 | tf_op jit(solution)/shard_map/ppermute | solution.py:422
  57.6 5.7 %collective-permute-start.4 = (bf16[2,192,512]{2,1,0:T(8,128)(2,1)S(1)}, bf16[2,192,512]{2,1,0:T(8,128)(2,1)S(1)}, u32[]{:S(2)}, u32[]{:S(2)}) collective-permute-start(bf16[2,192,512]{2,1,0:T(8,128)(2,1)S(1)} %get-tuple-element.38), channel_id=1, source_target_pairs={{8,0},{16,8},{24,16},{32,24},{40,32},{48,40},{56,48},{64,56},{72,6... | collective-permute-start | bytes 1179656 | tf_op jit(solution)/shard_map/ppermute | solution.py:423
  63.4 11.7 %collective-permute-done.5.refs_1_ = bf16[4,2,64,512]{3,2,1,0:T(8,128)(2,1)S(1)} collective-permute-done((bf16[4,2,64,512]{3,2,1,0:T(8,128)(2,1)S(1)}, bf16[4,2,64,512]{3,2,1,0:T(8,128)(2,1)S(1)}, u32[]{:S(2)}, u32[]{:S(2)}) %collective-permute-start.5) | collective-permute-done | bytes 524320 | tf_op jit(solution)/shard_map/ppermute | solution.py:417
  75.0 0.0 copy-start.7
  75.1 1.6 %collective-permute-start.7 = (bf16[2,2,64,512]{3,2,1,0:T(8,128)(2,1)S(1)}, bf16[2,2,64,512]{3,2,1,0:T(8,128)(2,1)S(1)}, u32[]{:S(2)}, u32[]{:S(2)}) collective-permute-start(bf16[2,2,64,512]{3,2,1,0:T(8,128)(2,1)S(1)} %slice.8), channel_id=1, source_target_pairs={{0,32},{8,40},{16,48},{24,56},{32,64},{40,72},{48,80},{56,88},{64,... | collective-permute-start | bytes 786440 | tf_op jit(solution)/shard_map/ppermute | solution.py:429
  76.7 0.0 collective-permute-done.6.refs_2_
  76.7 0.5 collective-permute-start.8
  77.2 0.0 collective-permute-done.4.after_ref
  77.3 0.0 collective-permute-done.3.before_ref
  77.3 5.4 %collective-permute-done.7.refs_3_ = bf16[2,2,64,512]{3,2,1,0:T(8,128)(2,1)S(1)} collective-permute-done((bf16[2,2,64,512]{3,2,1,0:T(8,128)(2,1)S(1)}, bf16[2,2,64,512]{3,2,1,0:T(8,128)(2,1)S(1)}, u32[]{:S(2)}, u32[]{:S(2)}) %collective-permute-start.7) | collective-permute-done | bytes 262176 | tf_op jit(solution)/shard_map/ppermute | solution.py:429
  82.7 1.5 %collective-permute-done.8.refs_4_ = bf16[2,2,64,512]{3,2,1,0:T(8,128)(2,1)S(1)} collective-permute-done((bf16[2,2,64,512]{3,2,1,0:T(8,128)(2,1)S(1)}, bf16[2,2,64,512]{3,2,1,0:T(8,128)(2,1)S(1)}, u32[]{:S(2)}, u32[]{:S(2)}) %collective-permute-start.8) | collective-permute-done | bytes 262176 | tf_op jit(solution)/shard_map/ppermute | solution.py:430
  84.2 13.5 %attend.1 = bf16[8,2,64,256]{3,2,1,0:T(8,128)(2,1)S(1)} custom-call(s32[1]{0:T(128)} %bitcast.place_ref, bf16[2,512,256]{2,1,0:T(8,128)(2,1)S(1)} %get-tuple-element.35.q_ref, bf16[2,256,512]{2,1,0:T(8,128)(2,1)S(1)} %collective-permute-done.3.before_ref, bf16[2,512,512]{2,1,0:T(8,128)(2,1)S(1)} %get-tuple-element.37.pair_ref, ...), custom_call_target="tpu_custom_call" | custom-call | tf_op jit(solution)/shard_map/attend/pallas_call | solution.py:295
  97.7 13.1 %all_to_all.16.att_ref = bf16[8,128,256]{2,1,0:T(8,128)(2,1)S(1)} all-to-all(bf16[8,128,256]{2,1,0:T(8,128)(2,1)S(1)} %bitcast.10), channel_id=1, replica_groups=mesh['sp'=16,'tp'=8] {'tp'}, dimensions={0} | all-to-all | bytes 1048576 | tf_op jit(solution)/shard_map/all_to_all | solution.py:437
  110.8 3.4 %copy-done.3 = bf16[2048,2048]{1,0:T(8,128)(2,1)S(1)} copy-done((bf16[2048,2048]{1,0:T(8,128)(2,1)S(1)}, bf16[2048,2048]{1,0:T(8,128)(2,1)}, u32[]{:S(2)}) %copy-start.3) | copy-done | bytes 8388632
  114.2 2.8 %finish.1 = bf16[2,64,2048]{2,1,0:T(8,128)(2,1)} custom-call(bf16[8,128,256]{2,1,0:T(8,128)(2,1)S(1)} %all_to_all.16.att_ref, bf16[2048,2048]{1,0:T(8,128)(2,1)S(1)} %copy-done.3, bf16[2,64,2048]{2,1,0:T(8,128)(2,1)S(1)} %copy-done.7, f32[8,8,256]{2,1,0:T(8,128)S(1)} %all_to_all.15.tiles_ref.tile_ref), custom_call_target="tpu_custom_call" | custom-call | tf_op jit(solution)/shard_map/finish/pallas_call | solution.py:337
  (26 shorter events, 0.1 us)
Async XLA Ops:
  6.5 30.8 %copy-start.9 = (f32[2048]{0:T(1024)S(1)}, f32[2048]{0:T(1024)}, u32[]{:S(2)}) copy-start(f32[2048]{0:T(1024)} %param.21) | copy-start | bytes 24580
  6.5 30.8 %copy-start.1 = (bf16[2048,256]{1,0:T(8,128)(2,1)S(1)}, bf16[2048,256]{1,0:T(8,128)(2,1)}, u32[]{:S(2)}) copy-start(bf16[2048,256]{1,0:T(8,128)(2,1)} %refs_0_.5) | copy-start | bytes 3145732
  6.5 30.8 %copy-start.2 = (bf16[2048,256]{1,0:T(8,128)(2,1)S(1)}, bf16[2048,256]{1,0:T(8,128)(2,1)}, u32[]{:S(2)}) copy-start(bf16[2048,256]{1,0:T(8,128)(2,1)} %refs_1_.5) | copy-start | bytes 3145732
  6.5 37.3 %copy-start.6 = (bf16[2048,256]{1,0:T(8,128)(2,1)S(1)}, bf16[2048,256]{1,0:T(8,128)(2,1)}, u32[]{:S(2)}) copy-start(bf16[2048,256]{1,0:T(8,128)(2,1)} %refs_2_.3) | copy-start | bytes 3145732
  6.5 37.3 %all-gather.3.cloned.1.call-start = ((), (), s32[]{:S(2)}) async-start(), calls=%async_computation.3 | async-start | bytes 4718592 | tf_op jit(solution)/shard_map/all_gather | solution.py:386
  7.3 103.6 %all-gather.5.cloned.1.call-start = ((), (), s32[]{:S(2)}) async-start(), calls=%async_computation.4 | async-start | bytes 9437184 | tf_op jit(solution)/shard_map/all_gather | solution.py:389
  7.3 1.0 copy-start.10
  8.3 0.8 copy-start.11
  9.2 0.8 copy-start.12
  10.0 0.7 copy-start.13
  10.7 0.7 copy-start.14
  12.3 14.2 %all-to-all-start = ((f32[16,8,256]{2,1,0:T(8,128)}), f32[16,8,256]{2,1,0:T(8,128)S(1)}, u32[]{:S(2)}, u32[]{:S(2)}) async-start(f32[16,8,256]{2,1,0:T(8,128)} %modulation_parts.1), calls=%async_computation | async-start | bytes 262144 | tf_op jit(solution)/shard_map/all_to_all | solution.py:391
  21.9 1.2 copy-start.4
  37.3 1.1 copy-start.8
  39.0 9.6 %collective-permute-start = (bf16[2,64,512]{2,1,0:T(8,128)(2,1)S(1)}, bf16[2,64,512]{2,1,0:T(8,128)(2,1)S(1)}, u32[]{:S(2)}, u32[]{:S(2)}) collective-permute-start(bf16[2,64,512]{2,1,0:T(8,128)(2,1)S(1)} %bitcast.12), channel_id=1, source_target_pairs={{0,8},{8,16},{16,24},{24,0},{32,40},{40,48},{48,56},{56,32},{64,72... | collective-permute-start | bytes 393224 | tf_op jit(solution)/shard_map/ppermute | solution.py:361
  39.6 9.0 %collective-permute-start.1 = (bf16[2,64,512]{2,1,0:T(8,128)(2,1)S(1)}, bf16[2,64,512]{2,1,0:T(8,128)(2,1)}, u32[]{:S(2)}, u32[]{:S(2)}) collective-permute-start(bf16[2,64,512]{2,1,0:T(8,128)(2,1)S(1)} %bitcast.13), channel_id=1, source_target_pairs={{0,16},{8,24},{16,0},{24,8},{32,48},{40,56},{48,32},{56,40},{64,80... | collective-permute-start | bytes 393224 | tf_op jit(solution)/shard_map/ppermute | solution.py:361
  41.8 7.0 %collective-permute-start.2 = (bf16[2,64,512]{2,1,0:T(8,128)(2,1)S(1)}, bf16[2,64,512]{2,1,0:T(8,128)(2,1)}, u32[]{:S(2)}, u32[]{:S(2)}) collective-permute-start(bf16[2,64,512]{2,1,0:T(8,128)(2,1)S(1)} %bitcast.14), channel_id=1, source_target_pairs={{0,24},{8,0},{16,8},{24,16},{32,56},{40,32},{48,40},{56,48},{64,88... | collective-permute-start | bytes 393224 | tf_op jit(solution)/shard_map/ppermute | solution.py:361
  43.9 2.2 %copy-start = (bf16[2,512,2048]{2,1,0:T(8,128)(2,1)S(1)}, bf16[2,512,2048]{2,1,0:T(8,128)(2,1)}, u32[]{:S(2)}) copy-start(bf16[2,512,2048]{2,1,0:T(8,128)(2,1)} %all-gather.3.cloned.1.call-done.rows_ref) | copy-start | bytes 12582916
  49.8 34.4 %copy-start.5 = (f32[2,256,896]{2,1,0:T(8,128)S(1)}, f32[2,256,896]{2,1,0:T(8,128)}, u32[]{:S(2)}) copy-start(f32[2,256,896]{2,1,0:T(8,128)} %copy-done.4) | copy-start | bytes 5505028
  49.8 34.4 %copy-start.15 = (f32[4]{0:T(128)S(1)}, f32[4]{0:T(128)}, u32[]{:S(2)}) copy-start(f32[4]{0:T(128)} %refs_6_.1) | copy-start | bytes 52
  49.8 25.2 %collective-permute-start.5 = (bf16[4,2,64,512]{3,2,1,0:T(8,128)(2,1)S(1)}, bf16[4,2,64,512]{3,2,1,0:T(8,128)(2,1)S(1)}, u32[]{:S(2)}, u32[]{:S(2)}) collective-permute-start(bf16[4,2,64,512]{3,2,1,0:T(8,128)(2,1)S(1)} %pad_maximum_fusion.refs_0_), channel_id=1, source_target_pairs={{0,32},{8,40},{16,48},{24,56},{32,64},{40,72},{48,80},{56,88},{64,... | collective-permute-start | bytes 1572872 | tf_op jit(solution)/shard_map/ppermute | solution.py:417
  51.3 25.4 %collective-permute-start.6 = (bf16[4,2,64,512]{3,2,1,0:T(8,128)(2,1)S(1)}, bf16[4,2,64,512]{3,2,1,0:T(8,128)(2,1)S(1)}, u32[]{:S(2)}, u32[]{:S(2)}) collective-permute-start(bf16[4,2,64,512]{3,2,1,0:T(8,128)(2,1)S(1)} %pad_maximum_fusion.refs_0_), channel_id=1, source_target_pairs={{0,96},{8,104},{16,112},{24,120},{32,0},{40,8},{48,16},{56,24},{64... | collective-permute-start | bytes 1572872 | tf_op jit(solution)/shard_map/ppermute | solution.py:418
  54.4 22.8 %collective-permute-start.3 = (bf16[2,256,512]{2,1,0:T(8,128)(2,1)S(1)}, bf16[2,256,512]{2,1,0:T(8,128)(2,1)S(1)}, u32[]{:S(2)}, u32[]{:S(2)}) collective-permute-start(bf16[2,256,512]{2,1,0:T(8,128)(2,1)S(1)} %get-tuple-element.36), channel_id=1, source_target_pairs={{0,8},{8,16},{16,24},{24,32},{32,40},{40,48},{48,56},{56,64},{64,7... | collective-permute-start | bytes 1572872 | tf_op jit(solution)/shard_map/ppermute | solution.py:422
  57.6 19.6 %collective-permute-start.4 = (bf16[2,192,512]{2,1,0:T(8,128)(2,1)S(1)}, bf16[2,192,512]{2,1,0:T(8,128)(2,1)S(1)}, u32[]{:S(2)}, u32[]{:S(2)}) collective-permute-start(bf16[2,192,512]{2,1,0:T(8,128)(2,1)S(1)} %get-tuple-element.38), channel_id=1, source_target_pairs={{8,0},{16,8},{24,16},{32,24},{40,32},{48,40},{56,48},{64,56},{72,6... | collective-permute-start | bytes 1179656 | tf_op jit(solution)/shard_map/ppermute | solution.py:423
  75.0 35.8 %copy-start.7 = (bf16[2,64,2048]{2,1,0:T(8,128)(2,1)S(1)}, bf16[2,64,2048]{2,1,0:T(8,128)(2,1)}, u32[]{:S(2)}) copy-start(bf16[2,64,2048]{2,1,0:T(8,128)(2,1)} %latent_ref.1) | copy-start | bytes 1572868
  75.1 7.6 %collective-permute-start.7 = (bf16[2,2,64,512]{3,2,1,0:T(8,128)(2,1)S(1)}, bf16[2,2,64,512]{3,2,1,0:T(8,128)(2,1)S(1)}, u32[]{:S(2)}, u32[]{:S(2)}) collective-permute-start(bf16[2,2,64,512]{3,2,1,0:T(8,128)(2,1)S(1)} %slice.8), channel_id=1, source_target_pairs={{0,32},{8,40},{16,48},{24,56},{32,64},{40,72},{48,80},{56,88},{64,... | collective-permute-start | bytes 786440 | tf_op jit(solution)/shard_map/ppermute | solution.py:429
  76.7 7.5 %collective-permute-start.8 = (bf16[2,2,64,512]{3,2,1,0:T(8,128)(2,1)S(1)}, bf16[2,2,64,512]{3,2,1,0:T(8,128)(2,1)S(1)}, u32[]{:S(2)}, u32[]{:S(2)}) collective-permute-start(bf16[2,2,64,512]{3,2,1,0:T(8,128)(2,1)S(1)} %slice.9), channel_id=1, source_target_pairs={{0,96},{8,104},{16,112},{24,120},{32,0},{40,8},{48,16},{56,24},{64... | collective-permute-start | bytes 786440 | tf_op jit(solution)/shard_map/ppermute | solution.py:430
  110.8 3.4 %copy-start.3 = (bf16[2048,2048]{1,0:T(8,128)(2,1)S(1)}, bf16[2048,2048]{1,0:T(8,128)(2,1)}, u32[]{:S(2)}) copy-start(bf16[2048,2048]{1,0:T(8,128)(2,1)} %all-gather.5.cloned.1.call-done.w_ref) | copy-start | bytes 25165828
Sparse Core Ops, SparseCore 0:
  9.0 34.7 all-gather.2
  45.6 49.5 all-gather.4
